TPU v7x, 128 devices: a whole 4x4x4 slice. The times are simulated.
128 devices in a mesh: sp: 16 (over z, x), dp: 8 (over y, core).
Axes of the slice: x: 4, y: 4, z: 4, core: 2. Of those that a mesh axis runs over, the one named last changes fastest.
Arguments:
- queries: bfloat16 [8, 2048, 16, 128], P('dp', 'sp'), may hold values from -3.5 to 2
- key_rows: bfloat16 [8, 2048, 16, 128], P('dp', 'sp'), may hold values from -4 to 5.3
- values: bfloat16 [8, 2048, 16, 128], P('dp', 'sp'), may hold values from -6 to 6
- residual: bfloat16 [8, 2048, 4096], P('dp', 'sp'), may hold values from -6 to 6
- out_weight: bfloat16 [2048, 4096], P(None, 'dp'), may hold values from -0.125 to 0.125
- mixer_gain: float32 [4096], replicated, may hold values from 0.1 to 1.9
- expert_gain: float32 [4096], replicated, may hold values from 0.1 to 1.9
- gate_weight: bfloat16 [128, 4096, 512], P(('sp', 'dp')), may hold values from -0.09375 to 0.09375
- up_weight: bfloat16 [128, 4096, 512], P(('sp', 'dp')), may hold values from -0.09375 to 0.09375
- expert_down_matrix: bfloat16 [128, 512, 4096], P(('sp', 'dp')), may hold values from -0.25 to 0.25
- routes: int32 [8, 2048, 2], P('dp', 'sp'), may hold values from 0 to 127, all different within a row; in each aligned block of 128 rows (0 to 127, 128 to 255, ..., all dimensions but the last counted through in order) at most 3 rows name the same one
- route_weight: float32 [8, 2048, 2], P('dp', 'sp'), may hold values from 0.1 to 1
- output_gain: float32 [4096], replicated, may hold values from 0.1 to 1.9
Outputs:
- output: bfloat16 [8, 2048, 4096], P('dp', 'sp')
Inputs may be any that keep to these rules, and one draw needn't show every extreme that they name: `routes`: each row names 2 different experts. Among the rows of one device no expert is named more than 3 times, and in every draw some device names some expert exactly 3 times.
All inputs are finite; a program needn't handle non-finite values.
Results may differ from a plain program's by a relative error of at most 0.009.
Values may be sent and summed in bfloat16 or wider, within the bound.
No kernel may reach another device: no remote copies, remote signals or barrier semaphores. Data moves between devices by JAX's collectives and lax.ppermute only.
A program may use at most 192 MiB of HBM per device.

v0:
```python
import jax
import jax.numpy as jnp
from jax import lax
from jax.sharding import PartitionSpec as P

EPSILON = 1e-06


def in_one_piece(arrays, axis, split_dim, concat_dim, along):
    widths = [a.shape[along] for a in arrays]
    both = jnp.concatenate(arrays, axis=along)
    whole = lax.all_to_all(both, axis, split_axis=split_dim, concat_axis=concat_dim, tiled=True)
    return tuple(jnp.split(whole, [sum(widths[:k]) for k in range(1, len(widths))], axis=along))


def normed_token_rows(matrix, gain):
    return matrix * lax.rsqrt(jnp.mean(matrix * matrix, axis=-1, keepdims=True) + EPSILON) * gain


def attend(query_rows, key_part, value_part):
    length = query_rows.shape[0]
    block_rows = min(512, length)
    score_scale = query_rows.shape[2] ** (-0.5)
    pieces = []
    for block_index in range(length // block_rows):
        row_start = block_index * block_rows
        row_stop = row_start + block_rows
        scores = (
            jnp.einsum(
                "qhd,khd->hqk",
                query_rows[row_start:row_stop],
                key_part[:row_stop],
                preferred_element_type=jnp.float32,
            )
            * score_scale
        )
        key_pos = lax.broadcasted_iota(jnp.int32, (1, block_rows, row_stop), 2)
        query_pos = lax.broadcasted_iota(jnp.int32, (1, block_rows, row_stop), 1) + row_start
        is_past = key_pos < query_pos
        log_keep = jnp.where(is_past, -jax.nn.softplus(scores), 0.0)
        suffix = lax.cumsum(log_keep, axis=2, reverse=True) - log_keep
        weights = jnp.where(is_past, jnp.exp(jax.nn.log_sigmoid(scores) + suffix), 0.0).astype(
            jnp.bfloat16
        )
        pieces.append(
            jnp.einsum(
                "hqk,khd->qhd", weights, value_part[:row_stop], preferred_element_type=jnp.float32
            ).astype(jnp.bfloat16)
        )
    return jnp.concatenate(pieces, axis=0)


def local(
    queries,
    key_rows,
    values,
    residual,
    out_weight,
    mixer_gain,
    expert_gain,
    gate_weight,
    up_weight,
    expert_down_matrix,
    routes,
    route_weight,
    output_gain,
):
    head_queries, head_keys, head_values = in_one_piece((queries, key_rows, values), "sp", 2, 1, 0)
    attended = attend(head_queries[0], head_keys[0], head_values[0])
    token_major = lax.all_to_all(attended[None], "sp", split_axis=1, concat_axis=2, tiled=True)
    local_rows = token_major.shape[1]
    flat_attn = token_major.reshape(local_rows, -1)
    projected = jnp.dot(
        flat_attn,
        lax.all_gather(out_weight, "dp", axis=1, tiled=True),
        preferred_element_type=jnp.float32,
    )
    stream = (residual[0].astype(jnp.float32) + normed_token_rows(projected, mixer_gain)).astype(
        jnp.bfloat16
    )
    expert_in = normed_token_rows(stream.astype(jnp.float32), expert_gain).astype(jnp.bfloat16)
    feature_count = expert_in.shape[1]
    experts = lax.axis_size("sp") * lax.axis_size("dp")
    top_count = routes.shape[2]
    capacity = max(2, 3 * local_rows // experts)
    picked_experts = routes[0].reshape(local_rows * top_count)
    onehot = (
        picked_experts[:, None]
        == lax.broadcasted_iota(jnp.int32, (local_rows * top_count, experts), 1)
    ).astype(jnp.int32)
    before = jnp.cumsum(onehot, axis=0) - onehot
    slot_rank = jnp.sum(before * onehot, axis=1)
    slot_index = slot_rank * experts + picked_experts
    source_row = lax.iota(jnp.int32, local_rows * top_count) // top_count
    slot_rows = (
        jnp.full((capacity * experts,), local_rows, jnp.int32).at[slot_index].set(source_row)
    )
    padded = jnp.concatenate([expert_in, jnp.zeros((1, feature_count), jnp.bfloat16)], axis=0)
    outgoing = jnp.take(padded, slot_rows, axis=0).reshape(capacity, experts, feature_count)
    arrived = lax.all_to_all(outgoing, ("sp", "dp"), split_axis=1, concat_axis=1, tiled=True)
    slot_count, sources, width_now = arrived.shape
    flat_rows = arrived.reshape(slot_count * sources, width_now)
    gate_out = jnp.dot(flat_rows, gate_weight[0], preferred_element_type=jnp.float32)
    upward = jnp.dot(flat_rows, up_weight[0], preferred_element_type=jnp.float32)
    hidden = (jax.nn.silu(gate_out) * upward).astype(jnp.bfloat16)
    result = jnp.dot(hidden, expert_down_matrix[0], preferred_element_type=jnp.float32).astype(
        jnp.bfloat16
    )
    returned = lax.all_to_all(
        result.reshape(slot_count, sources, width_now),
        ("sp", "dp"),
        split_axis=1,
        concat_axis=1,
        tiled=True,
    )
    gathered = jnp.take(returned.reshape(capacity * experts, feature_count), slot_index, axis=0)
    gathered = gathered.reshape(local_rows, top_count, feature_count)
    combined = jnp.sum(gathered.astype(jnp.float32) * route_weight[0][:, :, None], axis=1)
    output = (stream.astype(jnp.float32) + normed_token_rows(combined, output_gain)).astype(
        jnp.bfloat16
    )
    return output[None]


def solution(mesh):
    in_specs = (
        P("dp", "sp", None, None),
        P("dp", "sp", None, None),
        P("dp", "sp", None, None),
        P("dp", "sp", None),
        P(None, "dp"),
        P(),
        P(),
        P(("sp", "dp"), None, None),
        P(("sp", "dp"), None, None),
        P(("sp", "dp"), None, None),
        P("dp", "sp", None),
        P("dp", "sp", None),
        P(),
    )
    out_specs = P("dp", "sp", None)
    return jax.shard_map(local, mesh=mesh, in_specs=in_specs, out_specs=out_specs, check_vma=False)
```

profile of v0, /device:TPU:1, one launch (start us, length us, event | category | flops | bytes accessed | tf_op | source)
XLA Modules:
  0.0 382.3 jit_solution(1991847294519843783)
XLA Ops:
  10.1 8.4 %all-to-all-start = ((bf16[3,128,16,128]{3,1,0,2:T(8,128)(2,1)}), bf16[3,128,16,128]{3,1,0,2:T(8,128)(2,1)S(1)}, u32[]{:S(2)}, u32[]{:S(2)}) async-start(bf16[3,128,16,128]{3,1,0,2:T(8,128)(2,1)} %pad_maximum_fusion), calls=%async_computation | async-start | bytes 3145728 | tf_op jit(solution)/shard_map/all_to_all | solution.py:12
  20.3 2.2 scatter_custom_fusion
  23.7 17.9 %all-to-all-done = bf16[3,128,16,128]{3,1,0,2:T(8,128)(2,1)S(1)} async-done(((bf16[3,128,16,128]{3,1,0,2:T(8,128)(2,1)}), bf16[3,128,16,128]{3,1,0,2:T(8,128)(2,1)S(1)}, u32[]{:S(2)}, u32[]{:S(2)}) %all-to-all-start) | async-done | bytes 1572896 | tf_op jit(solution)/shard_map/all_to_all | solution.py:12
  41.8 1.6 fusion.68
  43.5 4.8 %fusion.70 = f32[1,512,4,128]{1,2,3,0:T(4,128)S(1)} fusion(f32[1,512,4,128]{1,3,2,0:T(8,128)S(1)} %bitcast.200), kind=kOutput, calls=%fused_computation.89 | output fusion | flops 33292288 | bytes 2097152 | tf_op jit(solution)/shard_map/reduce-window
  50.4 5.2 %fusion.22 = (f32[512,1536]{1,0:T(8,128)}, f32[512,1536]{1,0:T(8,128)}) fusion(s32[512]{0:T(512)S(1)} %iota_add_fusion.1, bf16[512,128]{1,0:T(8,128)(2,1)S(1)} %bitcast.211, bf16[1536,128]{1,0:T(8,128)(2,1)S(1)} %bitcast.209), kind=kOutput, calls=%fused_computation.38 | convolution fusion | flops 209190912 | bytes 6817792 | tf_op jit(solution)/shard_map/qhd,khd->hqk/dot_general | solution.py:29
  55.6 4.3 %copy.119 = f32[512,1536]{0,1:T(8,128)} copy(f32[512,1536]{1,0:T(8,128)} %get-tuple-element.19) | data formatting | bytes 6291456 | tf_op jit(solution)/shard_map/jit(_where)/select_n | solution.py:40
  60.0 11.8 %fusion.13 = f32[1,512,12,128]{1,2,3,0:T(8,128)S(1)} fusion(f32[1,512,12,128]{1,3,2,0:T(8,128)} %bitcast.185), kind=kOutput, calls=%fused_computation.25 | output fusion | flops 99876864 | bytes 6291456 | tf_op jit(solution)/shard_map/reduce-window.4
  71.8 3.7 copy.121
  76.4 2.1 broadcast.172
  78.4 3.7 copy.123
  82.1 3.6 copy.122
  86.9 1.6 fusion.38
  88.4 1.8 copy.143
  90.2 3.2 copy.116
  93.4 7.2 %fusion.95 = f32[1,512,8,128]{1,2,3,0:T(8,128)} fusion(f32[1,512,8,128]{1,2,3,0:T(8,128)} %copy.116), kind=kOutput, calls=%fused_computation.143 | output fusion | flops 66584576 | bytes 4194304 | tf_op jit(solution)/shard_map/reduce-window.2
  100.6 3.1 copy.117
  106.2 3.1 fusion.15
  109.4 2.9 copy.146
  112.2 5.8 %copy.124 = f32[1,512,16,128]{1,2,3,0:T(8,128)} copy(f32[1,512,16,128]{3,2,1,0:T(8,128)} %bitcast.178) | data formatting | bytes 8388608 | tf_op jit(solution)/shard_map/reshape.15
  118.0 12.8 %fusion.96 = f32[1,512,16,128]{1,2,3,0:T(8,128)} fusion(f32[1,512,16,128]{1,2,3,0:T(8,128)} %copy.124), kind=kOutput, calls=%fused_computation.144 | output fusion | flops 133169152 | bytes 8388608 | tf_op jit(solution)/shard_map/reduce-window.6
  130.8 5.9 %copy.125 = f32[1,512,16,128]{3,2,1,0:T(8,128)} copy(f32[1,512,16,128]{1,2,3,0:T(8,128)} %fusion.96) | data formatting | bytes 8388608 | tf_op jit(solution)/shard_map/reduce-window.6
  136.7 1.5 slice_bitcast_fusion.1
  138.2 1.5 reduce-window.45
  139.7 1.4 slice_bitcast_fusion
  141.1 1.6 copy.126
  142.8 2.3 fusion.66
  146.1 4.2 %fusion.54 = bf16[512,1,128]{0,2,1:T(8,128)(2,1)S(1)} fusion(bf16[1024,128]{1,0:T(8,128)(2,1)S(1)} %bitcast.210, f32[64,8,8,128]{3,2,1,0:T(8,128)S(1)} %bitcast.197, f32[64,8,8,128]{3,2,1,0:T(8,128)S(1)} %bitcast.198, f32[512,1024]{1,0:T(8,128)S(1)} %copy-done.6, s32[512]{0:T(512)S(1)} %copy-done.28), kind=kOutput, calls=%fused_computation.76 | convolution fusion | flops 146341888 | bytes 6686720 | tf_op jit(solution)/shard_map/hqk,khd->qhd/dot_general | solution.py:46
  150.4 5.0 %fusion.58 = bf16[512,1,128]{0,2,1:T(8,128)(2,1)S(1)} fusion(bf16[1536,128]{1,0:T(8,128)(2,1)S(1)} %bitcast.208, f32[512,1536]{1,0:T(8,128)S(1)} %copy-done.10, f32[512,1536]{1,0:T(8,128)S(1)} %copy-done.9, f32[512,1536]{1,0:T(8,128)S(1)} %copy-done.37, s32[512]{0:T(512)S(1)} %copy-done.34), kind=kOutput, calls=%fused_computation.78 | convolution fusion | flops 218693632 | bytes 9963520 | tf_op jit(solution)/shard_map/hqk,khd->qhd/dot_general | solution.py:46
  157.5 7.5 %fusion.55 = bf16[512,1,128]{0,2,1:T(8,128)(2,1)S(1)} fusion(bf16[2048,128]{1,0:T(8,128)(2,1)S(1)} %bitcast.207, f32[64,8,16,128]{3,2,1,0:T(8,128)S(1)} %bitcast.190, f32[64,8,16,128]{3,2,1,0:T(8,128)S(1)} %bitcast.189, f32[512,2048]{1,0:T(8,128)S(1)} %copy-done.2, s32[512]{0:T(512)S(1)} %copy-done.26), kind=kOutput, calls=%fused_computation.77 | convolution fusion | flops 292618240 | bytes 13240320 | tf_op jit(solution)/shard_map/hqk,khd->qhd/dot_general | solution.py:46
  166.4 11.7 %reduce = bf16[2048,128]{1,0:T(8,128)(2,1)S(1)} reduce(bf16[2048,1,1,128]{3,2,1,0:T(2,128)(2,1)S(1)} %bitcast.191, bf16[]{:T(256)} %broadcast.196), dimensions={1,2}, to_apply=%bitcast.151.reduce_sub_computation | reduce | bytes 1048578
  179.1 4.4 %all-to-all-start.1 = ((bf16[16,2,8192]{2,1,0:T(2,128)(2,1)}), bf16[16,2,8192]{2,1,0:T(2,128)(2,1)S(1)}, u32[]{:S(2)}, u32[]{:S(2)}) async-start(bf16[16,2,8192]{2,1,0:T(2,128)(2,1)} %reshape.457), calls=%async_computation.1 | async-start | bytes 1048576 | tf_op jit(solution)/shard_map/all_to_all | solution.py:70
  183.6 9.9 %all-to-all-done.1 = bf16[16,2,8192]{2,1,0:T(2,128)(2,1)S(1)} async-done(((bf16[16,2,8192]{2,1,0:T(2,128)(2,1)}), bf16[16,2,8192]{2,1,0:T(2,128)(2,1)S(1)}, u32[]{:S(2)}, u32[]{:S(2)}) %all-to-all-start.1) | async-done | bytes 524320 | tf_op jit(solution)/shard_map/all_to_all | solution.py:70
  194.5 8.3 %multiply_reduce_fusion.2 = (f32[128]{0:T(128)S(1)}, f32[128,4096]{1,0:T(8,128)S(1)}) fusion(bf16[128,2048]{0,1:T(8,128)(2,1)S(1)} %bitcast.195, bf16[2048,4096]{1,0:T(8,128)(2,1)} %all-gather.2.cloned.1.call-done), kind=kOutput, calls=%fused_computation.61 | convolution fusion | flops 2148532224 | bytes 19399168 | tf_op jit(solution)/shard_map/dot_general | solution.py:73
  204.9 4.0 %gather_fusion = bf16[384,4096]{1,0:T(8,128)(2,1)} fusion(bf16[129,4096]{1,0:T(8,128)(2,1)S(1)} %concatenate.11, s32[1024]{0:T(1024)S(1)} %pad_clamp_fusion.1), kind=kCustom, calls=%fused_computation | custom fusion | bytes 6292992 | tf_op jit(solution)/shard_map/jit(_take)/gather | solution.py:99
  209.0 5.0 %copy_select_fusion = bf16[3,128,4096]{2,0,1:T(4,128)(2,1)S(1)} fusion(bf16[3,128,4096]{2,1,0:T(8,128)(2,1)} %bitcast.183, pred[3,128]{0,1:T(8,128)(4,1)S(1)} %copy.136), kind=kLoop, calls=%fused_computation.24 | loop fusion | flops 1572864 | bytes 6291840 | tf_op jit(solution)/shard_map/jit(_take)/select_n | solution.py:99
  214.0 60.9 %all_to_all.40 = bf16[3,128,4096]{2,0,1:T(4,128)(2,1)S(1)} all-to-all(bf16[3,128,4096]{2,0,1:T(4,128)(2,1)S(1)} %copy_select_fusion), channel_id=1, replica_groups=mesh['sp'=16,'dp'=8] {'sp','dp'}, dimensions={1} | all-to-all | bytes 6291456 | tf_op jit(solution)/shard_map/all_to_all | solution.py:100
  275.0 2.3 copy.138
  277.2 2.7 fusion.11
  280.0 8.9 %convolution_convert_fusion = bf16[384,4096]{1,0:T(8,128)(2,1)} fusion(bf16[1,512,4096]{2,1,0:T(8,128)(2,1)} %param.22, bf16[384,4096]{1,0:T(8,128)(2,1)S(1)} %bitcast.193, bf16[1,4096,512]{2,1,0:T(8,128)(2,1)} %param.21, f32[384,512]{1,0:T(8,128)} %fusion.11), kind=kOutput, calls=%fused_computation.9 | convolution fusion | flops 3223977984 | bytes 15466496 | tf_op jit(solution)/shard_map/dot_general | solution.py:106
  288.9 6.5 %copy.139 = bf16[3,128,4096]{2,0,1:T(4,128)(2,1)} copy(bf16[3,128,4096]{2,1,0:T(8,128)(2,1)} %bitcast.194) | data formatting | bytes 6291456 | tf_op jit(solution)/shard_map/reshape | solution.py:110
  295.4 5.6 %all-to-all-start.3 = ((bf16[3,128,4096]{2,0,1:T(4,128)(2,1)}), bf16[3,128,4096]{2,0,1:T(4,128)(2,1)}, u32[]{:S(2)}, u32[]{:S(2)}) async-start(bf16[3,128,4096]{2,0,1:T(4,128)(2,1)} %copy.139), calls=%async_computation.3 | async-start | bytes 8388608 | tf_op jit(solution)/shard_map/all_to_all | solution.py:109
  301.6 52.3 %all-to-all-done.3 = bf16[3,128,4096]{2,0,1:T(4,128)(2,1)} async-done(((bf16[3,128,4096]{2,0,1:T(4,128)(2,1)}), bf16[3,128,4096]{2,0,1:T(4,128)(2,1)}, u32[]{:S(2)}, u32[]{:S(2)}) %all-to-all-start.3) | async-done | bytes 3145760 | tf_op jit(solution)/shard_map/all_to_all | solution.py:109
  353.9 4.5 %copy.140 = bf16[3,128,4096]{2,1,0:T(8,128)(2,1)S(1)} copy(bf16[3,128,4096]{2,0,1:T(4,128)(2,1)} %all-to-all-done.3) | data formatting | bytes 6291456 | tf_op jit(solution)/shard_map/all_to_all | solution.py:109
  358.4 3.2 gather_fusion.1
  361.6 3.3 gather.15
  364.9 8.7 %multiply_reduce_fusion = f32[128,4096]{1,0:T(8,128)S(1)} fusion(bf16[128,2,4096]{2,1,0:T(2,128)(2,1)S(1)} %gather.15, pred[128,2]{1,0:T(8,128)(4,1)S(1)} %copy.134, f32[128,2]{1,0:T(8,128)S(1)} %copy.141), kind=kLoop, calls=%fused_computation.27 | loop fusion | flops 3670016 | bytes 4195584 | tf_op jit(solution)/shard_map/reduce_sum | solution.py:118
  373.9 1.4 fusion.61
  (147 shorter events, 22.5 us)
Async XLA Ops:
  6.5 1.9 copy-start.14
  6.5 2.1 copy-start.15
  6.5 187.9 %all-gather.2.cloned.1.call-start = ((), (), s32[]{:S(2)}) async-start(), calls=%async_computation.4 | async-start | bytes 18874368 | tf_op jit(solution)/shard_map/all_gather | solution.py:75
  8.7 9.8 %copy-start.29 = (s32[1,128,2]{1,2,0:T(2,128)S(1)}, s32[1,128,2]{1,2,0:T(2,128)}, u32[]{:S(2)}) copy-start(s32[1,128,2]{1,2,0:T(2,128)} %param.23) | copy-start | bytes 3076
  10.1 31.5 %all-to-all-start = ((bf16[3,128,16,128]{3,1,0,2:T(8,128)(2,1)}), bf16[3,128,16,128]{3,1,0,2:T(8,128)(2,1)S(1)}, u32[]{:S(2)}, u32[]{:S(2)}) async-start(bf16[3,128,16,128]{3,1,0,2:T(8,128)(2,1)} %pad_maximum_fusion), calls=%async_computation | async-start | bytes 3145728 | tf_op jit(solution)/shard_map/all_to_all | solution.py:12
  19.7 0.6 copy-start.23
  20.3 3.4 copy-start.31
  22.5 27.9 %copy-start.33 = (s32[512]{0:T(512)}, s32[512]{0:T(512)S(1)}, u32[]{:S(2)}) copy-start(s32[512]{0:T(512)S(1)} %iota_add_fusion.1) | copy-start | bytes 6148
  71.8 3.7 copy-start
  85.7 1.2 copy-start.27
  86.9 3.3 copy-start.5
  104.6 1.6 copy-start.25
  106.2 3.1 copy-start.1
  130.8 11.9 %copy-start.8 = (f32[1,512,4,128]{1,3,2,0:T(8,128)S(1)}, f32[1,512,4,128]{1,3,2,0:T(8,128)}, u32[]{:S(2)}) copy-start(f32[1,512,4,128]{1,3,2,0:T(8,128)} %copy.115) | copy-start | bytes 3145732
  136.7 9.2 %copy-start.6 = (f32[512,1024]{1,0:T(8,128)S(1)}, f32[512,1024]{1,0:T(8,128)}, u32[]{:S(2)}) copy-start(f32[512,1024]{1,0:T(8,128)} %copy-done.5) | copy-start | bytes 6291460
  142.7 3.2 copy-start.11
  142.7 3.3 copy-start.18
  142.7 3.3 copy-start.28
  146.0 4.3 %copy-start.9 = (f32[512,1536]{1,0:T(8,128)S(1)}, f32[512,1536]{1,0:T(8,128)}, u32[]{:S(2)}) copy-start(f32[512,1536]{1,0:T(8,128)} %copy.123) | copy-start | bytes 9437188
  146.0 4.3 %copy-start.10 = (f32[512,1536]{1,0:T(8,128)S(1)}, f32[512,1536]{1,0:T(8,128)}, u32[]{:S(2)}) copy-start(f32[512,1536]{1,0:T(8,128)} %copy.122) | copy-start | bytes 9437188
  146.0 4.3 %copy-start.17 = (bf16[1,12,128,1,128]{4,2,1,3,0:T(8,128)(2,1)S(1)}, bf16[1,12,128,1,128]{4,2,1,3,0:T(8,128)(2,1)}, u32[]{:S(2)}) copy-start(bf16[1,12,128,1,128]{4,2,1,3,0:T(8,128)(2,1)} %get-tuple-element.16) | copy-start | bytes 1179652
  146.0 4.3 %copy-start.34 = (s32[512]{0:T(512)S(1)}, s32[512]{0:T(512)}, u32[]{:S(2)}) copy-start(s32[512]{0:T(512)} %copy-done.33) | copy-start | bytes 6148
  146.0 4.3 %copy-start.37 = (f32[512,1536]{1,0:T(8,128)S(1)}, f32[512,1536]{1,0:T(8,128)}, u32[]{:S(2)}) copy-start(f32[512,1536]{1,0:T(8,128)} %get-tuple-element.20) | copy-start | bytes 9437188
  150.3 5.0 %copy-start.13 = (f32[512,16]{1,0:T(8,128)S(1)}, f32[512,16]{1,0:T(8,128)}, u32[]{:S(2)}) copy-start(f32[512,16]{1,0:T(8,128)} %copy.126) | copy-start | bytes 98308
  150.3 6.2 %copy-start.7 = (f32[1,512,16,128]{3,2,1,0:T(8,128)S(1)}, f32[1,512,16,128]{3,2,1,0:T(8,128)}, u32[]{:S(2)}) copy-start(f32[1,512,16,128]{3,2,1,0:T(8,128)} %copy.125) | copy-start | bytes 12582916
  150.3 6.2 %copy-start.16 = (bf16[1,16,128,1,128]{4,2,1,3,0:T(8,128)(2,1)S(1)}, bf16[1,16,128,1,128]{4,2,1,3,0:T(8,128)(2,1)}, u32[]{:S(2)}) copy-start(bf16[1,16,128,1,128]{4,2,1,3,0:T(8,128)(2,1)} %get-tuple-element.18) | copy-start | bytes 1572868
  155.3 2.2 copy-start.2
  155.4 2.2 copy-start.26
  165.1 18.3 %copy-start.19 = (s32[384]{0:T(512)S(1)}, s32[384]{0:T(512)}, u32[]{:S(2)}) copy-start(s32[384]{0:T(512)} %scatter_custom_fusion) | copy-start | bytes 4612
  179.1 14.5 %all-to-all-start.1 = ((bf16[16,2,8192]{2,1,0:T(2,128)(2,1)}), bf16[16,2,8192]{2,1,0:T(2,128)(2,1)S(1)}, u32[]{:S(2)}, u32[]{:S(2)}) async-start(bf16[16,2,8192]{2,1,0:T(2,128)(2,1)} %reshape.457), calls=%async_computation.1 | async-start | bytes 1048576 | tf_op jit(solution)/shard_map/all_to_all | solution.py:70
  194.5 8.3 %copy-start.12 = (bf16[1,128,4096]{2,1,0:T(8,128)(2,1)S(1)}, bf16[1,128,4096]{2,1,0:T(8,128)(2,1)}, u32[]{:S(2)}) copy-start(bf16[1,128,4096]{2,1,0:T(8,128)(2,1)} %param.16) | copy-start | bytes 3145732
  194.5 8.3 %copy-start.20 = (f32[4096]{0:T(1024)S(1)}, f32[4096]{0:T(1024)}, u32[]{:S(2)}) copy-start(f32[4096]{0:T(1024)} %param.18) | copy-start | bytes 49156
  202.8 1.7 copy-start.21
  203.5 1.0 copy-start.3
  274.9 2.3 copy-start.36
  295.4 5.6 %copy-start.24 = (s32[256]{0:T(256)S(1)}, s32[256]{0:T(256)}, u32[]{:S(2)}) copy-start(s32[256]{0:T(256)} %copy-done.23) | copy-start | bytes 3076
  295.4 5.8 %copy-start.30 = (s32[1,128,2]{1,2,0:T(2,128)S(1)}, s32[1,128,2]{1,2,0:T(2,128)}, u32[]{:S(2)}) copy-start(s32[1,128,2]{1,2,0:T(2,128)} %param.23) | copy-start | bytes 3076
  295.4 6.0 %copy-start.35 = (f32[1,128,2]{1,2,0:T(2,128)S(1)}, f32[1,128,2]{1,2,0:T(2,128)}, u32[]{:S(2)}) copy-start(f32[1,128,2]{1,2,0:T(2,128)} %param.24) | copy-start | bytes 3076
  295.4 6.1 %copy-start.32 = (s32[256,1]{0,1:T(1,128)S(1)}, s32[256,1]{0,1:T(1,128)}, u32[]{:S(2)}) copy-start(s32[256,1]{0,1:T(1,128)} %copy-done.31) | copy-start | bytes 3076
  295.4 58.5 %all-to-all-start.3 = ((bf16[3,128,4096]{2,0,1:T(4,128)(2,1)}), bf16[3,128,4096]{2,0,1:T(4,128)(2,1)}, u32[]{:S(2)}, u32[]{:S(2)}) async-start(bf16[3,128,4096]{2,0,1:T(4,128)(2,1)} %copy.139), calls=%async_computation.3 | async-start | bytes 8388608 | tf_op jit(solution)/shard_map/all_to_all | solution.py:109
  364.9 9.0 %copy-start.4 = (bf16[128,4096]{1,0:T(8,128)(2,1)S(1)}, bf16[128,4096]{1,0:T(8,128)(2,1)}, u32[]{:S(2)}) copy-start(bf16[128,4096]{1,0:T(8,128)(2,1)} %copy-done.3) | copy-start | bytes 3145732
  364.9 9.0 %copy-start.22 = (f32[4096]{0:T(1024)S(1)}, f32[4096]{0:T(1024)}, u32[]{:S(2)}) copy-start(f32[4096]{0:T(1024)} %param.25) | copy-start | bytes 49156
Sparse Core Ops, SparseCore 0:
  9.0 88.5 all-gather.1
where the time goes:
time: 386 us; the launch traced here: 382 us
  local copies, waits for them, and re-layouts  86.5 us (22%)
  waiting for transfers between devices  80.8 us (21%)
  other arithmetic  76.4 us (20%)
  blocking collectives  60.9 us (16%)
  matrix products  44.9 us (12%)
  starting transfers between devices  18.4 us (5%)
  between operations  14.4 us (4%)
    all_to_all x1, blocking collectives, local(): lax.all_to_all(outgoing, ('sp', 'dp'), split_axis=1, concat_axis=1, tiled...  60.9 us
    all_to_all x1, waiting for transfers between devices, local(): lax.all_to_all(result.reshape(slot_count, sources, width_now), ('sp', 'dp...  52.3 us
    another operation x24, local copies, waits for them, and re-layouts  40.3 us
    another operation x11, other arithmetic  38.4 us
    all_to_all x1, waiting for transfers between devices, in_one_piece(): lax.all_to_all(both, axis, split_axis=split_dim, concat_axis=concat_dim,...  17.9 us
    dot_general x4, matrix products, attend(): jnp.einsum('hqk,khd->qhd', weights, value_part[:row_stop], preferred_elem...  17 us
    unnamed x3, other arithmetic  16.4 us
    unnamed x87, local copies, waits for them, and re-layouts  10.9 us
  transfers between devices with their start and end apart: 4, of which 3 were waited for; matrix products, arithmetic and copies ran while one was open for 38% of the time, Pallas kernels for 0%

commit v1 on v0

v1 whole, which is shorter than its diff:
```python
import functools
import math

import jax
import jax.numpy as jnp
from jax import lax
from jax.experimental import pallas as pl
from jax.experimental.pallas import tpu as pltpu
from jax.sharding import Mesh, PartitionSpec as P

EPSILON = 1e-06
F32 = jnp.float32
BF16 = jnp.bfloat16
DP = ("yh", "yl", "c")
ALL = ("sp", "yh", "yl", "c")
VMEM = pl.BlockSpec(memory_space=pltpu.VMEM)
SMEM = pl.BlockSpec(memory_space=pltpu.SMEM)


def attend_kernel(x_ref, o_ref):
    blocks, _, hd = x_ref.shape
    tile = 256
    scale = math.log2(math.e) * hd ** -0.5
    row = lax.broadcasted_iota(jnp.int32, (256, 256), 0) % 128
    col = lax.broadcasted_iota(jnp.int32, (256, 256), 1)
    sums = jnp.where((col >= 128) | (row > col), 1.0, 0.0).astype(BF16)
    query_pos = lax.broadcasted_iota(jnp.int32, (tile, 128), 0)
    key_pos = lax.broadcasted_iota(jnp.int32, (tile, 128), 1)

    def two(block, start):
        return jnp.concatenate(
            [x_ref[2 * block, start : start + 128], x_ref[2 * block + 1, start : start + 128]], axis=0
        )

    for i in range(blocks // 2):
        q = two(i, 0)
        carry, total = None, None
        for j in range(i, -1, -1):
            z = (
                lax.dot_general(q, two(j, 128), (((1,), (1,)), ((), ())), preferred_element_type=F32)
                * scale
            )
            weights = [None, None]
            for half in (1, 0):
                zh = z[:, half * 128 : half * 128 + 128]
                keep = jnp.maximum(zh, 0.0) + jnp.log2(1.0 + jnp.exp2(-jnp.abs(zh)))
                take = zh - keep
                if i == j:
                    past = key_pos + half * 128 < query_pos
                    keep = jnp.where(past, keep, 0.0)
                high = keep.astype(BF16)
                low = (keep - high.astype(F32)).astype(BF16)
                s = jnp.dot(jnp.concatenate([high, low], axis=1), sums, preferred_element_type=F32)
                e = take - s[:, :128]
                if carry is not None:
                    e = e - carry
                w = jnp.exp2(e)
                if i == j:
                    w = jnp.where(past, w, 0.0)
                weights[half] = w.astype(BF16)
                carry = s[:, 128:] if carry is None else carry + s[:, 128:]
            part = jnp.dot(
                jnp.concatenate(weights, axis=1), two(j, 256), preferred_element_type=F32
            )
            total = part if total is None else total + part
        total = total.astype(BF16)
        for copy in range(o_ref.shape[1]):
            o_ref[2 * i, copy] = total[:128]
            o_ref[2 * i + 1, copy] = total[128:]


def attend(x, copies):
    blocks = x.shape[0]
    return pl.pallas_call(
        attend_kernel,
        out_shape=jax.ShapeDtypeStruct((blocks, copies, 128, 128), BF16),
        in_specs=[VMEM],
        out_specs=VMEM,
        compiler_params=pltpu.CompilerParams(vmem_limit_bytes=24 << 20),
        cost_estimate=pl.CostEstimate(
            flops=12 * 10**9, bytes_accessed=3 * 10**6, transcendentals=7 * 10**6
        ),
        name="attend",
    )(x)


def project_kernel(index_ref, x_ref, w0, w1, w2, w3, own_ref, other_ref):
    mine = index_ref[0]
    heads = x_ref.shape[0]
    rows = [
        jnp.concatenate([x_ref[h, member] for h in range(heads)], axis=1)
        for member in (mine, 1 - mine)
    ]
    both = jnp.concatenate(rows, axis=0)
    for k, w_ref in enumerate((w0, w1, w2, w3)):
        for n in range(0, 512, 256):
            out = jnp.dot(both, w_ref[:, n : n + 256], preferred_element_type=F32)
            own_ref[k, :, n : n + 256] = out[:128]
            other_ref[k, :, n : n + 256] = out[128:].astype(BF16)


def project(index, x, ws):
    return pl.pallas_call(
        project_kernel,
        out_shape=(
            jax.ShapeDtypeStruct((4, 128, 512), F32),
            jax.ShapeDtypeStruct((4, 128, 512), BF16),
        ),
        in_specs=[SMEM, VMEM, VMEM, VMEM, VMEM, VMEM],
        out_specs=(VMEM, VMEM),
        compiler_params=pltpu.CompilerParams(vmem_limit_bytes=32 << 20),
        cost_estimate=pl.CostEstimate(flops=2 * 10**9, bytes_accessed=11 * 10**6, transcendentals=0),
        name="project",
    )(index, x, *ws)


def to_rows(inner, outer):
    i = lax.broadcasted_iota(jnp.int32, (256, 256), 0)
    k = lax.broadcasted_iota(jnp.int32, (256, 256), 1)
    return jnp.where(k == (i % inner) * outer + i // inner, 1.0, 0.0).astype(BF16)


def stack_blocks(lower, upper):
    left = jnp.concatenate([lower[:, c * 128 : c * 128 + 128] for c in range(32)], axis=0)
    right = jnp.concatenate([upper[:, c * 128 : c * 128 + 128] for c in range(32)], axis=0)
    return jnp.concatenate([left, right], axis=1)


def mix_kernel(
    place_ref, slot_ref, own_ref, got_ref, residual_ref, mixer_ref, expert_ref,
    stream_ref, out_ref, proj_ref, rows_ref,
):
    for k in range(4):
        proj_ref[:, pl.ds(pl.multiple_of(place_ref[k] * 512, 512), 512)] = own_ref[k]
        proj_ref[:, pl.ds(pl.multiple_of(place_ref[4 + k] * 512, 512), 512)] = got_ref[k].astype(F32)
    spread = to_rows(32, 8)
    width = proj_ref.shape[1]

    @pl.loop(0, proj_ref.shape[0] // 16)
    def _(g):
        at = pl.ds(pl.multiple_of(g * 16, 16), 16)
        p = proj_ref[at, :]
        r = lax.rsqrt(jnp.sum(p * p, axis=1, keepdims=True) * (1.0 / width) + EPSILON)
        stream = (residual_ref[at, :].astype(F32) + p * r * mixer_ref[...]).astype(BF16)
        s = stream.astype(F32)
        r = lax.rsqrt(jnp.sum(s * s, axis=1, keepdims=True) * (1.0 / width) + EPSILON)
        x = s * r * expert_ref[...]
        for value, ref in ((s, stream_ref), (x, rows_ref)):
            spread_out = jnp.dot(
                spread, stack_blocks(value[:8], value[8:]).astype(BF16), preferred_element_type=F32
            ).astype(BF16)
            ref[pl.ds(g * 16, 8)] = spread_out[:, :128].reshape(8, 32, 128)
            ref[pl.ds(g * 16 + 8, 8)] = spread_out[:, 128:].reshape(8, 32, 128)

    experts = out_ref.shape[0]

    @pl.loop(0, experts, unroll=4)
    def _(e):
        for slot in range(out_ref.shape[1] // 32):
            out_ref[e, slot * 32 : slot * 32 + 32, :] = rows_ref[slot_ref[slot * experts + e]]


def mix(place, slots, own, got, residual, mixer_gain, expert_gain):
    tokens, width = residual.shape
    return pl.pallas_call(
        mix_kernel,
        out_shape=(
            jax.ShapeDtypeStruct((tokens, 32, 128), BF16),
            jax.ShapeDtypeStruct((128, slots.shape[0] // 128 * 32, 128), BF16),
        ),
        in_specs=[SMEM, SMEM, VMEM, VMEM, VMEM, VMEM, VMEM],
        out_specs=(VMEM, VMEM),
        scratch_shapes=[pltpu.VMEM((tokens, width), F32), pltpu.VMEM((tokens, 32, 128), BF16)],
        compiler_params=pltpu.CompilerParams(vmem_limit_bytes=24 << 20),
        cost_estimate=pl.CostEstimate(flops=10**9, bytes_accessed=8 * 10**6, transcendentals=0),
        name="mix",
    )(place, slots, own, got, residual, mixer_gain, expert_gain)


def expert_kernel(x_ref, gate_ref, up_ref, down_ref, o_ref, rows_ref, hidden_ref, result_ref):
    sources = x_ref.shape[0]
    slots = x_ref.shape[1] // 32
    gather = to_rows(8, 32)
    spread = to_rows(32, 8)

    for slot in range(slots):

        @pl.loop(0, sources // 16)
        def _(g):
            at = slice(slot * 32, slot * 32 + 32)
            left = x_ref[pl.ds(g * 16, 8), at, :].reshape(256, 128)
            right = x_ref[pl.ds(g * 16 + 8, 8), at, :].reshape(256, 128)
            got = jnp.dot(
                gather, jnp.concatenate([left, right], axis=1), preferred_element_type=F32
            )
            to = pl.ds(pl.multiple_of(slot * sources + g * 16, 16), 16)
            for c in range(32):
                rows_ref[to, c * 128 : c * 128 + 128] = jnp.concatenate(
                    [got[c * 8 : c * 8 + 8, :128], got[c * 8 : c * 8 + 8, 128:]], axis=0
                ).astype(BF16)

    for n in range(0, 512, 256):
        a = jnp.dot(rows_ref[...], gate_ref[:, n : n + 256], preferred_element_type=F32)
        b = jnp.dot(rows_ref[...], up_ref[:, n : n + 256], preferred_element_type=F32)
        hidden_ref[:, n : n + 256] = (a / (1.0 + jnp.exp(-a)) * b).astype(BF16)

    @pl.loop(0, 16)
    def _(n):
        at = pl.ds(pl.multiple_of(n * 256, 256), 256)
        result_ref[:, at] = jnp.dot(hidden_ref[...], down_ref[:, at], preferred_element_type=F32)

    for slot in range(slots):

        @pl.loop(0, sources // 16)
        def _(g):
            base = slot * sources + g * 16
            lower = result_ref[pl.ds(pl.multiple_of(base, 8), 8), :]
            upper = result_ref[pl.ds(pl.multiple_of(base + 8, 8), 8), :]
            out = jnp.dot(
                spread, stack_blocks(lower, upper).astype(BF16), preferred_element_type=F32
            ).astype(BF16)
            at = slice(slot * 32, slot * 32 + 32)
            o_ref[pl.ds(g * 16, 8), at, :] = out[:, :128].reshape(8, 32, 128)
            o_ref[pl.ds(g * 16 + 8, 8), at, :] = out[:, 128:].reshape(8, 32, 128)


def run_experts(x, gate, up, down):
    rows = x.shape[0] * (x.shape[1] // 32)
    return pl.pallas_call(
        expert_kernel,
        out_shape=jax.ShapeDtypeStruct(x.shape, BF16),
        in_specs=[VMEM] * 4,
        out_specs=VMEM,
        scratch_shapes=[
            pltpu.VMEM((rows, 4096), BF16),
            pltpu.VMEM((rows, 512), BF16),
            pltpu.VMEM((rows, 4096), F32),
        ],
        compiler_params=pltpu.CompilerParams(vmem_limit_bytes=48 << 20),
        cost_estimate=pl.CostEstimate(flops=6 * 10**9, bytes_accessed=19 * 10**6, transcendentals=0),
        name="experts",
    )(x, gate, up, down)


def combine_kernel(expert_ref, rank_ref, weight_ref, x_ref, stream_ref, gain_ref, o_ref, out_ref):
    tokens = stream_ref.shape[0]
    gather = to_rows(8, 32)
    gain = gain_ref[...]

    @pl.loop(0, tokens, unroll=8)
    def _(t):
        total = None
        for k in range(2):
            rank = pl.multiple_of(rank_ref[2 * t + k] * 32, 32)
            part = x_ref[expert_ref[2 * t + k], pl.ds(rank, 32), :].astype(F32) * weight_ref[2 * t + k]
            total = part if total is None else total + part
        square = jnp.sum(jnp.sum(total * total, axis=0, keepdims=True), axis=1, keepdims=True)
        r = lax.rsqrt(square * (1.0 / 4096) + EPSILON)
        out_ref[t] = (stream_ref[t].astype(F32) + total * r * gain).astype(BF16)

    @pl.loop(0, tokens // 16)
    def _(g):
        left = out_ref[pl.ds(g * 16, 8)].reshape(256, 128)
        right = out_ref[pl.ds(g * 16 + 8, 8)].reshape(256, 128)
        got = jnp.dot(gather, jnp.concatenate([left, right], axis=1), preferred_element_type=F32)
        to = pl.ds(pl.multiple_of(g * 16, 16), 16)
        for c in range(32):
            o_ref[to, c * 128 : c * 128 + 128] = jnp.concatenate(
                [got[c * 8 : c * 8 + 8, :128], got[c * 8 : c * 8 + 8, 128:]], axis=0
            ).astype(BF16)


def combine(expert, rank, weight, x, stream, gain):
    tokens = stream.shape[0]
    return pl.pallas_call(
        combine_kernel,
        out_shape=jax.ShapeDtypeStruct((tokens, 4096), BF16),
        in_specs=[SMEM, SMEM, SMEM, VMEM, VMEM, VMEM],
        out_specs=VMEM,
        scratch_shapes=[pltpu.VMEM((tokens, 32, 128), BF16)],
        compiler_params=pltpu.CompilerParams(vmem_limit_bytes=24 << 20),
        cost_estimate=pl.CostEstimate(flops=10**9, bytes_accessed=6 * 10**6, transcendentals=0),
        name="combine",
    )(expert, rank, weight, x, stream, gain)


def local(
    queries, key_rows, values, residual, out_weight, mixer_gain, expert_gain,
    gate_weight, up_weight, expert_down_matrix, routes, route_weight, output_gain,
):
    yh, yl, core = (lax.axis_index(a) for a in DP)
    y = yh * 2 + yl

    swap = [(d, d ^ 1) for d in range(8)]
    across = [(d, 6 - d // 2 * 2 + d % 2) for d in range(8)]
    w_near = lax.ppermute(out_weight, DP, across)
    w_core = lax.ppermute(out_weight, DP, swap)
    w_near_core = lax.ppermute(w_near, DP, swap)

    def held(chip):
        return [chip * 2 + core, chip * 2 + 1 - core, 6 - chip * 2 + core, 7 - chip * 2 - core]

    place = jnp.stack(held(y) + held(y ^ 1)).astype(jnp.int32)

    picks = routes[0].reshape(-1)
    count = picks.shape[0]
    onehot = picks[:, None] == lax.broadcasted_iota(jnp.int32, (count, 128), 1)
    earlier = lax.broadcasted_iota(jnp.int32, (count, count), 0) > lax.broadcasted_iota(
        jnp.int32, (count, count), 1
    )
    before = jnp.dot(earlier.astype(BF16), onehot.astype(BF16), preferred_element_type=F32)
    rank = jnp.sum(jnp.where(onehot, before, 0.0), axis=1).astype(jnp.int32)
    token = lax.iota(jnp.int32, count) // routes.shape[2]
    slots = jnp.concatenate(
        [
            jnp.sum(jnp.where(onehot & (rank == s)[:, None], token[:, None], 0), axis=0)
            for s in range(3)
        ]
    ).astype(jnp.int32)

    packed = jnp.concatenate(
        [jnp.transpose(a[0], (1, 0, 2)) for a in (queries, key_rows, values)], axis=1
    )
    by_head = lax.all_to_all(packed, "sp", split_axis=0, concat_axis=0, tiled=True)
    attended = attend(by_head, 2).reshape(32, 128, 128)
    paired = lax.all_to_all(attended, ("sp", "yl"), split_axis=0, concat_axis=0, tiled=True)
    own, other = project(
        yl.reshape(1).astype(jnp.int32), paired.reshape(16, 2, 128, 128),
        (out_weight, w_core, w_near, w_near_core),
    )
    got = lax.ppermute(other, "yl", [(0, 1), (1, 0)])
    stream, outgoing = mix(
        place, slots, own, got, residual[0], mixer_gain.reshape(1, -1), expert_gain.reshape(1, -1)
    )
    arrived = lax.all_to_all(outgoing, ALL, split_axis=0, concat_axis=0, tiled=True)
    result = run_experts(arrived, gate_weight[0], up_weight[0], expert_down_matrix[0])
    returned = lax.all_to_all(result, ALL, split_axis=0, concat_axis=0, tiled=True)
    output = combine(
        picks, rank, route_weight[0].reshape(-1), returned, stream, output_gain.reshape(32, 128)
    )
    return output[None]


def solution(mesh):
    mesh = Mesh(mesh.devices.reshape(16, 2, 2, 2), ALL)
    in_specs = (
        P(DP, "sp", None, None),
        P(DP, "sp", None, None),
        P(DP, "sp", None, None),
        P(DP, "sp", None),
        P(None, DP),
        P(),
        P(),
        P(ALL, None, None),
        P(ALL, None, None),
        P(ALL, None, None),
        P(DP, "sp", None),
        P(DP, "sp", None),
        P(),
    )
    return jax.shard_map(
        local, mesh=mesh, in_specs=in_specs, out_specs=P(DP, "sp", None), check_vma=False
    )
```

time: 386 us -> 238 us (0.62)
  local copies, waits for them, and re-layouts: 86.5 us -> 7.09 us
  other arithmetic: 76.4 us -> 1.53 us
  Pallas kernels: 0 us -> 49.8 us
  matrix products: 44.9 us -> 0.23 us
  waiting for transfers between devices: 80.8 us -> 102 us
  between operations: 14.4 us -> 0.2 us
  blocking collectives: 60.9 us -> 49.7 us
  starting transfers between devices: 18.4 us -> 26.8 us
    pallas_call x0 -> x5, Pallas kernels: none -> 49.8 us  [the longest x1 22.7 us: run_experts(): pl.pallas_call(expert_kernel, out_shape=jax.ShapeDtypeStruct(x.shape, BF1...]
    dot_general x11 -> x1, matrix products: 44.9 us -> 0.23 us  [local(): jnp.dot(earlier.astype(BF16), onehot.astype(BF16), preferred_element_type...]
    ppermute x0 -> x4, waiting for transfers between devices: none -> 44.2 us  [the longest x1 32.5 us: local(): w_near = lax.ppermute(out_weight, DP, across)]
    another operation x25 -> x3, local copies, waits for them, and re-layouts: 40.4 us -> 0.37 us  [the longest x1 0.14 us: local(): picks = routes[0].reshape(-1)]
    another operation x11 -> x0, other arithmetic: 38.4 us -> none
    all_to_all x3, waiting for transfers between devices: 80.1 us -> 58.1 us  [the longest x1 41.5 us: local(): lax.all_to_all(result, ALL, split_axis=0, concat_axis=0, tiled=True)]
    unnamed x3 -> x0, other arithmetic: 16.4 us -> none
    all_to_all x1, blocking collectives: 60.9 us -> 49.7 us  [local(): lax.all_to_all(outgoing, ALL, split_axis=0, concat_axis=0, tiled=True)]
  transfers between devices with their start and end apart: 4 -> 7, of which waited for: 3 -> 4; matrix products, arithmetic and copies ran while one was open for 38% -> 2% of each run, Pallas kernels for 0% -> 5%
where the time goes in v1:
time: 238 us
  waiting for transfers between devices  102 us (43%)
  Pallas kernels  49.8 us (21%)
  blocking collectives  49.7 us (21%)
  starting transfers between devices  26.8 us (11%)
  local copies, waits for them, and re-layouts  7.09 us (3%)
    all_to_all x1, blocking collectives, local(): lax.all_to_all(outgoing, ALL, split_axis=0, concat_axis=0, tiled=True)  49.7 us
    all_to_all x1, waiting for transfers between devices, local(): lax.all_to_all(result, ALL, split_axis=0, concat_axis=0, tiled=True)  41.5 us
    ppermute x1, waiting for transfers between devices, local(): w_near = lax.ppermute(out_weight, DP, across)  32.5 us
    pallas_call x1, Pallas kernels, run_experts(): pl.pallas_call(expert_kernel, out_shape=jax.ShapeDtypeStruct(x.shape, BF1...  22.7 us
    all_to_all x1, waiting for transfers between devices, local(): lax.all_to_all(attended, ('sp', 'yl'), split_axis=0, concat_axis=0, tiled...  16.6 us
    ppermute x1, waiting for transfers between devices, local(): got = lax.ppermute(other, 'yl', [(0, 1), (1, 0)])  11.7 us
    pallas_call x1, Pallas kernels, attend(): pl.pallas_call(attend_kernel, out_shape=jax.ShapeDtypeStruct((blocks, cop...  11.3 us
    all_to_all x1, starting transfers between devices, local(): lax.all_to_all(attended, ('sp', 'yl'), split_axis=0, concat_axis=0, tiled...  8.07 us
  transfers between devices with their start and end apart: 7, of which 4 were waited for; matrix products, arithmetic and copies ran while one was open for 2% of the time, Pallas kernels for 5%

profile of v1, /device:TPU:1, one launch (start us, length us, event | category | flops | bytes accessed | tf_op | source)
XLA Modules:
  0.0 237.7 jit_solution(11909133340105848930)
XLA Ops:
  0.0 3.6 %collective-permute-start.1 = (bf16[2048,512]{1,0:T(8,128)(2,1)}, bf16[2048,512]{1,0:T(8,128)(2,1)}, u32[]{:S(2)}, u32[]{:S(2)}) collective-permute-start(bf16[2048,512]{1,0:T(8,128)(2,1)} %w0.1), channel_id=1, source_target_pairs={{0,6},{1,7},{2,4},{3,5},{4,2},{5,3},{6,0},{7,1},{8,14},{9,15},{10,... | collective-permute-start | bytes 6291464 | tf_op jit(solution)/shard_map/ppermute | solution.py:296
  3.6 1.2 copy.25
  4.7 1.5 copy_bitcast_fusion
  6.2 0.0 copy-start.1
  6.2 1.4 pad_maximum_fusion
  7.6 7.6 %all-to-all-start = ((bf16[16,384,128]{2,1,0:T(8,128)(2,1)}), bf16[16,384,128]{2,1,0:T(8,128)(2,1)}, u32[]{:S(2)}, u32[]{:S(2)}) async-start(bf16[16,384,128]{2,1,0:T(8,128)(2,1)} %pad_maximum_fusion), calls=%async_computation | async-start | bytes 3145728 | tf_op jit(solution)/shard_map/all_to_all | solution.py:324
  15.2 0.0 copy-done.1
  15.2 0.0 copy-start.9
  15.2 1.3 collective-permute-start
  16.6 32.5 %collective-permute-done.1.w2 = bf16[2048,512]{1,0:T(8,128)(2,1)} collective-permute-done((bf16[2048,512]{1,0:T(8,128)(2,1)}, bf16[2048,512]{1,0:T(8,128)(2,1)}, u32[]{:S(2)}, u32[]{:S(2)}) %collective-permute-start.1) | collective-permute-done | bytes 2097184 | tf_op jit(solution)/shard_map/ppermute | solution.py:296
  49.1 1.4 collective-permute-start.2
  50.5 0.0 all-to-all-done.x_ref
  50.5 11.3 %attend.1 = bf16[16,2,128,128]{3,2,1,0:T(8,128)(2,1)S(1)} custom-call(bf16[16,384,128]{2,1,0:T(8,128)(2,1)} %all-to-all-done.x_ref), custom_call_target="tpu_custom_call" | custom-call | flops 12000000000 | bytes 3000000 | tf_op jit(solution)/shard_map/attend/pallas_call | solution.py:74
  61.8 0.0 copy-start.2
  61.8 1.0 copy-done.2
  62.8 8.1 %all-to-all-start.1 = ((bf16[32,128,128]{2,1,0:T(8,128)(2,1)}), bf16[32,128,128]{2,1,0:T(8,128)(2,1)S(1)}, u32[]{:S(2)}, u32[]{:S(2)}) async-start(bf16[32,128,128]{2,1,0:T(8,128)(2,1)} %bitcast.33), calls=%async_computation.1 | async-start | bytes 2097152 | tf_op jit(solution)/shard_map/all_to_all | solution.py:326
  70.9 0.0 copy-done.9
  70.9 0.1 copy.17
  71.0 0.1 reshape_squeeze.6.expert_ref
  71.1 0.1 stack.35.place_ref
  71.2 0.2 fusion
  71.5 0.0 collective-permute-done.w1
  71.5 16.6 %all-to-all-done.1 = bf16[32,128,128]{2,1,0:T(8,128)(2,1)S(1)} async-done(((bf16[32,128,128]{2,1,0:T(8,128)(2,1)}), bf16[32,128,128]{2,1,0:T(8,128)(2,1)S(1)}, u32[]{:S(2)}, u32[]{:S(2)}) %all-to-all-start.1) | async-done | bytes 1048608 | tf_op jit(solution)/shard_map/all_to_all | solution.py:326
  88.0 0.0 collective-permute-done.2.w3
  88.0 0.0 copy-start.6
  88.0 0.0 copy-start.7
  88.0 5.3 %project.1 = (f32[4,128,512]{2,1,0:T(8,128)S(1)}, bf16[4,128,512]{2,1,0:T(8,128)(2,1)S(1)}) custom-call(s32[1]{0:T(128)} %bitcast.8.index_ref, bf16[16,2,128,128]{3,2,1,0:T(8,128)(2,1)S(1)} %bitcast.32, bf16[2048,512]{1,0:T(8,128)(2,1)S(1)} %copy-done.1, bf16[2048,512]{1,0:T(8,128)(2,1)} %collective-permute-done.w1, ...), custom_call_target="tpu_custom_call" | custom-call | flops 2000000000 | bytes 11000000 | tf_op jit(solution)/shard_map/project/pallas_call | solution.py:103
  93.3 0.3 collective-permute-start.3
  93.6 0.2 select_reduce_fusion.2
  93.8 11.7 %collective-permute-done.3.got_ref = bf16[4,128,512]{2,1,0:T(8,128)(2,1)S(1)} collective-permute-done((bf16[4,128,512]{2,1,0:T(8,128)(2,1)S(1)}, bf16[4,128,512]{2,1,0:T(8,128)(2,1)S(1)}, u32[]{:S(2)}, u32[]{:S(2)}) %collective-permute-start.3) | collective-permute-done | bytes 524320 | tf_op jit(solution)/shard_map/ppermute | solution.py:331
  105.5 0.0 copy-done.6
  105.5 0.0 copy-done.7
  105.5 0.0 copy-done.8
  105.5 5.1 %mix.1 = (bf16[128,32,128]{2,1,0:T(8,128)(2,1)S(1)}, bf16[128,96,128]{2,1,0:T(8,128)(2,1)S(1)}) custom-call(s32[8]{0:T(128)S(1)} %stack.35.place_ref, s32[384]{0:T(512)S(1)} %pad_add_fusion.slot_ref, f32[4,128,512]{2,1,0:T(8,128)S(1)} %get-tuple-element.9.own_ref, bf16[4,128,512]{2,1,0:T(8,128)(2,1)S(1)} %collective-permute-done.3.got_ref, ...), custom_call_target="tpu_custom_call" | custom-call | flops 1000000000 | bytes 8000000 | tf_op jit(solution)/shard_map/mix/pallas_call | solution.py:165
  110.6 0.0 copy-start.3
  110.6 49.7 %all_to_all.20.x_ref = bf16[128,96,128]{2,1,0:T(8,128)(2,1)} all-to-all(bf16[128,96,128]{2,1,0:T(8,128)(2,1)S(1)} %get-tuple-element.11), channel_id=1, replica_groups=mesh['sp'=16,'yh'=2,'yl'=2,'c'=2] {'sp','yh','yl','c'}, dimensions={0} | all-to-all | bytes 6291456 | tf_op jit(solution)/shard_map/all_to_all | solution.py:335
  160.2 0.0 copy-done.3
  160.2 22.7 %experts.1 = bf16[128,96,128]{2,1,0:T(8,128)(2,1)S(1)} custom-call(bf16[128,96,128]{2,1,0:T(8,128)(2,1)} %all_to_all.20.x_ref, bf16[4096,512]{1,0:T(8,128)(2,1)} %bitcast.39, bf16[4096,512]{1,0:T(8,128)(2,1)} %bitcast.40, bf16[512,4096]{1,0:T(8,128)(2,1)} %bitcast.41), custom_call_target="tpu_custom_call" | custom-call | flops 6000000000 | bytes 19000000 | tf_op jit(solution)/shard_map/experts/pallas_call | solution.py:229
  182.9 0.0 copy-start
  182.9 1.6 copy-done
  184.6 4.6 %all-to-all-start.3 = ((bf16[128,96,128]{2,1,0:T(8,128)(2,1)}), bf16[128,96,128]{2,1,0:T(8,128)(2,1)S(1)}, u32[]{:S(2)}, u32[]{:S(2)}) async-start(bf16[128,96,128]{2,1,0:T(8,128)(2,1)} %copy-done), calls=%async_computation.3 | async-start | bytes 6291456 | tf_op jit(solution)/shard_map/all_to_all | solution.py:337
  189.2 0.0 copy-done.10
  189.2 0.1 copy.18
  189.3 0.1 reshape_squeeze.7.weight_ref
  189.5 41.5 %all-to-all-done.3.x_ref = bf16[128,96,128]{2,1,0:T(8,128)(2,1)S(1)} async-done(((bf16[128,96,128]{2,1,0:T(8,128)(2,1)}), bf16[128,96,128]{2,1,0:T(8,128)(2,1)S(1)}, u32[]{:S(2)}, u32[]{:S(2)}) %all-to-all-start.3) | async-done | bytes 3145760 | tf_op jit(solution)/shard_map/all_to_all | solution.py:337
  231.0 0.0 copy-done.5
  231.0 1.2 copy-done.4
  232.2 5.5 %combine.1 = bf16[128,4096]{1,0:T(8,128)(2,1)} custom-call(s32[256]{0:T(256)S(1)} %reshape_squeeze.6.expert_ref, s32[256]{0:T(256)S(1)} %convert_element_type.2.rank_ref, f32[256]{0:T(256)S(1)} %reshape_squeeze.7.weight_ref, bf16[128,96,128]{2,1,0:T(8,128)(2,1)S(1)} %all-to-all-done.3.x_ref, bf16[128,32,128]{2,1,0:T(8,128)(2,1)S(1)} %copy-done.4, ...), custom_call_target="tpu_custom_call" | custom-call | flops 1000000000 | bytes 6000000 | tf_op jit(solution)/shard_map/combine/pallas_call | solution.py:275
  (8 shorter events, 0.0 us)
Async XLA Ops:
  0.0 49.1 %collective-permute-start.1 = (bf16[2048,512]{1,0:T(8,128)(2,1)}, bf16[2048,512]{1,0:T(8,128)(2,1)}, u32[]{:S(2)}, u32[]{:S(2)}) collective-permute-start(bf16[2048,512]{1,0:T(8,128)(2,1)} %w0.1), channel_id=1, source_target_pairs={{0,6},{1,7},{2,4},{3,5},{4,2},{5,3},{6,0},{7,1},{8,14},{9,15},{10,... | collective-permute-start | bytes 6291464 | tf_op jit(solution)/shard_map/ppermute | solution.py:296
  6.2 9.0 %copy-start.1 = (bf16[2048,512]{1,0:T(8,128)(2,1)S(1)}, bf16[2048,512]{1,0:T(8,128)(2,1)}, u32[]{:S(2)}) copy-start(bf16[2048,512]{1,0:T(8,128)(2,1)} %w0.1) | copy-start | bytes 6291460
  7.6 42.9 %all-to-all-start = ((bf16[16,384,128]{2,1,0:T(8,128)(2,1)}), bf16[16,384,128]{2,1,0:T(8,128)(2,1)}, u32[]{:S(2)}, u32[]{:S(2)}) async-start(bf16[16,384,128]{2,1,0:T(8,128)(2,1)} %pad_maximum_fusion), calls=%async_computation | async-start | bytes 3145728 | tf_op jit(solution)/shard_map/all_to_all | solution.py:324
  15.2 55.6 %copy-start.9 = (s32[1,128,2]{1,2,0:T(2,128)S(1)}, s32[1,128,2]{1,2,0:T(2,128)}, u32[]{:S(2)}) copy-start(s32[1,128,2]{1,2,0:T(2,128)} %param.23) | copy-start | bytes 3076
  15.2 56.2 %collective-permute-start = (bf16[2048,512]{1,0:T(8,128)(2,1)S(1)}, bf16[2048,512]{1,0:T(8,128)(2,1)}, u32[]{:S(2)}, u32[]{:S(2)}) collective-permute-start(bf16[2048,512]{1,0:T(8,128)(2,1)S(1)} %copy-done.1), channel_id=1, source_target_pairs={{0,1},{1,0},{2,3},{3,2},{4,5},{5,4},{6,7},{7,6},{8,9},{9,8},{10,11... | collective-permute-start | bytes 6291464 | tf_op jit(solution)/shard_map/ppermute | solution.py:297
  49.1 38.9 %collective-permute-start.2 = (bf16[2048,512]{1,0:T(8,128)(2,1)}, bf16[2048,512]{1,0:T(8,128)(2,1)}, u32[]{:S(2)}, u32[]{:S(2)}) collective-permute-start(bf16[2048,512]{1,0:T(8,128)(2,1)} %collective-permute-done.1.w2), channel_id=1, source_target_pairs={{0,1},{1,0},{2,3},{3,2},{4,5},{5,4},{6,7},{7,6},{8,9},{9,8},{10,11... | collective-permute-start | bytes 6291464 | tf_op jit(solution)/shard_map/ppermute | solution.py:298
  61.8 1.0 copy-start.2
  62.8 25.3 %all-to-all-start.1 = ((bf16[32,128,128]{2,1,0:T(8,128)(2,1)}), bf16[32,128,128]{2,1,0:T(8,128)(2,1)S(1)}, u32[]{:S(2)}, u32[]{:S(2)}) async-start(bf16[32,128,128]{2,1,0:T(8,128)(2,1)} %bitcast.33), calls=%async_computation.1 | async-start | bytes 2097152 | tf_op jit(solution)/shard_map/all_to_all | solution.py:326
  88.0 17.4 %copy-start.6 = (bf16[1,128,4096]{2,1,0:T(8,128)(2,1)S(1)}, bf16[1,128,4096]{2,1,0:T(8,128)(2,1)}, u32[]{:S(2)}) copy-start(bf16[1,128,4096]{2,1,0:T(8,128)(2,1)} %param.16) | copy-start | bytes 3145732
  88.0 17.4 %copy-start.7 = (f32[4096]{0:T(1024)S(1)}, f32[4096]{0:T(1024)}, u32[]{:S(2)}) copy-start(f32[4096]{0:T(1024)} %param.18) | copy-start | bytes 49156
  88.0 17.4 %copy-start.8 = (f32[4096]{0:T(1024)S(1)}, f32[4096]{0:T(1024)}, u32[]{:S(2)}) copy-start(f32[4096]{0:T(1024)} %param.19) | copy-start | bytes 49156
  93.3 12.1 %collective-permute-start.3 = (bf16[4,128,512]{2,1,0:T(8,128)(2,1)S(1)}, bf16[4,128,512]{2,1,0:T(8,128)(2,1)S(1)}, u32[]{:S(2)}, u32[]{:S(2)}) collective-permute-start(bf16[4,128,512]{2,1,0:T(8,128)(2,1)S(1)} %get-tuple-element.10), channel_id=1, source_target_pairs={{0,2},{2,0},{1,3},{3,1},{4,6},{6,4},{5,7},{7,5},{8,10},{10,8},{9,1... | collective-permute-start | bytes 1572872 | tf_op jit(solution)/shard_map/ppermute | solution.py:331
  110.6 49.7 %copy-start.3 = (bf16[128,32,128]{2,1,0:T(8,128)(2,1)}, bf16[128,32,128]{2,1,0:T(8,128)(2,1)S(1)}, u32[]{:S(2)}) copy-start(bf16[128,32,128]{2,1,0:T(8,128)(2,1)S(1)} %get-tuple-element.12.stream_ref) | copy-start | bytes 3145732
  182.9 1.6 copy-start
  184.6 4.6 %copy-start.10 = (f32[1,128,2]{1,2,0:T(2,128)S(1)}, f32[1,128,2]{1,2,0:T(2,128)}, u32[]{:S(2)}) copy-start(f32[1,128,2]{1,2,0:T(2,128)} %param.24) | copy-start | bytes 3076
  184.6 46.4 %copy-start.5 = (f32[4096]{0:T(1024)S(1)}, f32[4096]{0:T(1024)}, u32[]{:S(2)}) copy-start(f32[4096]{0:T(1024)} %param.25) | copy-start | bytes 49156
  184.6 46.4 %all-to-all-start.3 = ((bf16[128,96,128]{2,1,0:T(8,128)(2,1)}), bf16[128,96,128]{2,1,0:T(8,128)(2,1)S(1)}, u32[]{:S(2)}, u32[]{:S(2)}) async-start(bf16[128,96,128]{2,1,0:T(8,128)(2,1)} %copy-done), calls=%async_computation.3 | async-start | bytes 6291456 | tf_op jit(solution)/shard_map/all_to_all | solution.py:337
  231.0 1.2 copy-start.4

commit v2 on v1

--- a/solution.py
+++ b/solution.py
@@ -1,4 +1,3 @@
-import functools
 import math
 
 import jax
@@ -8,12 +7,14 @@
 from jax.experimental.pallas import tpu as pltpu
 from jax.sharding import Mesh, PartitionSpec as P
 
+
 EPSILON = 1e-06
 F32 = jnp.float32
 BF16 = jnp.bfloat16
 DP = ("yh", "yl", "c")
 ALL = ("sp", "yh", "yl", "c")
 VMEM = pl.BlockSpec(memory_space=pltpu.VMEM)
+HBM = pl.BlockSpec(memory_space=pltpu.HBM)
 SMEM = pl.BlockSpec(memory_space=pltpu.SMEM)
 
 
@@ -177,15 +178,32 @@
     )(place, slots, own, got, residual, mixer_gain, expert_gain)
 
 
-def expert_kernel(x_ref, gate_ref, up_ref, down_ref, o_ref, rows_ref, hidden_ref, result_ref):
+def expert_kernel(
+    x_hbm, gate_hbm, up_hbm, down_hbm, o_hbm,
+    x_ref, gate_ref, up_ref, down_ref, o_ref, rows_ref, hidden_ref, result_ref, in_sem, out_sem,
+):
     sources = x_ref.shape[0]
     slots = x_ref.shape[1] // 32
     gather = to_rows(8, 32)
     spread = to_rows(32, 8)
+    weights = ((gate_hbm, gate_ref), (up_hbm, up_ref), (down_hbm, down_ref))
+
+    def slot_copy(source, target, sem, slot):
+        at = pl.ds(slot * 32, 32)
+        return pltpu.make_async_copy(source.at[:, at, :], target.at[:, at, :], sem.at[slot])
+
+    x_copies = [slot_copy(x_hbm, x_ref, in_sem, slot) for slot in range(slots)]
+    w_copies = [
+        pltpu.make_async_copy(source, target, in_sem.at[slots + k])
+        for k, (source, target) in enumerate(weights)
+    ]
+    for copy in x_copies + w_copies:
+        copy.start()
 
     for slot in range(slots):
-
-        @pl.loop(0, sources // 16)
+        x_copies[slot].wait()
+
+        @pl.loop(0, sources // 16, unroll=8)
         def _(g):
             at = slice(slot * 32, slot * 32 + 32)
             left = x_ref[pl.ds(g * 16, 8), at, :].reshape(256, 128)
@@ -199,19 +217,23 @@
                     [got[c * 8 : c * 8 + 8, :128], got[c * 8 : c * 8 + 8, 128:]], axis=0
                 ).astype(BF16)
 
+    w_copies[0].wait()
+    w_copies[1].wait()
     for n in range(0, 512, 256):
         a = jnp.dot(rows_ref[...], gate_ref[:, n : n + 256], preferred_element_type=F32)
         b = jnp.dot(rows_ref[...], up_ref[:, n : n + 256], preferred_element_type=F32)
         hidden_ref[:, n : n + 256] = (a / (1.0 + jnp.exp(-a)) * b).astype(BF16)
 
-    @pl.loop(0, 16)
-    def _(n):
-        at = pl.ds(pl.multiple_of(n * 256, 256), 256)
-        result_ref[:, at] = jnp.dot(hidden_ref[...], down_ref[:, at], preferred_element_type=F32)
-
+    w_copies[2].wait()
+    for n in range(0, 4096, 1024):
+        result_ref[:, n : n + 1024] = jnp.dot(
+            hidden_ref[...], down_ref[:, n : n + 1024], preferred_element_type=F32
+        )
+
+    o_copies = [slot_copy(o_ref, o_hbm, out_sem, slot) for slot in range(slots)]
     for slot in range(slots):
 
-        @pl.loop(0, sources // 16)
+        @pl.loop(0, sources // 16, unroll=8)
         def _(g):
             base = slot * sources + g * 16
             lower = result_ref[pl.ds(pl.multiple_of(base, 8), 8), :]
@@ -223,18 +245,30 @@
             o_ref[pl.ds(g * 16, 8), at, :] = out[:, :128].reshape(8, 32, 128)
             o_ref[pl.ds(g * 16 + 8, 8), at, :] = out[:, 128:].reshape(8, 32, 128)
 
+        o_copies[slot].start()
+    for copy in o_copies:
+        copy.wait()
+
 
 def run_experts(x, gate, up, down):
-    rows = x.shape[0] * (x.shape[1] // 32)
+    slots = x.shape[1] // 32
+    rows = x.shape[0] * slots
     return pl.pallas_call(
         expert_kernel,
-        out_shape=jax.ShapeDtypeStruct(x.shape, BF16),
-        in_specs=[VMEM] * 4,
-        out_specs=VMEM,
+        out_shape=pltpu.HBM(x.shape, BF16),
+        in_specs=[HBM] * 4,
+        out_specs=HBM,
         scratch_shapes=[
+            pltpu.VMEM(x.shape, BF16),
+            pltpu.VMEM(gate.shape, BF16),
+            pltpu.VMEM(up.shape, BF16),
+            pltpu.VMEM(down.shape, BF16),
+            pltpu.VMEM(x.shape, BF16),
             pltpu.VMEM((rows, 4096), BF16),
             pltpu.VMEM((rows, 512), BF16),
             pltpu.VMEM((rows, 4096), F32),
+            pltpu.SemaphoreType.DMA((slots + 3,)),
+            pltpu.SemaphoreType.DMA((slots,)),
         ],
         compiler_params=pltpu.CompilerParams(vmem_limit_bytes=48 << 20),
         cost_estimate=pl.CostEstimate(flops=6 * 10**9, bytes_accessed=19 * 10**6, transcendentals=0),
@@ -284,7 +318,7 @@
     )(expert, rank, weight, x, stream, gain)
 
 
-def local(
+def layer(
     queries, key_rows, values, residual, out_weight, mixer_gain, expert_gain,
     gate_weight, up_weight, expert_down_matrix, routes, route_weight, output_gain,
 ):
@@ -359,5 +393,5 @@
         P(),
     )
     return jax.shard_map(
-        local, mesh=mesh, in_specs=in_specs, out_specs=P(DP, "sp", None), check_vma=False
-    )
+        layer, mesh=mesh, in_specs=in_specs, out_specs=P(DP, "sp", None), check_vma=False
+    )

time: 238 us -> 225 us (0.945)
  Pallas kernels: 49.8 us -> 38.2 us
    pallas_call x1, Pallas kernels: 22.7 us -> 11.1 us  [run_experts(): pl.pallas_call(expert_kernel, out_shape=pltpu.HBM(x.shape, BF16), in_spec...]
    unnamed x25 -> x23, local copies, waits for them, and re-layouts: 5.25 us -> 3.64 us
where the time goes in v2:
time: 225 us; the launch traced here: 224 us
  waiting for transfers between devices  102 us (45%)
  blocking collectives  49.6 us (22%)
  Pallas kernels  38.2 us (17%)
  starting transfers between devices  26.7 us (12%)
  local copies, waits for them, and re-layouts  5.48 us (2%)
    all_to_all x1, blocking collectives, layer(): lax.all_to_all(outgoing, ALL, split_axis=0, concat_axis=0, tiled=True)  49.6 us
    all_to_all x1, waiting for transfers between devices, layer(): lax.all_to_all(result, ALL, split_axis=0, concat_axis=0, tiled=True)  41.5 us
    ppermute x1, waiting for transfers between devices, layer(): w_near = lax.ppermute(out_weight, DP, across)  32.5 us
    all_to_all x1, waiting for transfers between devices, layer(): lax.all_to_all(attended, ('sp', 'yl'), split_axis=0, concat_axis=0, tiled...  16.6 us
    ppermute x1, waiting for transfers between devices, layer(): got = lax.ppermute(other, 'yl', [(0, 1), (1, 0)])  11.7 us
    pallas_call x1, Pallas kernels, attend(): pl.pallas_call(attend_kernel, out_shape=jax.ShapeDtypeStruct((blocks, cop...  11.3 us
    pallas_call x1, Pallas kernels, run_experts(): pl.pallas_call(expert_kernel, out_shape=pltpu.HBM(x.shape, BF16), in_spec...  11.1 us
    all_to_all x1, starting transfers between devices, layer(): lax.all_to_all(attended, ('sp', 'yl'), split_axis=0, concat_axis=0, tiled...  8.07 us
  transfers between devices with their start and end apart: 7, of which 4 were waited for; matrix products, arithmetic and copies ran while one was open for 2% of the time, Pallas kernels for 5%

profile of v2, /device:TPU:1, one launch (start us, length us, event | category | flops | bytes accessed | tf_op | source)
XLA Modules:
  0.0 224.2 jit_solution(7022100716564881517)
XLA Ops:
  0.0 3.6 %collective-permute-start.1 = (bf16[2048,512]{1,0:T(8,128)(2,1)}, bf16[2048,512]{1,0:T(8,128)(2,1)}, u32[]{:S(2)}, u32[]{:S(2)}) collective-permute-start(bf16[2048,512]{1,0:T(8,128)(2,1)} %w0.1), channel_id=1, source_target_pairs={{0,6},{1,7},{2,4},{3,5},{4,2},{5,3},{6,0},{7,1},{8,14},{9,15},{10,... | collective-permute-start | bytes 6291464 | tf_op jit(solution)/shard_map/ppermute | solution.py:330
  3.6 1.2 copy.25
  4.7 1.5 copy_bitcast_fusion
  6.2 0.0 copy-start
  6.2 1.4 pad_maximum_fusion
  7.6 7.6 %all-to-all-start = ((bf16[16,384,128]{2,1,0:T(8,128)(2,1)}), bf16[16,384,128]{2,1,0:T(8,128)(2,1)}, u32[]{:S(2)}, u32[]{:S(2)}) async-start(bf16[16,384,128]{2,1,0:T(8,128)(2,1)} %pad_maximum_fusion), calls=%async_computation | async-start | bytes 3145728 | tf_op jit(solution)/shard_map/all_to_all | solution.py:358
  15.2 0.0 copy-done
  15.2 0.0 copy-start.8
  15.3 1.3 collective-permute-start
  16.6 32.5 %collective-permute-done.1.w2 = bf16[2048,512]{1,0:T(8,128)(2,1)} collective-permute-done((bf16[2048,512]{1,0:T(8,128)(2,1)}, bf16[2048,512]{1,0:T(8,128)(2,1)}, u32[]{:S(2)}, u32[]{:S(2)}) %collective-permute-start.1) | collective-permute-done | bytes 2097184 | tf_op jit(solution)/shard_map/ppermute | solution.py:330
  49.1 1.4 collective-permute-start.2
  50.5 0.0 all-to-all-done.x_ref
  50.5 11.3 %attend.1 = bf16[16,2,128,128]{3,2,1,0:T(8,128)(2,1)S(1)} custom-call(bf16[16,384,128]{2,1,0:T(8,128)(2,1)} %all-to-all-done.x_ref), custom_call_target="tpu_custom_call" | custom-call | flops 12000000000 | bytes 3000000 | tf_op jit(solution)/shard_map/attend/pallas_call | solution.py:75
  61.8 0.0 copy-start.1
  61.8 1.0 copy-done.1
  62.8 8.1 %all-to-all-start.1 = ((bf16[32,128,128]{2,1,0:T(8,128)(2,1)}), bf16[32,128,128]{2,1,0:T(8,128)(2,1)S(1)}, u32[]{:S(2)}, u32[]{:S(2)}) async-start(bf16[32,128,128]{2,1,0:T(8,128)(2,1)} %bitcast.33), calls=%async_computation.1 | async-start | bytes 2097152 | tf_op jit(solution)/shard_map/all_to_all | solution.py:360
  70.9 0.0 copy-done.8
  70.9 0.1 copy.17
  71.0 0.1 reshape_squeeze.6.expert_ref
  71.1 0.1 stack.35.place_ref
  71.2 0.2 fusion
  71.5 0.0 collective-permute-done.w1
  71.5 16.6 %all-to-all-done.1 = bf16[32,128,128]{2,1,0:T(8,128)(2,1)S(1)} async-done(((bf16[32,128,128]{2,1,0:T(8,128)(2,1)}), bf16[32,128,128]{2,1,0:T(8,128)(2,1)S(1)}, u32[]{:S(2)}, u32[]{:S(2)}) %all-to-all-start.1) | async-done | bytes 1048608 | tf_op jit(solution)/shard_map/all_to_all | solution.py:360
  88.0 0.0 collective-permute-done.2.w3
  88.0 0.0 copy-start.5
  88.0 0.0 copy-start.6
  88.0 5.3 %project.1 = (f32[4,128,512]{2,1,0:T(8,128)S(1)}, bf16[4,128,512]{2,1,0:T(8,128)(2,1)S(1)}) custom-call(s32[1]{0:T(128)} %bitcast.8.index_ref, bf16[16,2,128,128]{3,2,1,0:T(8,128)(2,1)S(1)} %bitcast.32, bf16[2048,512]{1,0:T(8,128)(2,1)S(1)} %copy-done, bf16[2048,512]{1,0:T(8,128)(2,1)} %collective-permute-done.w1, ...), custom_call_target="tpu_custom_call" | custom-call | flops 2000000000 | bytes 11000000 | tf_op jit(solution)/shard_map/project/pallas_call | solution.py:104
  93.3 0.3 collective-permute-start.3
  93.6 0.2 select_reduce_fusion.2
  93.8 11.7 %collective-permute-done.3.got_ref = bf16[4,128,512]{2,1,0:T(8,128)(2,1)S(1)} collective-permute-done((bf16[4,128,512]{2,1,0:T(8,128)(2,1)S(1)}, bf16[4,128,512]{2,1,0:T(8,128)(2,1)S(1)}, u32[]{:S(2)}, u32[]{:S(2)}) %collective-permute-start.3) | collective-permute-done | bytes 524320 | tf_op jit(solution)/shard_map/ppermute | solution.py:365
  105.5 0.0 copy-done.5
  105.5 0.0 copy-done.6
  105.5 0.0 copy-done.7
  105.5 5.1 %mix.1 = (bf16[128,32,128]{2,1,0:T(8,128)(2,1)S(1)}, bf16[128,96,128]{2,1,0:T(8,128)(2,1)S(1)}) custom-call(s32[8]{0:T(128)S(1)} %stack.35.place_ref, s32[384]{0:T(512)S(1)} %pad_add_fusion.slot_ref, f32[4,128,512]{2,1,0:T(8,128)S(1)} %get-tuple-element.9.own_ref, bf16[4,128,512]{2,1,0:T(8,128)(2,1)S(1)} %collective-permute-done.3.got_ref, ...), custom_call_target="tpu_custom_call" | custom-call | flops 1000000000 | bytes 8000000 | tf_op jit(solution)/shard_map/mix/pallas_call | solution.py:166
  110.6 0.0 copy-start.2
  110.6 49.6 %all_to_all.20.x_hbm = bf16[128,96,128]{2,1,0:T(8,128)(2,1)S(1)} all-to-all(bf16[128,96,128]{2,1,0:T(8,128)(2,1)S(1)} %get-tuple-element.11), channel_id=1, replica_groups=mesh['sp'=16,'yh'=2,'yl'=2,'c'=2] {'sp','yh','yl','c'}, dimensions={0} | all-to-all | bytes 6291456 | tf_op jit(solution)/shard_map/all_to_all | solution.py:369
  160.1 0.0 copy-done.2
  160.1 11.1 %experts.1 = bf16[128,96,128]{2,1,0:T(8,128)(2,1)} custom-call(bf16[128,96,128]{2,1,0:T(8,128)(2,1)S(1)} %all_to_all.20.x_hbm, bf16[4096,512]{1,0:T(8,128)(2,1)} %bitcast.39, bf16[4096,512]{1,0:T(8,128)(2,1)} %bitcast.40, bf16[512,4096]{1,0:T(8,128)(2,1)} %bitcast.41), custom_call_target="tpu_custom_call" | custom-call | flops 6000000000 | bytes 19000000 | tf_op jit(solution)/shard_map/experts/pallas_call | solution.py:256
  171.2 0.0 copy-start.9
  171.2 0.0 copy-start.4
  171.2 4.5 %all-to-all-start.3 = ((bf16[128,96,128]{2,1,0:T(8,128)(2,1)}), bf16[128,96,128]{2,1,0:T(8,128)(2,1)S(1)}, u32[]{:S(2)}, u32[]{:S(2)}) async-start(bf16[128,96,128]{2,1,0:T(8,128)(2,1)} %experts.1), calls=%async_computation.3 | async-start | bytes 6291456 | tf_op jit(solution)/shard_map/all_to_all | solution.py:371
  175.8 0.0 copy-done.9
  175.8 0.1 copy.18
  175.9 0.1 reshape_squeeze.7.weight_ref
  176.0 41.5 %all-to-all-done.3.x_ref = bf16[128,96,128]{2,1,0:T(8,128)(2,1)S(1)} async-done(((bf16[128,96,128]{2,1,0:T(8,128)(2,1)}), bf16[128,96,128]{2,1,0:T(8,128)(2,1)S(1)}, u32[]{:S(2)}, u32[]{:S(2)}) %all-to-all-start.3) | async-done | bytes 3145760 | tf_op jit(solution)/shard_map/all_to_all | solution.py:371
  217.5 0.0 copy-done.4
  217.5 1.2 copy-done.3
  218.8 5.5 %combine.1 = bf16[128,4096]{1,0:T(8,128)(2,1)} custom-call(s32[256]{0:T(256)S(1)} %reshape_squeeze.6.expert_ref, s32[256]{0:T(256)S(1)} %convert_element_type.2.rank_ref, f32[256]{0:T(256)S(1)} %reshape_squeeze.7.weight_ref, bf16[128,96,128]{2,1,0:T(8,128)(2,1)S(1)} %all-to-all-done.3.x_ref, bf16[128,32,128]{2,1,0:T(8,128)(2,1)S(1)} %copy-done.3, ...), custom_call_target="tpu_custom_call" | custom-call | flops 1000000000 | bytes 6000000 | tf_op jit(solution)/shard_map/combine/pallas_call | solution.py:309
  (6 shorter events, 0.0 us)
Async XLA Ops:
  0.0 49.1 %collective-permute-start.1 = (bf16[2048,512]{1,0:T(8,128)(2,1)}, bf16[2048,512]{1,0:T(8,128)(2,1)}, u32[]{:S(2)}, u32[]{:S(2)}) collective-permute-start(bf16[2048,512]{1,0:T(8,128)(2,1)} %w0.1), channel_id=1, source_target_pairs={{0,6},{1,7},{2,4},{3,5},{4,2},{5,3},{6,0},{7,1},{8,14},{9,15},{10,... | collective-permute-start | bytes 6291464 | tf_op jit(solution)/shard_map/ppermute | solution.py:330
  6.2 9.0 %copy-start = (bf16[2048,512]{1,0:T(8,128)(2,1)S(1)}, bf16[2048,512]{1,0:T(8,128)(2,1)}, u32[]{:S(2)}) copy-start(bf16[2048,512]{1,0:T(8,128)(2,1)} %w0.1) | copy-start | bytes 6291460
  7.6 42.9 %all-to-all-start = ((bf16[16,384,128]{2,1,0:T(8,128)(2,1)}), bf16[16,384,128]{2,1,0:T(8,128)(2,1)}, u32[]{:S(2)}, u32[]{:S(2)}) async-start(bf16[16,384,128]{2,1,0:T(8,128)(2,1)} %pad_maximum_fusion), calls=%async_computation | async-start | bytes 3145728 | tf_op jit(solution)/shard_map/all_to_all | solution.py:358
  15.2 55.6 %copy-start.8 = (s32[1,128,2]{1,2,0:T(2,128)S(1)}, s32[1,128,2]{1,2,0:T(2,128)}, u32[]{:S(2)}) copy-start(s32[1,128,2]{1,2,0:T(2,128)} %param.23) | copy-start | bytes 3076
  15.3 56.2 %collective-permute-start = (bf16[2048,512]{1,0:T(8,128)(2,1)S(1)}, bf16[2048,512]{1,0:T(8,128)(2,1)}, u32[]{:S(2)}, u32[]{:S(2)}) collective-permute-start(bf16[2048,512]{1,0:T(8,128)(2,1)S(1)} %copy-done), channel_id=1, source_target_pairs={{0,1},{1,0},{2,3},{3,2},{4,5},{5,4},{6,7},{7,6},{8,9},{9,8},{10,11... | collective-permute-start | bytes 6291464 | tf_op jit(solution)/shard_map/ppermute | solution.py:331
  49.1 38.9 %collective-permute-start.2 = (bf16[2048,512]{1,0:T(8,128)(2,1)}, bf16[2048,512]{1,0:T(8,128)(2,1)}, u32[]{:S(2)}, u32[]{:S(2)}) collective-permute-start(bf16[2048,512]{1,0:T(8,128)(2,1)} %collective-permute-done.1.w2), channel_id=1, source_target_pairs={{0,1},{1,0},{2,3},{3,2},{4,5},{5,4},{6,7},{7,6},{8,9},{9,8},{10,11... | collective-permute-start | bytes 6291464 | tf_op jit(solution)/shard_map/ppermute | solution.py:332
  61.8 1.0 copy-start.1
  62.8 25.3 %all-to-all-start.1 = ((bf16[32,128,128]{2,1,0:T(8,128)(2,1)}), bf16[32,128,128]{2,1,0:T(8,128)(2,1)S(1)}, u32[]{:S(2)}, u32[]{:S(2)}) async-start(bf16[32,128,128]{2,1,0:T(8,128)(2,1)} %bitcast.33), calls=%async_computation.1 | async-start | bytes 2097152 | tf_op jit(solution)/shard_map/all_to_all | solution.py:360
  88.0 17.4 %copy-start.5 = (bf16[1,128,4096]{2,1,0:T(8,128)(2,1)S(1)}, bf16[1,128,4096]{2,1,0:T(8,128)(2,1)}, u32[]{:S(2)}) copy-start(bf16[1,128,4096]{2,1,0:T(8,128)(2,1)} %param.16) | copy-start | bytes 3145732
  88.0 17.4 %copy-start.6 = (f32[4096]{0:T(1024)S(1)}, f32[4096]{0:T(1024)}, u32[]{:S(2)}) copy-start(f32[4096]{0:T(1024)} %param.18) | copy-start | bytes 49156
  88.0 17.4 %copy-start.7 = (f32[4096]{0:T(1024)S(1)}, f32[4096]{0:T(1024)}, u32[]{:S(2)}) copy-start(f32[4096]{0:T(1024)} %param.19) | copy-start | bytes 49156
  93.3 12.1 %collective-permute-start.3 = (bf16[4,128,512]{2,1,0:T(8,128)(2,1)S(1)}, bf16[4,128,512]{2,1,0:T(8,128)(2,1)S(1)}, u32[]{:S(2)}, u32[]{:S(2)}) collective-permute-start(bf16[4,128,512]{2,1,0:T(8,128)(2,1)S(1)} %get-tuple-element.10), channel_id=1, source_target_pairs={{0,2},{2,0},{1,3},{3,1},{4,6},{6,4},{5,7},{7,5},{8,10},{10,8},{9,1... | collective-permute-start | bytes 1572872 | tf_op jit(solution)/shard_map/ppermute | solution.py:365
  110.6 49.6 %copy-start.2 = (bf16[128,32,128]{2,1,0:T(8,128)(2,1)}, bf16[128,32,128]{2,1,0:T(8,128)(2,1)S(1)}, u32[]{:S(2)}) copy-start(bf16[128,32,128]{2,1,0:T(8,128)(2,1)S(1)} %get-tuple-element.12.stream_ref) | copy-start | bytes 3145732
  171.2 4.5 %copy-start.9 = (f32[1,128,2]{1,2,0:T(2,128)S(1)}, f32[1,128,2]{1,2,0:T(2,128)}, u32[]{:S(2)}) copy-start(f32[1,128,2]{1,2,0:T(2,128)} %param.24) | copy-start | bytes 3076
  171.2 46.3 %copy-start.4 = (f32[4096]{0:T(1024)S(1)}, f32[4096]{0:T(1024)}, u32[]{:S(2)}) copy-start(f32[4096]{0:T(1024)} %param.25) | copy-start | bytes 49156
  171.2 46.3 %all-to-all-start.3 = ((bf16[128,96,128]{2,1,0:T(8,128)(2,1)}), bf16[128,96,128]{2,1,0:T(8,128)(2,1)S(1)}, u32[]{:S(2)}, u32[]{:S(2)}) async-start(bf16[128,96,128]{2,1,0:T(8,128)(2,1)} %experts.1), calls=%async_computation.3 | async-start | bytes 6291456 | tf_op jit(solution)/shard_map/all_to_all | solution.py:371
  217.5 1.2 copy-start.3

commit v3 on v2

--- a/solution.py
+++ b/solution.py
@@ -1,3 +1,4 @@
+import functools
 import math
 
 import jax
@@ -65,16 +66,15 @@
             )
             total = part if total is None else total + part
         total = total.astype(BF16)
-        for copy in range(o_ref.shape[1]):
-            o_ref[2 * i, copy] = total[:128]
-            o_ref[2 * i + 1, copy] = total[128:]
-
-
-def attend(x, copies):
+        o_ref[2 * i] = total[:128]
+        o_ref[2 * i + 1] = total[128:]
+
+
+def attend(x):
     blocks = x.shape[0]
     return pl.pallas_call(
         attend_kernel,
-        out_shape=jax.ShapeDtypeStruct((blocks, copies, 128, 128), BF16),
+        out_shape=jax.ShapeDtypeStruct((blocks, 128, 128), BF16),
         in_specs=[VMEM],
         out_specs=VMEM,
         compiler_params=pltpu.CompilerParams(vmem_limit_bytes=24 << 20),
@@ -85,34 +85,44 @@
     )(x)
 
 
-def project_kernel(index_ref, x_ref, w0, w1, w2, w3, own_ref, other_ref):
-    mine = index_ref[0]
-    heads = x_ref.shape[0]
+def project_kernel(own_x_ref, other_x_ref, *refs, parts):
+    heads = own_x_ref.shape[0]
     rows = [
-        jnp.concatenate([x_ref[h, member] for h in range(heads)], axis=1)
-        for member in (mine, 1 - mine)
+        jnp.concatenate([ref[h] for h in range(heads)], axis=1) for ref in (own_x_ref, other_x_ref)
     ]
     both = jnp.concatenate(rows, axis=0)
-    for k, w_ref in enumerate((w0, w1, w2, w3)):
+    own_ref, other_ref = refs[-2:]
+    at = 0
+    for k, count in enumerate(parts):
         for n in range(0, 512, 256):
-            out = jnp.dot(both, w_ref[:, n : n + 256], preferred_element_type=F32)
+            out, start = None, 0
+            for ref in refs[at : at + count]:
+                stop = start + ref.shape[0]
+                part = jnp.dot(
+                    both[:, start:stop], ref[:, n : n + 256], preferred_element_type=F32
+                )
+                out = part if out is None else out + part
+                start = stop
             own_ref[k, :, n : n + 256] = out[:128]
-            other_ref[k, :, n : n + 256] = out[128:].astype(BF16)
-
-
-def project(index, x, ws):
+            other_ref[k, :, n : n + 256] = out[128:]
+        at += count
+
+
+def project(own_x, other_x, shards):
+    parts = tuple(len(shard) for shard in shards)
+    weights = [part for shard in shards for part in shard]
+    count = len(parts)
+    shape = jax.ShapeDtypeStruct((count, 128, 512), F32)
     return pl.pallas_call(
-        project_kernel,
-        out_shape=(
-            jax.ShapeDtypeStruct((4, 128, 512), F32),
-            jax.ShapeDtypeStruct((4, 128, 512), BF16),
+        functools.partial(project_kernel, parts=parts),
+        out_shape=(shape, shape),
+        in_specs=[VMEM] * (2 + len(weights)),
+        out_specs=(VMEM, VMEM),
+        compiler_params=pltpu.CompilerParams(vmem_limit_bytes=24 << 20),
+        cost_estimate=pl.CostEstimate(
+            flops=count * 10**9, bytes_accessed=count * 3 * 10**6, transcendentals=0
         ),
-        in_specs=[SMEM, VMEM, VMEM, VMEM, VMEM, VMEM],
-        out_specs=(VMEM, VMEM),
-        compiler_params=pltpu.CompilerParams(vmem_limit_bytes=32 << 20),
-        cost_estimate=pl.CostEstimate(flops=2 * 10**9, bytes_accessed=11 * 10**6, transcendentals=0),
-        name="project",
-    )(index, x, *ws)
+    )(own_x, other_x, *weights)
 
 
 def to_rows(inner, outer):
@@ -128,12 +138,12 @@
 
 
 def mix_kernel(
-    place_ref, slot_ref, own_ref, got_ref, residual_ref, mixer_ref, expert_ref,
+    place_ref, slot_ref, own_ref, own_far_ref, got_ref, got_far_ref, residual_ref, mixer_ref, expert_ref,
     stream_ref, out_ref, proj_ref, rows_ref,
 ):
-    for k in range(4):
-        proj_ref[:, pl.ds(pl.multiple_of(place_ref[k] * 512, 512), 512)] = own_ref[k]
-        proj_ref[:, pl.ds(pl.multiple_of(place_ref[4 + k] * 512, 512), 512)] = got_ref[k].astype(F32)
+    blocks = [ref[k] for ref in (own_ref, own_far_ref, got_ref, got_far_ref) for k in range(ref.shape[0])]
+    for k, block in enumerate(blocks):
+        proj_ref[:, pl.ds(pl.multiple_of(place_ref[k] * 512, 512), 512)] = block
     spread = to_rows(32, 8)
     width = proj_ref.shape[1]
 
@@ -161,7 +171,7 @@
             out_ref[e, slot * 32 : slot * 32 + 32, :] = rows_ref[slot_ref[slot * experts + e]]
 
 
-def mix(place, slots, own, got, residual, mixer_gain, expert_gain):
+def mix(place, slots, projected, residual, mixer_gain, expert_gain):
     tokens, width = residual.shape
     return pl.pallas_call(
         mix_kernel,
@@ -169,13 +179,13 @@
             jax.ShapeDtypeStruct((tokens, 32, 128), BF16),
             jax.ShapeDtypeStruct((128, slots.shape[0] // 128 * 32, 128), BF16),
         ),
-        in_specs=[SMEM, SMEM, VMEM, VMEM, VMEM, VMEM, VMEM],
+        in_specs=[SMEM, SMEM] + [VMEM] * 7,
         out_specs=(VMEM, VMEM),
         scratch_shapes=[pltpu.VMEM((tokens, width), F32), pltpu.VMEM((tokens, 32, 128), BF16)],
         compiler_params=pltpu.CompilerParams(vmem_limit_bytes=24 << 20),
         cost_estimate=pl.CostEstimate(flops=10**9, bytes_accessed=8 * 10**6, transcendentals=0),
         name="mix",
-    )(place, slots, own, got, residual, mixer_gain, expert_gain)
+    )(place, slots, *projected, residual, mixer_gain, expert_gain)
 
 
 def expert_kernel(
@@ -325,16 +335,22 @@
     yh, yl, core = (lax.axis_index(a) for a in DP)
     y = yh * 2 + yl
 
-    swap = [(d, d ^ 1) for d in range(8)]
-    across = [(d, 6 - d // 2 * 2 + d % 2) for d in range(8)]
-    w_near = lax.ppermute(out_weight, DP, across)
-    w_core = lax.ppermute(out_weight, DP, swap)
-    w_near_core = lax.ppermute(w_near, DP, swap)
-
-    def held(chip):
-        return [chip * 2 + core, chip * 2 + 1 - core, 6 - chip * 2 + core, 7 - chip * 2 - core]
-
-    place = jnp.stack(held(y) + held(y ^ 1)).astype(jnp.int32)
+    right = [(d, (d + 2) % 8) for d in range(8)]
+    left = [(d, (d + 6) % 8) for d in range(8)]
+    swap = [(0, 1), (1, 0)]
+    half = out_weight.shape[0] // 2
+    top, bottom = out_weight[:half], out_weight[half:]
+    before_top = lax.ppermute(top, DP, right)
+    after_bottom = lax.ppermute(bottom, DP, left)
+    before_bottom = lax.ppermute(bottom, DP, right)
+    after_top = lax.ppermute(top, DP, left)
+    far_top = lax.ppermute(before_top, DP, right)
+    far_bottom = lax.ppermute(after_bottom, DP, left)
+
+    def held(member):
+        return [(y + step) % 4 * 2 + member for step in (0, 3, 1, 2)]
+
+    place = jnp.stack(held(core) + held(1 - core)).astype(jnp.int32)
 
     picks = routes[0].reshape(-1)
     count = picks.shape[0]
@@ -356,15 +372,18 @@
         [jnp.transpose(a[0], (1, 0, 2)) for a in (queries, key_rows, values)], axis=1
     )
     by_head = lax.all_to_all(packed, "sp", split_axis=0, concat_axis=0, tiled=True)
-    attended = attend(by_head, 2).reshape(32, 128, 128)
-    paired = lax.all_to_all(attended, ("sp", "yl"), split_axis=0, concat_axis=0, tiled=True)
+    attended = attend(by_head)
+    own_x = lax.all_to_all(attended, "sp", split_axis=0, concat_axis=0, tiled=True)
+    other_x = lax.ppermute(own_x, "c", swap)
     own, other = project(
-        yl.reshape(1).astype(jnp.int32), paired.reshape(16, 2, 128, 128),
-        (out_weight, w_core, w_near, w_near_core),
-    )
-    got = lax.ppermute(other, "yl", [(0, 1), (1, 0)])
+        own_x, other_x, ((out_weight,), (before_top, before_bottom), (after_top, after_bottom))
+    )
+    got = lax.ppermute(other, "c", swap)
+    own_far, other_far = project(own_x, other_x, ((far_top, far_bottom),))
+    got_far = lax.ppermute(other_far, "c", swap)
     stream, outgoing = mix(
-        place, slots, own, got, residual[0], mixer_gain.reshape(1, -1), expert_gain.reshape(1, -1)
+        place, slots, (own, own_far, got, got_far), residual[0], mixer_gain.reshape(1, -1),
+        expert_gain.reshape(1, -1),
     )
     arrived = lax.all_to_all(outgoing, ALL, split_axis=0, concat_axis=0, tiled=True)
     result = run_experts(arrived, gate_weight[0], up_weight[0], expert_down_matrix[0])

time: 225 us -> 218 us (0.969)
  waiting for transfers between devices: 102 us -> 72.9 us
  blocking collectives: 49.6 us -> 65 us
  local copies, waits for them, and re-layouts: 5.48 us -> 8.74 us
    ppermute x4 -> x9, waiting for transfers between devices: 44.2 us -> 15.2 us  [the longest x1 13.3 us: layer(): far_top = lax.ppermute(before_top, DP, right)]
    all_to_all x1 -> x0, waiting for transfers between devices: 16.6 us -> none  [layer(): lax.all_to_all(attended, ('sp', 'yl'), split_axis=0, concat_axis=0, tiled...]
    all_to_all x1, waiting for transfers between devices: 0.01 us -> 16.2 us  [layer(): lax.all_to_all(packed, 'sp', split_axis=0, concat_axis=0, tiled=True)]
    all_to_all x0 -> x1, blocking collectives: none -> 14.7 us  [layer(): lax.all_to_all(attended, 'sp', split_axis=0, concat_axis=0, tiled=True)]
    ppermute x4 -> x9, starting transfers between devices: 6.48 us -> 15.4 us  [the longest x1 2.73 us: layer(): after_bottom = lax.ppermute(bottom, DP, left)]
    all_to_all x1 -> x0, starting transfers between devices: 8.07 us -> none  [layer(): lax.all_to_all(attended, ('sp', 'yl'), split_axis=0, concat_axis=0, tiled...]
    pallas_call x2 -> x3, Pallas kernels: 16.6 us -> 18.4 us  [the longest x1 11.3 us: attend(): pl.pallas_call(attend_kernel, out_shape=jax.ShapeDtypeStruct((blocks, 128...]
    unnamed x23 -> x29, local copies, waits for them, and re-layouts: 3.64 us -> 5.44 us
  transfers between devices with their start and end apart: 7 -> 11, of which waited for: 4 -> 6; matrix products, arithmetic and copies ran while one was open for 2% -> 1% of each run, Pallas kernels for 5% -> 8%
where the time goes in v3:
time: 218 us; the launch traced here: 217 us
  waiting for transfers between devices  72.9 us (33%)
  blocking collectives  65 us (30%)
  Pallas kernels  40 us (18%)
  starting transfers between devices  28.4 us (13%)
  local copies, waits for them, and re-layouts  8.74 us (4%)
    all_to_all x1, blocking collectives, layer(): lax.all_to_all(outgoing, ALL, split_axis=0, concat_axis=0, tiled=True)  50.3 us
    all_to_all x1, waiting for transfers between devices, layer(): lax.all_to_all(result, ALL, split_axis=0, concat_axis=0, tiled=True)  41.5 us
    all_to_all x1, waiting for transfers between devices, layer(): lax.all_to_all(packed, 'sp', split_axis=0, concat_axis=0, tiled=True)  16.2 us
    all_to_all x1, blocking collectives, layer(): lax.all_to_all(attended, 'sp', split_axis=0, concat_axis=0, tiled=True)  14.7 us
    ppermute x1, waiting for transfers between devices, layer(): far_top = lax.ppermute(before_top, DP, right)  13.3 us
    pallas_call x1, Pallas kernels, attend(): pl.pallas_call(attend_kernel, out_shape=jax.ShapeDtypeStruct((blocks, 128...  11.3 us
    pallas_call x1, Pallas kernels, run_experts(): pl.pallas_call(expert_kernel, out_shape=pltpu.HBM(x.shape, BF16), in_spec...  11.1 us
    all_to_all x1, starting transfers between devices, layer(): lax.all_to_all(packed, 'sp', split_axis=0, concat_axis=0, tiled=True)  8.46 us
  transfers between devices with their start and end apart: 11, of which 6 were waited for; matrix products, arithmetic and copies ran while one was open for 1% of the time, Pallas kernels for 8%

profile of v3, /device:TPU:1, one launch (start us, length us, event | category | flops | bytes accessed | tf_op | source)
XLA Modules:
  0.0 216.9 jit_solution(6430298997394605536)
XLA Ops:
  0.0 1.2 copy.25
  1.2 1.5 copy_bitcast_fusion
  2.7 0.0 copy-start
  2.7 1.2 pad_maximum_fusion
  3.9 8.5 %all-to-all-start = ((bf16[16,384,128]{2,1,0:T(8,128)(2,1)}), bf16[16,384,128]{2,1,0:T(8,128)(2,1)}, u32[]{:S(2)}, u32[]{:S(2)}) async-start(bf16[16,384,128]{2,1,0:T(8,128)(2,1)} %pad_maximum_fusion), calls=%async_computation | async-start | bytes 3145728 | tf_op jit(solution)/shard_map/all_to_all | solution.py:374
  12.4 1.5 fusion.5
  13.9 2.7 %collective-permute-start.4 = (bf16[1024,512]{1,0:T(8,128)(2,1)}, bf16[1024,512]{1,0:T(8,128)(2,1)}, u32[]{:S(2)}, u32[]{:S(2)}) collective-permute-start(bf16[1024,512]{1,0:T(8,128)(2,1)} %get-tuple-element.20), channel_id=1, source_target_pairs={{0,6},{1,7},{2,0},{3,1},{4,2},{5,3},{6,4},{7,5},{8,14},{9,15},{10,... | collective-permute-start | bytes 3145736 | tf_op jit(solution)/shard_map/ppermute | solution.py:344
  16.6 0.0 collective-permute-start.2
  16.6 0.0 collective-permute-start.1
  16.6 2.7 %collective-permute-start.3 = (bf16[1024,512]{1,0:T(8,128)(2,1)}, bf16[1024,512]{1,0:T(8,128)(2,1)}, u32[]{:S(2)}, u32[]{:S(2)}) collective-permute-start(bf16[1024,512]{1,0:T(8,128)(2,1)} %get-tuple-element.21), channel_id=1, source_target_pairs={{0,6},{1,7},{2,0},{3,1},{4,2},{5,3},{6,4},{7,5},{8,14},{9,15},{10,... | collective-permute-start | bytes 3145736 | tf_op jit(solution)/shard_map/ppermute | solution.py:346
  19.3 16.2 %all-to-all-done.x_ref = bf16[16,384,128]{2,1,0:T(8,128)(2,1)} async-done(((bf16[16,384,128]{2,1,0:T(8,128)(2,1)}), bf16[16,384,128]{2,1,0:T(8,128)(2,1)}, u32[]{:S(2)}, u32[]{:S(2)}) %all-to-all-start) | async-done | bytes 1572896 | tf_op jit(solution)/shard_map/all_to_all | solution.py:374
  35.5 11.3 %attend.1 = bf16[16,128,128]{2,1,0:T(8,128)(2,1)S(1)} custom-call(bf16[16,384,128]{2,1,0:T(8,128)(2,1)} %all-to-all-done.x_ref), custom_call_target="tpu_custom_call" | custom-call | flops 12000000000 | bytes 3000000 | tf_op jit(solution)/shard_map/attend/pallas_call | solution.py:75
  46.9 14.7 %all_to_all.20.own_x_ref = bf16[16,128,128]{2,1,0:T(8,128)(2,1)S(1)} all-to-all(bf16[16,128,128]{2,1,0:T(8,128)(2,1)S(1)} %attend.1), channel_id=1, replica_groups=mesh['sp'=16,'yh'=2,'yl'=2,'c'=2] {'sp'}, dimensions={0} | all-to-all | bytes 1048576 | tf_op jit(solution)/shard_map/all_to_all | solution.py:376
  61.5 2.1 collective-permute-start
  63.6 0.5 collective-permute-done.1.refs_1_
  64.1 0.8 collective-permute-start.5
  64.9 0.0 collective-permute-done.4.refs_4_
  64.9 1.8 collective-permute-start.6
  66.8 0.1 copy.17
  66.9 0.1 reshape_squeeze.6.expert_ref
  67.0 0.0 collective-permute-done.2.refs_2_
  67.0 0.0 collective-permute-done.3.refs_3_
  67.0 4.8 %shard_map.127 = (f32[3,128,512]{2,1,0:T(8,128)S(1)}, f32[3,128,512]{2,1,0:T(8,128)}) custom-call(bf16[16,128,128]{2,1,0:T(8,128)(2,1)S(1)} %all_to_all.20.own_x_ref, bf16[16,128,128]{2,1,0:T(8,128)(2,1)S(1)} %collective-permute-done.other_x_ref, bf16[2048,512]{1,0:T(8,128)(2,1)S(1)} %copy-done, bf16[1024,512]{1,0:T(8,128)(2,1)} %collective-permute-done.1.refs_1_, ...), custom_call_target="tpu_custom_call" | custom-call | flops 3000000000 | bytes 9000000 | tf_op jit(solution)/shard_map/pallas_call | solution.py:116
  71.9 2.7 %collective-permute-start.7 = (f32[3,128,512]{2,1,0:T(8,128)}, f32[3,128,512]{2,1,0:T(8,128)S(1)}, u32[]{:S(2)}, u32[]{:S(2)}) collective-permute-start(f32[3,128,512]{2,1,0:T(8,128)} %get-tuple-element.13), channel_id=1, source_target_pairs={{0,1},{1,0},{2,3},{3,2},{4,5},{5,4},{6,7},{7,6},{8,9},{9,8},{10,11... | collective-permute-start | bytes 2359304 | tf_op jit(solution)/shard_map/ppermute | solution.py:381
  74.6 0.2 fusion
  74.9 13.3 %collective-permute-done.5.refs_0_ = bf16[1024,512]{1,0:T(8,128)(2,1)} collective-permute-done((bf16[1024,512]{1,0:T(8,128)(2,1)}, bf16[1024,512]{1,0:T(8,128)(2,1)}, u32[]{:S(2)}, u32[]{:S(2)}) %collective-permute-start.5) | collective-permute-done | bytes 1048608 | tf_op jit(solution)/shard_map/ppermute | solution.py:347
  88.2 0.4 collective-permute-done.6.refs_1_
  88.7 2.2 %shard_map.128 = (f32[1,128,512]{2,1,0:T(8,128)S(1)}, f32[1,128,512]{2,1,0:T(8,128)S(1)}) custom-call(bf16[16,128,128]{2,1,0:T(8,128)(2,1)S(1)} %all_to_all.20.own_x_ref, bf16[16,128,128]{2,1,0:T(8,128)(2,1)S(1)} %collective-permute-done.other_x_ref, bf16[1024,512]{1,0:T(8,128)(2,1)} %collective-permute-done.5.refs_0_, ...), custom_call_target="tpu_custom_call" | custom-call | flops 1000000000 | bytes 3000000 | tf_op jit(solution)/shard_map/pallas_call | solution.py:116
  90.9 0.7 copy-done.9
  91.6 2.5 %collective-permute-start.8 = (f32[1,128,512]{2,1,0:T(8,128)S(1)}, f32[1,128,512]{2,1,0:T(8,128)S(1)}, u32[]{:S(2)}, u32[]{:S(2)}) collective-permute-start(f32[1,128,512]{2,1,0:T(8,128)S(1)} %get-tuple-element.14), channel_id=1, source_target_pairs={{0,1},{1,0},{2,3},{3,2},{4,5},{5,4},{6,7},{7,6},{8,9},{9,8},{10,11... | collective-permute-start | bytes 786440 | tf_op jit(solution)/shard_map/ppermute | solution.py:383
  94.1 0.1 stack.35.place_ref
  94.2 0.2 select_reduce_fusion.2
  94.4 0.9 collective-permute-done.8.got_far_ref
  95.3 0.0 collective-permute-done.7.got_ref
  95.3 1.1 copy-done.8
  96.4 0.9 copy-done.10
  97.4 5.1 %mix.1 = (bf16[128,32,128]{2,1,0:T(8,128)(2,1)S(1)}, bf16[128,96,128]{2,1,0:T(8,128)(2,1)S(1)}) custom-call(s32[8]{0:T(128)S(1)} %stack.35.place_ref, s32[384]{0:T(512)S(1)} %pad_add_fusion.slot_ref, f32[3,128,512]{2,1,0:T(8,128)S(1)} %copy-done.8, f32[1,128,512]{2,1,0:T(8,128)S(1)} %copy-done.10, f32[3,128,512]{2,1,0:T(8,128)S(1)} %collective-permute-done.7.got_ref, ...), custom_call_target="tpu_custom_call" | custom-call | flops 1000000000 | bytes 8000000 | tf_op jit(solution)/shard_map/mix/pallas_call | solution.py:176
  102.4 0.0 copy-start.1
  102.5 50.3 %all_to_all.21.x_hbm = bf16[128,96,128]{2,1,0:T(8,128)(2,1)S(1)} all-to-all(bf16[128,96,128]{2,1,0:T(8,128)(2,1)S(1)} %get-tuple-element.15), channel_id=1, replica_groups=mesh['sp'=16,'yh'=2,'yl'=2,'c'=2] {'sp','yh','yl','c'}, dimensions={0} | all-to-all | bytes 6291456 | tf_op jit(solution)/shard_map/all_to_all | solution.py:388
  152.8 11.1 %experts.1 = bf16[128,96,128]{2,1,0:T(8,128)(2,1)} custom-call(bf16[128,96,128]{2,1,0:T(8,128)(2,1)S(1)} %all_to_all.21.x_hbm, bf16[4096,512]{1,0:T(8,128)(2,1)} %bitcast.34, bf16[4096,512]{1,0:T(8,128)(2,1)} %bitcast.35, bf16[512,4096]{1,0:T(8,128)(2,1)} %bitcast.36), custom_call_target="tpu_custom_call" | custom-call | flops 6000000000 | bytes 19000000 | tf_op jit(solution)/shard_map/experts/pallas_call | solution.py:266
  163.9 0.0 copy-start.12
  163.9 0.0 copy-start.3
  163.9 4.5 %all-to-all-start.3 = ((bf16[128,96,128]{2,1,0:T(8,128)(2,1)}), bf16[128,96,128]{2,1,0:T(8,128)(2,1)S(1)}, u32[]{:S(2)}, u32[]{:S(2)}) async-start(bf16[128,96,128]{2,1,0:T(8,128)(2,1)} %experts.1), calls=%async_computation.3 | async-start | bytes 6291456 | tf_op jit(solution)/shard_map/all_to_all | solution.py:390
  168.5 0.1 copy.18
  168.6 0.1 reshape_squeeze.7.weight_ref
  168.7 41.5 %all-to-all-done.3.x_ref = bf16[128,96,128]{2,1,0:T(8,128)(2,1)S(1)} async-done(((bf16[128,96,128]{2,1,0:T(8,128)(2,1)}), bf16[128,96,128]{2,1,0:T(8,128)(2,1)S(1)}, u32[]{:S(2)}, u32[]{:S(2)}) %all-to-all-start.3) | async-done | bytes 3145760 | tf_op jit(solution)/shard_map/all_to_all | solution.py:390
  210.2 1.2 copy-done.2
  211.5 5.5 %combine.1 = bf16[128,4096]{1,0:T(8,128)(2,1)} custom-call(s32[256]{0:T(256)S(1)} %reshape_squeeze.6.expert_ref, s32[256]{0:T(256)S(1)} %convert_element_type.2.rank_ref, f32[256]{0:T(256)S(1)} %reshape_squeeze.7.weight_ref, bf16[128,96,128]{2,1,0:T(8,128)(2,1)S(1)} %all-to-all-done.3.x_ref, bf16[128,32,128]{2,1,0:T(8,128)(2,1)S(1)} %copy-done.2, ...), custom_call_target="tpu_custom_call" | custom-call | flops 1000000000 | bytes 6000000 | tf_op jit(solution)/shard_map/combine/pallas_call | solution.py:319
  (23 shorter events, 0.1 us)
Async XLA Ops:
  2.7 9.7 %copy-start = (bf16[2048,512]{1,0:T(8,128)(2,1)S(1)}, bf16[2048,512]{1,0:T(8,128)(2,1)}, u32[]{:S(2)}) copy-start(bf16[2048,512]{1,0:T(8,128)(2,1)} %refs_0_.1) | copy-start | bytes 6291460
  3.9 31.6 %all-to-all-start = ((bf16[16,384,128]{2,1,0:T(8,128)(2,1)}), bf16[16,384,128]{2,1,0:T(8,128)(2,1)}, u32[]{:S(2)}, u32[]{:S(2)}) async-start(bf16[16,384,128]{2,1,0:T(8,128)(2,1)} %pad_maximum_fusion), calls=%async_computation | async-start | bytes 3145728 | tf_op jit(solution)/shard_map/all_to_all | solution.py:374
  13.9 51.0 %collective-permute-start.4 = (bf16[1024,512]{1,0:T(8,128)(2,1)}, bf16[1024,512]{1,0:T(8,128)(2,1)}, u32[]{:S(2)}, u32[]{:S(2)}) collective-permute-start(bf16[1024,512]{1,0:T(8,128)(2,1)} %get-tuple-element.20), channel_id=1, source_target_pairs={{0,6},{1,7},{2,0},{3,1},{4,2},{5,3},{6,4},{7,5},{8,14},{9,15},{10,... | collective-permute-start | bytes 3145736 | tf_op jit(solution)/shard_map/ppermute | solution.py:344
  16.6 50.4 %collective-permute-start.2 = (bf16[1024,512]{1,0:T(8,128)(2,1)}, bf16[1024,512]{1,0:T(8,128)(2,1)}, u32[]{:S(2)}, u32[]{:S(2)}) collective-permute-start(bf16[1024,512]{1,0:T(8,128)(2,1)} %get-tuple-element.20), channel_id=1, source_target_pairs={{0,2},{1,3},{2,4},{3,5},{4,6},{5,7},{6,0},{7,1},{8,10},{9,11},{10,... | collective-permute-start | bytes 3145736 | tf_op jit(solution)/shard_map/ppermute | solution.py:345
  16.6 50.2 %copy-start.11 = (s32[1,128,2]{1,2,0:T(2,128)S(1)}, s32[1,128,2]{1,2,0:T(2,128)}, u32[]{:S(2)}) copy-start(s32[1,128,2]{1,2,0:T(2,128)} %param.23) | copy-start | bytes 3076
  16.6 47.5 %collective-permute-start.1 = (bf16[1024,512]{1,0:T(8,128)(2,1)}, bf16[1024,512]{1,0:T(8,128)(2,1)}, u32[]{:S(2)}, u32[]{:S(2)}) collective-permute-start(bf16[1024,512]{1,0:T(8,128)(2,1)} %get-tuple-element.21), channel_id=1, source_target_pairs={{0,2},{1,3},{2,4},{3,5},{4,6},{5,7},{6,0},{7,1},{8,10},{9,11},{10,... | collective-permute-start | bytes 3145736 | tf_op jit(solution)/shard_map/ppermute | solution.py:343
  16.6 50.4 %collective-permute-start.3 = (bf16[1024,512]{1,0:T(8,128)(2,1)}, bf16[1024,512]{1,0:T(8,128)(2,1)}, u32[]{:S(2)}, u32[]{:S(2)}) collective-permute-start(bf16[1024,512]{1,0:T(8,128)(2,1)} %get-tuple-element.21), channel_id=1, source_target_pairs={{0,6},{1,7},{2,0},{3,1},{4,2},{5,3},{6,4},{7,5},{8,14},{9,15},{10,... | collective-permute-start | bytes 3145736 | tf_op jit(solution)/shard_map/ppermute | solution.py:346
  61.5 5.5 %collective-permute-start = (bf16[16,128,128]{2,1,0:T(8,128)(2,1)S(1)}, bf16[16,128,128]{2,1,0:T(8,128)(2,1)S(1)}, u32[]{:S(2)}, u32[]{:S(2)}) collective-permute-start(bf16[16,128,128]{2,1,0:T(8,128)(2,1)S(1)} %all_to_all.20.own_x_ref), channel_id=1, source_target_pairs={{0,1},{1,0},{2,3},{3,2},{4,5},{5,4},{6,7},{7,6},{8,9},{9,8},{10,11... | collective-permute-start | bytes 1572872 | tf_op jit(solution)/shard_map/ppermute | solution.py:377
  64.1 24.1 %collective-permute-start.5 = (bf16[1024,512]{1,0:T(8,128)(2,1)}, bf16[1024,512]{1,0:T(8,128)(2,1)}, u32[]{:S(2)}, u32[]{:S(2)}) collective-permute-start(bf16[1024,512]{1,0:T(8,128)(2,1)} %collective-permute-done.1.refs_1_), channel_id=1, source_target_pairs={{0,2},{1,3},{2,4},{3,5},{4,6},{5,7},{6,0},{7,1},{8,10},{9,11},{10,... | collective-permute-start | bytes 3145736 | tf_op jit(solution)/shard_map/ppermute | solution.py:347
  64.9 23.8 %collective-permute-start.6 = (bf16[1024,512]{1,0:T(8,128)(2,1)}, bf16[1024,512]{1,0:T(8,128)(2,1)}, u32[]{:S(2)}, u32[]{:S(2)}) collective-permute-start(bf16[1024,512]{1,0:T(8,128)(2,1)} %collective-permute-done.4.refs_4_), channel_id=1, source_target_pairs={{0,6},{1,7},{2,0},{3,1},{4,2},{5,3},{6,4},{7,5},{8,14},{9,15},{10,... | collective-permute-start | bytes 3145736 | tf_op jit(solution)/shard_map/ppermute | solution.py:348
  71.9 22.2 %copy-start.7 = (f32[3,128,512]{2,1,0:T(8,128)}, f32[3,128,512]{2,1,0:T(8,128)S(1)}, u32[]{:S(2)}) copy-start(f32[3,128,512]{2,1,0:T(8,128)S(1)} %get-tuple-element.11.own_ref) | copy-start | bytes 2359300
  71.9 23.4 %copy-start.4 = (bf16[1,128,4096]{2,1,0:T(8,128)(2,1)S(1)}, bf16[1,128,4096]{2,1,0:T(8,128)(2,1)}, u32[]{:S(2)}) copy-start(bf16[1,128,4096]{2,1,0:T(8,128)(2,1)} %param.16) | copy-start | bytes 3145732
  71.9 23.4 %copy-start.5 = (f32[4096]{0:T(1024)S(1)}, f32[4096]{0:T(1024)}, u32[]{:S(2)}) copy-start(f32[4096]{0:T(1024)} %param.18) | copy-start | bytes 49156
  71.9 23.4 %copy-start.6 = (f32[4096]{0:T(1024)S(1)}, f32[4096]{0:T(1024)}, u32[]{:S(2)}) copy-start(f32[4096]{0:T(1024)} %param.19) | copy-start | bytes 49156
  71.9 23.4 %collective-permute-start.7 = (f32[3,128,512]{2,1,0:T(8,128)}, f32[3,128,512]{2,1,0:T(8,128)S(1)}, u32[]{:S(2)}, u32[]{:S(2)}) collective-permute-start(f32[3,128,512]{2,1,0:T(8,128)} %get-tuple-element.13), channel_id=1, source_target_pairs={{0,1},{1,0},{2,3},{3,2},{4,5},{5,4},{6,7},{7,6},{8,9},{9,8},{10,11... | collective-permute-start | bytes 2359304 | tf_op jit(solution)/shard_map/ppermute | solution.py:381
  90.9 0.7 copy-start.9
  91.6 3.7 %collective-permute-start.8 = (f32[1,128,512]{2,1,0:T(8,128)S(1)}, f32[1,128,512]{2,1,0:T(8,128)S(1)}, u32[]{:S(2)}, u32[]{:S(2)}) collective-permute-start(f32[1,128,512]{2,1,0:T(8,128)S(1)} %get-tuple-element.14), channel_id=1, source_target_pairs={{0,1},{1,0},{2,3},{3,2},{4,5},{5,4},{6,7},{7,6},{8,9},{9,8},{10,11... | collective-permute-start | bytes 786440 | tf_op jit(solution)/shard_map/ppermute | solution.py:383
  95.3 1.1 copy-start.8
  96.4 0.9 copy-start.10
  102.4 50.4 %copy-start.1 = (bf16[128,32,128]{2,1,0:T(8,128)(2,1)}, bf16[128,32,128]{2,1,0:T(8,128)(2,1)S(1)}, u32[]{:S(2)}) copy-start(bf16[128,32,128]{2,1,0:T(8,128)(2,1)S(1)} %get-tuple-element.16.stream_ref) | copy-start | bytes 3145732
  163.9 4.5 %copy-start.12 = (f32[1,128,2]{1,2,0:T(2,128)S(1)}, f32[1,128,2]{1,2,0:T(2,128)}, u32[]{:S(2)}) copy-start(f32[1,128,2]{1,2,0:T(2,128)} %param.24) | copy-start | bytes 3076
  163.9 46.3 %copy-start.3 = (f32[4096]{0:T(1024)S(1)}, f32[4096]{0:T(1024)}, u32[]{:S(2)}) copy-start(f32[4096]{0:T(1024)} %param.25) | copy-start | bytes 49156
  163.9 46.3 %all-to-all-start.3 = ((bf16[128,96,128]{2,1,0:T(8,128)(2,1)}), bf16[128,96,128]{2,1,0:T(8,128)(2,1)S(1)}, u32[]{:S(2)}, u32[]{:S(2)}) async-start(bf16[128,96,128]{2,1,0:T(8,128)(2,1)} %experts.1), calls=%async_computation.3 | async-start | bytes 6291456 | tf_op jit(solution)/shard_map/all_to_all | solution.py:390
  210.2 1.2 copy-start.2

commit v4 on v3

--- a/solution.py
+++ b/solution.py
@@ -15,6 +15,7 @@
 DP = ("yh", "yl", "c")
 ALL = ("sp", "yh", "yl", "c")
 VMEM = pl.BlockSpec(memory_space=pltpu.VMEM)
+ANY = pl.BlockSpec(memory_space=pl.ANY)
 HBM = pl.BlockSpec(memory_space=pltpu.HBM)
 SMEM = pl.BlockSpec(memory_space=pltpu.SMEM)
 
@@ -77,7 +78,7 @@
         out_shape=jax.ShapeDtypeStruct((blocks, 128, 128), BF16),
         in_specs=[VMEM],
         out_specs=VMEM,
-        compiler_params=pltpu.CompilerParams(vmem_limit_bytes=24 << 20),
+        compiler_params=pltpu.CompilerParams(vmem_limit_bytes=14 << 20),
         cost_estimate=pl.CostEstimate(
             flops=12 * 10**9, bytes_accessed=3 * 10**6, transcendentals=7 * 10**6
         ),
@@ -85,27 +86,103 @@
     )(x)
 
 
+def split_kernel(w_hbm, top_ref, bottom_ref, sem):
+    half = top_ref.shape[0]
+    copies = [
+        pltpu.make_async_copy(w_hbm.at[pl.ds(k * half, half), :], ref, sem.at[k])
+        for k, ref in enumerate((top_ref, bottom_ref))
+    ]
+    for copy in copies:
+        copy.start()
+    for copy in copies:
+        copy.wait()
+
+
+def split(w):
+    shape = jax.ShapeDtypeStruct((w.shape[0] // 2, w.shape[1]), w.dtype)
+    return pl.pallas_call(
+        split_kernel,
+        out_shape=(shape, shape),
+        in_specs=[HBM],
+        out_specs=(VMEM, VMEM),
+        scratch_shapes=[pltpu.SemaphoreType.DMA((2,))],
+        compiler_params=pltpu.CompilerParams(vmem_limit_bytes=60 << 20),
+        cost_estimate=pl.CostEstimate(flops=10**6, bytes_accessed=4 * 10**6, transcendentals=0),
+        name="split",
+    )(w)
+
+
+def route_kernel(picks_ref, rank_ref, slot_ref):
+    tokens = picks_ref.shape[1]
+    experts = 128
+    expert = lax.broadcasted_iota(jnp.int32, (experts, tokens), 0)
+    one, zero = jnp.ones((), F32), jnp.zeros((), F32)
+    earlier = jnp.where(
+        lax.broadcasted_iota(jnp.int32, (tokens, tokens), 0)
+        < lax.broadcasted_iota(jnp.int32, (tokens, tokens), 1),
+        one, zero,
+    ).astype(BF16)
+    number = lax.broadcasted_iota(jnp.int32, (1, tokens), 1).astype(F32)
+    taken, slots = None, None
+    for k in range(picks_ref.shape[0]):
+        onehot = jnp.where(expert == picks_ref[k : k + 1, :], one, zero)
+        before = jnp.dot(onehot.astype(BF16), earlier, preferred_element_type=F32)
+        if taken is not None:
+            before = before + taken
+        rank = jnp.sum(onehot * before, axis=0, keepdims=True)
+        count = jnp.sum(onehot, axis=1, keepdims=True)
+        taken = count if taken is None else taken + count
+        rank_ref[k : k + 1, :] = rank.astype(jnp.int32)
+        slot = lax.broadcasted_iota(jnp.int32, (8, tokens), 0).astype(F32)
+        held = jnp.where(slot == rank, number, zero).astype(BF16)
+        part = lax.dot_general(
+            held, onehot.astype(BF16), (((1,), (1,)), ((), ())), preferred_element_type=F32
+        )
+        slots = part if slots is None else slots + part
+    slot_ref[...] = slots.astype(jnp.int32)
+
+
+def route(picks):
+    return pl.pallas_call(
+        route_kernel,
+        out_shape=(
+            jax.ShapeDtypeStruct(picks.shape, jnp.int32),
+            jax.ShapeDtypeStruct((8, 128), jnp.int32),
+        ),
+        in_specs=[VMEM],
+        out_specs=(VMEM, VMEM),
+        compiler_params=pltpu.CompilerParams(vmem_limit_bytes=4 << 20),
+        cost_estimate=pl.CostEstimate(flops=2 * 10**7, bytes_accessed=10**4, transcendentals=0),
+        name="route",
+    )(picks)
+
+
 def project_kernel(own_x_ref, other_x_ref, *refs, parts):
+    count = sum(parts)
+    weights, (own_ref, other_ref, w_ref, sem) = refs[:count], refs[count:]
+    copies, at = [], 0
+    for k, number in enumerate(parts):
+        rows = w_ref.shape[1] // number
+        for n in range(number):
+            target = w_ref.at[k, pl.ds(n * rows, rows), :]
+            copies.append(pltpu.make_async_copy(weights[at], target, sem.at[at]))
+            at += 1
+    for copy in copies:
+        copy.start()
     heads = own_x_ref.shape[0]
     rows = [
         jnp.concatenate([ref[h] for h in range(heads)], axis=1) for ref in (own_x_ref, other_x_ref)
     ]
     both = jnp.concatenate(rows, axis=0)
-    own_ref, other_ref = refs[-2:]
     at = 0
-    for k, count in enumerate(parts):
+    for k, number in enumerate(parts):
+        for copy in copies[at : at + number]:
+            copy.wait()
+        at += number
         for n in range(0, 512, 256):
-            out, start = None, 0
-            for ref in refs[at : at + count]:
-                stop = start + ref.shape[0]
-                part = jnp.dot(
-                    both[:, start:stop], ref[:, n : n + 256], preferred_element_type=F32
-                )
-                out = part if out is None else out + part
-                start = stop
+            out = jnp.dot(both, w_ref[k, :, n : n + 256], preferred_element_type=F32)
             own_ref[k, :, n : n + 256] = out[:128]
             other_ref[k, :, n : n + 256] = out[128:]
-        at += count
 
 
 def project(own_x, other_x, shards):
@@ -116,9 +193,13 @@
     return pl.pallas_call(
         functools.partial(project_kernel, parts=parts),
         out_shape=(shape, shape),
-        in_specs=[VMEM] * (2 + len(weights)),
+        in_specs=[VMEM, VMEM] + [ANY] * len(weights),
         out_specs=(VMEM, VMEM),
-        compiler_params=pltpu.CompilerParams(vmem_limit_bytes=24 << 20),
+        scratch_shapes=[
+            pltpu.VMEM((count, 2048, 512), BF16),
+            pltpu.SemaphoreType.DMA((len(weights),)),
+        ],
+        compiler_params=pltpu.CompilerParams(vmem_limit_bytes=(5 + 3 * count) << 20),
         cost_estimate=pl.CostEstimate(
             flops=count * 10**9, bytes_accessed=count * 3 * 10**6, transcendentals=0
         ),
@@ -138,16 +219,19 @@
 
 
 def mix_kernel(
-    place_ref, slot_ref, own_ref, own_far_ref, got_ref, got_far_ref, residual_ref, mixer_ref, expert_ref,
+    slot_ref, own_ref, own_far_ref, got_ref, got_far_ref, residual_ref, mixer_ref, expert_ref,
     stream_ref, out_ref, proj_ref, rows_ref,
 ):
-    blocks = [ref[k] for ref in (own_ref, own_far_ref, got_ref, got_far_ref) for k in range(ref.shape[0])]
-    for k, block in enumerate(blocks):
-        proj_ref[:, pl.ds(pl.multiple_of(place_ref[k] * 512, 512), 512)] = block
+    chip, core = lax.axis_index("yh") * 2 + lax.axis_index("yl"), lax.axis_index("c")
+    for member, near, far in ((core, own_ref, own_far_ref), (1 - core, got_ref, got_far_ref)):
+        for k, step in enumerate((0, 3, 1, 2)):
+            at = lax.rem(chip + step, 4) * 1024 + member * 512
+            block = near[k] if k < 3 else far[0]
+            proj_ref[:, pl.ds(pl.multiple_of(at, 512), 512)] = block
     spread = to_rows(32, 8)
     width = proj_ref.shape[1]
 
-    @pl.loop(0, proj_ref.shape[0] // 16)
+    @pl.loop(0, proj_ref.shape[0] // 16, unroll=8)
     def _(g):
         at = pl.ds(pl.multiple_of(g * 16, 16), 16)
         p = proj_ref[at, :]
@@ -165,27 +249,27 @@
 
     experts = out_ref.shape[0]
 
-    @pl.loop(0, experts, unroll=4)
+    @pl.loop(0, experts, unroll=16)
     def _(e):
         for slot in range(out_ref.shape[1] // 32):
-            out_ref[e, slot * 32 : slot * 32 + 32, :] = rows_ref[slot_ref[slot * experts + e]]
-
-
-def mix(place, slots, projected, residual, mixer_gain, expert_gain):
+            out_ref[e, slot * 32 : slot * 32 + 32, :] = rows_ref[slot_ref[slot, e]]
+
+
+def mix(slots, projected, residual, mixer_gain, expert_gain):
     tokens, width = residual.shape
     return pl.pallas_call(
         mix_kernel,
         out_shape=(
             jax.ShapeDtypeStruct((tokens, 32, 128), BF16),
-            jax.ShapeDtypeStruct((128, slots.shape[0] // 128 * 32, 128), BF16),
+            jax.ShapeDtypeStruct((128, 96, 128), BF16),
         ),
-        in_specs=[SMEM, SMEM] + [VMEM] * 7,
+        in_specs=[SMEM] + [VMEM] * 7,
         out_specs=(VMEM, VMEM),
         scratch_shapes=[pltpu.VMEM((tokens, width), F32), pltpu.VMEM((tokens, 32, 128), BF16)],
-        compiler_params=pltpu.CompilerParams(vmem_limit_bytes=24 << 20),
+        compiler_params=pltpu.CompilerParams(vmem_limit_bytes=14 << 20),
         cost_estimate=pl.CostEstimate(flops=10**9, bytes_accessed=8 * 10**6, transcendentals=0),
         name="mix",
-    )(place, slots, *projected, residual, mixer_gain, expert_gain)
+    )(slots, *projected, residual, mixer_gain, expert_gain)
 
 
 def expert_kernel(
@@ -280,7 +364,7 @@
             pltpu.SemaphoreType.DMA((slots + 3,)),
             pltpu.SemaphoreType.DMA((slots,)),
         ],
-        compiler_params=pltpu.CompilerParams(vmem_limit_bytes=48 << 20),
+        compiler_params=pltpu.CompilerParams(vmem_limit_bytes=56 << 20),
         cost_estimate=pl.CostEstimate(flops=6 * 10**9, bytes_accessed=19 * 10**6, transcendentals=0),
         name="experts",
     )(x, gate, up, down)
@@ -291,18 +375,18 @@
     gather = to_rows(8, 32)
     gain = gain_ref[...]
 
-    @pl.loop(0, tokens, unroll=8)
+    @pl.loop(0, tokens, unroll=16)
     def _(t):
         total = None
         for k in range(2):
-            rank = pl.multiple_of(rank_ref[2 * t + k] * 32, 32)
-            part = x_ref[expert_ref[2 * t + k], pl.ds(rank, 32), :].astype(F32) * weight_ref[2 * t + k]
+            rank = pl.multiple_of(rank_ref[k, t] * 32, 32)
+            part = x_ref[expert_ref[k, t], pl.ds(rank, 32), :].astype(F32) * weight_ref[k, t]
             total = part if total is None else total + part
         square = jnp.sum(jnp.sum(total * total, axis=0, keepdims=True), axis=1, keepdims=True)
         r = lax.rsqrt(square * (1.0 / 4096) + EPSILON)
         out_ref[t] = (stream_ref[t].astype(F32) + total * r * gain).astype(BF16)
 
-    @pl.loop(0, tokens // 16)
+    @pl.loop(0, tokens // 16, unroll=8)
     def _(g):
         left = out_ref[pl.ds(g * 16, 8)].reshape(256, 128)
         right = out_ref[pl.ds(g * 16 + 8, 8)].reshape(256, 128)
@@ -322,7 +406,7 @@
         in_specs=[SMEM, SMEM, SMEM, VMEM, VMEM, VMEM],
         out_specs=VMEM,
         scratch_shapes=[pltpu.VMEM((tokens, 32, 128), BF16)],
-        compiler_params=pltpu.CompilerParams(vmem_limit_bytes=24 << 20),
+        compiler_params=pltpu.CompilerParams(vmem_limit_bytes=14 << 20),
         cost_estimate=pl.CostEstimate(flops=10**9, bytes_accessed=6 * 10**6, transcendentals=0),
         name="combine",
     )(expert, rank, weight, x, stream, gain)
@@ -332,14 +416,10 @@
     queries, key_rows, values, residual, out_weight, mixer_gain, expert_gain,
     gate_weight, up_weight, expert_down_matrix, routes, route_weight, output_gain,
 ):
-    yh, yl, core = (lax.axis_index(a) for a in DP)
-    y = yh * 2 + yl
-
     right = [(d, (d + 2) % 8) for d in range(8)]
     left = [(d, (d + 6) % 8) for d in range(8)]
     swap = [(0, 1), (1, 0)]
-    half = out_weight.shape[0] // 2
-    top, bottom = out_weight[:half], out_weight[half:]
+    top, bottom = split(out_weight)
     before_top = lax.ppermute(top, DP, right)
     after_bottom = lax.ppermute(bottom, DP, left)
     before_bottom = lax.ppermute(bottom, DP, right)
@@ -347,26 +427,8 @@
     far_top = lax.ppermute(before_top, DP, right)
     far_bottom = lax.ppermute(after_bottom, DP, left)
 
-    def held(member):
-        return [(y + step) % 4 * 2 + member for step in (0, 3, 1, 2)]
-
-    place = jnp.stack(held(core) + held(1 - core)).astype(jnp.int32)
-
-    picks = routes[0].reshape(-1)
-    count = picks.shape[0]
-    onehot = picks[:, None] == lax.broadcasted_iota(jnp.int32, (count, 128), 1)
-    earlier = lax.broadcasted_iota(jnp.int32, (count, count), 0) > lax.broadcasted_iota(
-        jnp.int32, (count, count), 1
-    )
-    before = jnp.dot(earlier.astype(BF16), onehot.astype(BF16), preferred_element_type=F32)
-    rank = jnp.sum(jnp.where(onehot, before, 0.0), axis=1).astype(jnp.int32)
-    token = lax.iota(jnp.int32, count) // routes.shape[2]
-    slots = jnp.concatenate(
-        [
-            jnp.sum(jnp.where(onehot & (rank == s)[:, None], token[:, None], 0), axis=0)
-            for s in range(3)
-        ]
-    ).astype(jnp.int32)
+    picks = jnp.transpose(routes[0])
+    rank, slots = route(picks)
 
     packed = jnp.concatenate(
         [jnp.transpose(a[0], (1, 0, 2)) for a in (queries, key_rows, values)], axis=1
@@ -376,20 +438,20 @@
     own_x = lax.all_to_all(attended, "sp", split_axis=0, concat_axis=0, tiled=True)
     other_x = lax.ppermute(own_x, "c", swap)
     own, other = project(
-        own_x, other_x, ((out_weight,), (before_top, before_bottom), (after_top, after_bottom))
+        own_x, other_x, ((top, bottom), (before_top, before_bottom), (after_top, after_bottom))
     )
     got = lax.ppermute(other, "c", swap)
     own_far, other_far = project(own_x, other_x, ((far_top, far_bottom),))
     got_far = lax.ppermute(other_far, "c", swap)
     stream, outgoing = mix(
-        place, slots, (own, own_far, got, got_far), residual[0], mixer_gain.reshape(1, -1),
+        slots, (own, own_far, got, got_far), residual[0], mixer_gain.reshape(1, -1),
         expert_gain.reshape(1, -1),
     )
     arrived = lax.all_to_all(outgoing, ALL, split_axis=0, concat_axis=0, tiled=True)
     result = run_experts(arrived, gate_weight[0], up_weight[0], expert_down_matrix[0])
     returned = lax.all_to_all(result, ALL, split_axis=0, concat_axis=0, tiled=True)
     output = combine(
-        picks, rank, route_weight[0].reshape(-1), returned, stream, output_gain.reshape(32, 128)
+        picks, rank, jnp.transpose(route_weight[0]), returned, stream, output_gain.reshape(32, 128)
     )
     return output[None]
 

time: 218 us -> 210 us (0.963)
  blocking collectives: 65 us -> 112 us
  waiting for transfers between devices: 72.9 us -> 34.3 us
  local copies, waits for them, and re-layouts: 8.74 us -> 2.7 us
  Pallas kernels: 40 us -> 35.5 us
  starting transfers between devices: 28.4 us -> 24.1 us
    all_to_all x0 -> x1, blocking collectives: none -> 46.5 us  [layer(): lax.all_to_all(result, ALL, split_axis=0, concat_axis=0, tiled=True)]
    all_to_all x1 -> x0, waiting for transfers between devices: 41.5 us -> none  [layer(): lax.all_to_all(result, ALL, split_axis=0, concat_axis=0, tiled=True)]
    all_to_all x1 -> x0, starting transfers between devices: 4.49 us -> none  [layer(): lax.all_to_all(result, ALL, split_axis=0, concat_axis=0, tiled=True)]
    unnamed x29 -> x17, local copies, waits for them, and re-layouts: 5.44 us -> 1.22 us
    pallas_call x0 -> x2, Pallas kernels: none -> 3.18 us  [the longest x1 2.89 us: split(): pl.pallas_call(split_kernel, out_shape=(shape, shape), in_specs=[HBM], ou...]
    pallas_call x2, Pallas kernels: 7.08 us -> 4.08 us  [project(): pl.pallas_call(functools.partial(project_kernel, parts=parts), out_shape=...]
    ppermute x1, waiting for transfers between devices: 0.47 us -> 3.31 us  [layer(): before_top = lax.ppermute(top, DP, right)]
    pallas_call x1, Pallas kernels: 5.05 us -> 2.87 us  [mix(): pl.pallas_call(mix_kernel, out_shape=(jax.ShapeDtypeStruct((tokens, 32, 1...]
  transfers between devices with their start and end apart: 11 -> 10, of which waited for: 6 -> 4; matrix products, arithmetic and copies ran while one was open for 1% -> 0% of each run, Pallas kernels for 8% -> 8%
where the time goes in v4:
time: 210 us
  blocking collectives  112 us (53%)
  Pallas kernels  35.5 us (17%)
  waiting for transfers between devices  34.3 us (16%)
  starting transfers between devices  24.1 us (11%)
  local copies, waits for them, and re-layouts  2.7 us (1%)
    all_to_all x1, blocking collectives, layer(): lax.all_to_all(outgoing, ALL, split_axis=0, concat_axis=0, tiled=True)  50.3 us
    all_to_all x1, blocking collectives, layer(): lax.all_to_all(result, ALL, split_axis=0, concat_axis=0, tiled=True)  46.5 us
    ppermute x1, waiting for transfers between devices, layer(): far_top = lax.ppermute(before_top, DP, right)  15.4 us
    all_to_all x1, blocking collectives, layer(): lax.all_to_all(attended, 'sp', split_axis=0, concat_axis=0, tiled=True)  15.1 us
    all_to_all x1, waiting for transfers between devices, layer(): lax.all_to_all(packed, 'sp', split_axis=0, concat_axis=0, tiled=True)  14.7 us
    pallas_call x1, Pallas kernels, run_experts(): pl.pallas_call(expert_kernel, out_shape=pltpu.HBM(x.shape, BF16), in_spec...  11.8 us
    pallas_call x1, Pallas kernels, attend(): pl.pallas_call(attend_kernel, out_shape=jax.ShapeDtypeStruct((blocks, 128...  9.93 us
    all_to_all x1, starting transfers between devices, layer(): lax.all_to_all(packed, 'sp', split_axis=0, concat_axis=0, tiled=True)  8.42 us
  transfers between devices with their start and end apart: 10, of which 4 were waited for; matrix products, arithmetic and copies ran while one was open for 0% of the time, Pallas kernels for 8%

profile of v4, /device:TPU:1, one launch (start us, length us, event | category | flops | bytes accessed | tf_op | source)
XLA Modules:
  0.0 209.9 jit_solution(6671176536930247018)
XLA Ops:
  0.0 1.2 copy.20
  1.2 1.5 copy_bitcast_fusion
  2.7 1.3 pad_maximum_fusion
  3.9 8.4 %all-to-all-start = ((bf16[16,384,128]{2,1,0:T(8,128)(2,1)}), bf16[16,384,128]{2,1,0:T(8,128)(2,1)S(1)}, u32[]{:S(2)}, u32[]{:S(2)}) async-start(bf16[16,384,128]{2,1,0:T(8,128)(2,1)} %pad_maximum_fusion), calls=%async_computation | async-start | bytes 3145728 | tf_op jit(solution)/shard_map/all_to_all | solution.py:436
  12.3 2.9 %split.1 = (bf16[1024,512]{1,0:T(8,128)(2,1)}, bf16[1024,512]{1,0:T(8,128)(2,1)}) custom-call(bf16[2048,512]{1,0:T(8,128)(2,1)} %w_hbm.1), custom_call_target="tpu_custom_call" | custom-call | flops 1000000 | bytes 4000000 | tf_op jit(solution)/shard_map/split/pallas_call | solution.py:103
  15.2 2.8 %collective-permute-start.4 = (bf16[1024,512]{1,0:T(8,128)(2,1)}, bf16[1024,512]{1,0:T(8,128)(2,1)S(1)}, u32[]{:S(2)}, u32[]{:S(2)}) collective-permute-start(bf16[1024,512]{1,0:T(8,128)(2,1)} %get-tuple-element.18.refs_1_), channel_id=1, source_target_pairs={{0,6},{1,7},{2,0},{3,1},{4,2},{5,3},{6,4},{7,5},{8,14},{9,15},{10,... | collective-permute-start | bytes 3145736 | tf_op jit(solution)/shard_map/ppermute | solution.py:424
  18.1 0.0 collective-permute-start.2
  18.1 0.0 collective-permute-start.1
  18.1 2.7 %collective-permute-start.3 = (bf16[1024,512]{1,0:T(8,128)(2,1)}, bf16[1024,512]{1,0:T(8,128)(2,1)}, u32[]{:S(2)}, u32[]{:S(2)}) collective-permute-start(bf16[1024,512]{1,0:T(8,128)(2,1)} %get-tuple-element.17.refs_0_), channel_id=1, source_target_pairs={{0,6},{1,7},{2,0},{3,1},{4,2},{5,3},{6,4},{7,5},{8,14},{9,15},{10,... | collective-permute-start | bytes 3145736 | tf_op jit(solution)/shard_map/ppermute | solution.py:426
  20.8 14.7 %all-to-all-done.x_ref = bf16[16,384,128]{2,1,0:T(8,128)(2,1)S(1)} async-done(((bf16[16,384,128]{2,1,0:T(8,128)(2,1)}), bf16[16,384,128]{2,1,0:T(8,128)(2,1)S(1)}, u32[]{:S(2)}, u32[]{:S(2)}) %all-to-all-start) | async-done | bytes 1572896 | tf_op jit(solution)/shard_map/all_to_all | solution.py:436
  35.4 9.9 %attend.1 = bf16[16,128,128]{2,1,0:T(8,128)(2,1)S(1)} custom-call(bf16[16,384,128]{2,1,0:T(8,128)(2,1)S(1)} %all-to-all-done.x_ref), custom_call_target="tpu_custom_call" | custom-call | flops 12000000000 | bytes 3000000 | tf_op jit(solution)/shard_map/attend/pallas_call | solution.py:76
  45.4 15.1 %all_to_all.20.own_x_ref = bf16[16,128,128]{2,1,0:T(8,128)(2,1)S(1)} all-to-all(bf16[16,128,128]{2,1,0:T(8,128)(2,1)S(1)} %attend.1), channel_id=1, replica_groups=mesh['sp'=16,'yh'=2,'yl'=2,'c'=2] {'sp'}, dimensions={0} | all-to-all | bytes 1048576 | tf_op jit(solution)/shard_map/all_to_all | solution.py:438
  60.4 1.8 collective-permute-start
  62.2 3.3 %collective-permute-done.1.refs_2_ = bf16[1024,512]{1,0:T(8,128)(2,1)} collective-permute-done((bf16[1024,512]{1,0:T(8,128)(2,1)}, bf16[1024,512]{1,0:T(8,128)(2,1)}, u32[]{:S(2)}, u32[]{:S(2)}) %collective-permute-start.1) | collective-permute-done | bytes 1048608 | tf_op jit(solution)/shard_map/ppermute | solution.py:423
  65.5 0.0 collective-permute-start.5
  65.5 0.0 collective-permute-done.4.refs_5_
  65.5 2.7 %collective-permute-start.6 = (bf16[1024,512]{1,0:T(8,128)(2,1)S(1)}, bf16[1024,512]{1,0:T(8,128)(2,1)S(1)}, u32[]{:S(2)}, u32[]{:S(2)}) collective-permute-start(bf16[1024,512]{1,0:T(8,128)(2,1)S(1)} %collective-permute-done.4.refs_5_), channel_id=1, source_target_pairs={{0,6},{1,7},{2,0},{3,1},{4,2},{5,3},{6,4},{7,5},{8,14},{9,15},{10,... | collective-permute-start | bytes 3145736 | tf_op jit(solution)/shard_map/ppermute | solution.py:428
  68.2 0.0 collective-permute-done.2.refs_3_
  68.2 0.0 collective-permute-done.3.refs_4_
  68.2 0.0 collective-permute-done.other_x_ref
  68.2 0.0 copy-done.4
  68.2 0.0 copy-done.5
  68.2 3.2 %shard_map.127 = (f32[3,128,512]{2,1,0:T(8,128)S(1)}, f32[3,128,512]{2,1,0:T(8,128)S(1)}) custom-call(bf16[16,128,128]{2,1,0:T(8,128)(2,1)S(1)} %all_to_all.20.own_x_ref, bf16[16,128,128]{2,1,0:T(8,128)(2,1)S(1)} %collective-permute-done.other_x_ref, bf16[1024,512]{1,0:T(8,128)(2,1)S(1)} %copy-done.4, bf16[1024,512]{1,0:T(8,128)(2,1)S(1)} %copy-done.5, ...), custom_call_target="tpu_custom_call" | custom-call | flops 3000000000 | bytes 9000000 | tf_op jit(solution)/shard_map/pallas_call | solution.py:193
  71.4 0.0 copy-start.1
  71.4 0.0 copy-start.3
  71.4 0.0 copy-start.6
  71.4 0.0 copy-start.7
  71.5 2.7 %collective-permute-start.7 = (f32[3,128,512]{2,1,0:T(8,128)S(1)}, f32[3,128,512]{2,1,0:T(8,128)S(1)}, u32[]{:S(2)}, u32[]{:S(2)}) collective-permute-start(f32[3,128,512]{2,1,0:T(8,128)S(1)} %get-tuple-element.21), channel_id=1, source_target_pairs={{0,1},{1,0},{2,3},{3,2},{4,5},{5,4},{6,7},{7,6},{8,9},{9,8},{10,11... | collective-permute-start | bytes 2359304 | tf_op jit(solution)/shard_map/ppermute | solution.py:443
  74.2 15.4 %collective-permute-done.5.refs_0_ = bf16[1024,512]{1,0:T(8,128)(2,1)S(1)} collective-permute-done((bf16[1024,512]{1,0:T(8,128)(2,1)}, bf16[1024,512]{1,0:T(8,128)(2,1)S(1)}, u32[]{:S(2)}, u32[]{:S(2)}) %collective-permute-start.5) | collective-permute-done | bytes 1048608 | tf_op jit(solution)/shard_map/ppermute | solution.py:427
  89.6 0.0 collective-permute-done.6.refs_1_
  89.6 0.9 shard_map.128
  90.5 3.0 %collective-permute-start.8 = (f32[1,128,512]{2,1,0:T(8,128)S(1)}, f32[1,128,512]{2,1,0:T(8,128)S(1)}, u32[]{:S(2)}, u32[]{:S(2)}) collective-permute-start(f32[1,128,512]{2,1,0:T(8,128)S(1)} %get-tuple-element.22), channel_id=1, source_target_pairs={{0,1},{1,0},{2,3},{3,2},{4,5},{5,4},{6,7},{7,6},{8,9},{9,8},{10,11... | collective-permute-start | bytes 786440 | tf_op jit(solution)/shard_map/ppermute | solution.py:445
  93.5 0.0 copy-done.1
  93.5 0.3 route.1
  93.8 0.9 collective-permute-done.8.got_far_ref
  94.7 0.0 collective-permute-done.7.got_ref
  94.7 0.0 copy-done.3
  94.7 0.0 copy-done.6
  94.7 0.0 copy-done.7
  94.7 2.9 %mix.1 = (bf16[128,32,128]{2,1,0:T(8,128)(2,1)S(1)}, bf16[128,96,128]{2,1,0:T(8,128)(2,1)S(1)}) custom-call(s32[8,128]{1,0:T(8,128)S(1)} %get-tuple-element.16.slot_ref, f32[3,128,512]{2,1,0:T(8,128)S(1)} %get-tuple-element.19.own_ref, f32[1,128,512]{2,1,0:T(8,128)S(1)} %get-tuple-element.20.own_far_ref, f32[3,128,512]{2,1,0:T(8,128)S(1)} %collective-permute-done.7.got_ref, ...), custom_call_target="tpu_custom_call" | custom-call | flops 1000000000 | bytes 8000000 | tf_op jit(solution)/shard_map/mix/pallas_call | solution.py:260
  97.6 50.3 %all_to_all.21.x_hbm = bf16[128,96,128]{2,1,0:T(8,128)(2,1)} all-to-all(bf16[128,96,128]{2,1,0:T(8,128)(2,1)S(1)} %get-tuple-element.23), channel_id=1, replica_groups=mesh['sp'=16,'yh'=2,'yl'=2,'c'=2] {'sp','yh','yl','c'}, dimensions={0} | all-to-all | bytes 6291456 | tf_op jit(solution)/shard_map/all_to_all | solution.py:450
  147.9 11.8 %experts.1 = bf16[128,96,128]{2,1,0:T(8,128)(2,1)} custom-call(bf16[128,96,128]{2,1,0:T(8,128)(2,1)} %all_to_all.21.x_hbm, bf16[4096,512]{1,0:T(8,128)(2,1)} %bitcast.35, bf16[4096,512]{1,0:T(8,128)(2,1)} %bitcast.36, bf16[512,4096]{1,0:T(8,128)(2,1)} %bitcast.37), custom_call_target="tpu_custom_call" | custom-call | flops 6000000000 | bytes 19000000 | tf_op jit(solution)/shard_map/experts/pallas_call | solution.py:350
  159.7 0.0 copy-start
  159.7 0.0 copy-start.2
  159.7 46.5 %all_to_all.22.x_ref = bf16[128,96,128]{2,1,0:T(8,128)(2,1)S(1)} all-to-all(bf16[128,96,128]{2,1,0:T(8,128)(2,1)} %experts.1), channel_id=1, replica_groups=mesh['sp'=16,'yh'=2,'yl'=2,'c'=2] {'sp','yh','yl','c'}, dimensions={0} | all-to-all | bytes 6291456 | tf_op jit(solution)/shard_map/all_to_all | solution.py:452
  206.2 0.0 copy-done
  206.2 0.0 copy-done.2
  206.2 3.6 %combine.1 = bf16[128,4096]{1,0:T(8,128)(2,1)} custom-call(s32[2,128]{1,0:T(2,128)S(1)} %bitcast.29, s32[2,128]{1,0:T(2,128)S(1)} %get-tuple-element.15.rank_ref, f32[2,128]{1,0:T(2,128)S(1)} %bitcast.30, bf16[128,96,128]{2,1,0:T(8,128)(2,1)S(1)} %all_to_all.22.x_ref, bf16[128,32,128]{2,1,0:T(8,128)(2,1)S(1)} %get-tuple-element.24.stream_ref, ...), custom_call_target="tpu_custom_call" | custom-call | flops 1000000000 | bytes 6000000 | tf_op jit(solution)/shard_map/combine/pallas_call | solution.py:403
  (2 shorter events, 0.0 us)
Async XLA Ops:
  3.9 31.5 %all-to-all-start = ((bf16[16,384,128]{2,1,0:T(8,128)(2,1)}), bf16[16,384,128]{2,1,0:T(8,128)(2,1)S(1)}, u32[]{:S(2)}, u32[]{:S(2)}) async-start(bf16[16,384,128]{2,1,0:T(8,128)(2,1)} %pad_maximum_fusion), calls=%async_computation | async-start | bytes 3145728 | tf_op jit(solution)/shard_map/all_to_all | solution.py:436
  15.2 50.3 %collective-permute-start.4 = (bf16[1024,512]{1,0:T(8,128)(2,1)}, bf16[1024,512]{1,0:T(8,128)(2,1)S(1)}, u32[]{:S(2)}, u32[]{:S(2)}) collective-permute-start(bf16[1024,512]{1,0:T(8,128)(2,1)} %get-tuple-element.18.refs_1_), channel_id=1, source_target_pairs={{0,6},{1,7},{2,0},{3,1},{4,2},{5,3},{6,4},{7,5},{8,14},{9,15},{10,... | collective-permute-start | bytes 3145736 | tf_op jit(solution)/shard_map/ppermute | solution.py:424
  18.1 50.2 %collective-permute-start.2 = (bf16[1024,512]{1,0:T(8,128)(2,1)}, bf16[1024,512]{1,0:T(8,128)(2,1)}, u32[]{:S(2)}, u32[]{:S(2)}) collective-permute-start(bf16[1024,512]{1,0:T(8,128)(2,1)} %get-tuple-element.18.refs_1_), channel_id=1, source_target_pairs={{0,2},{1,3},{2,4},{3,5},{4,6},{5,7},{6,0},{7,1},{8,10},{9,11},{10,... | collective-permute-start | bytes 3145736 | tf_op jit(solution)/shard_map/ppermute | solution.py:425
  18.1 47.5 %collective-permute-start.1 = (bf16[1024,512]{1,0:T(8,128)(2,1)}, bf16[1024,512]{1,0:T(8,128)(2,1)}, u32[]{:S(2)}, u32[]{:S(2)}) collective-permute-start(bf16[1024,512]{1,0:T(8,128)(2,1)} %get-tuple-element.17.refs_0_), channel_id=1, source_target_pairs={{0,2},{1,3},{2,4},{3,5},{4,6},{5,7},{6,0},{7,1},{8,10},{9,11},{10,... | collective-permute-start | bytes 3145736 | tf_op jit(solution)/shard_map/ppermute | solution.py:423
  18.1 50.1 %collective-permute-start.3 = (bf16[1024,512]{1,0:T(8,128)(2,1)}, bf16[1024,512]{1,0:T(8,128)(2,1)}, u32[]{:S(2)}, u32[]{:S(2)}) collective-permute-start(bf16[1024,512]{1,0:T(8,128)(2,1)} %get-tuple-element.17.refs_0_), channel_id=1, source_target_pairs={{0,6},{1,7},{2,0},{3,1},{4,2},{5,3},{6,4},{7,5},{8,14},{9,15},{10,... | collective-permute-start | bytes 3145736 | tf_op jit(solution)/shard_map/ppermute | solution.py:426
  35.4 32.8 %copy-start.4 = (bf16[1024,512]{1,0:T(8,128)(2,1)S(1)}, bf16[1024,512]{1,0:T(8,128)(2,1)}, u32[]{:S(2)}) copy-start(bf16[1024,512]{1,0:T(8,128)(2,1)} %get-tuple-element.17.refs_0_) | copy-start | bytes 3145732
  35.4 32.8 %copy-start.5 = (bf16[1024,512]{1,0:T(8,128)(2,1)S(1)}, bf16[1024,512]{1,0:T(8,128)(2,1)}, u32[]{:S(2)}) copy-start(bf16[1024,512]{1,0:T(8,128)(2,1)} %get-tuple-element.18.refs_1_) | copy-start | bytes 3145732
  60.4 7.8 %collective-permute-start = (bf16[16,128,128]{2,1,0:T(8,128)(2,1)S(1)}, bf16[16,128,128]{2,1,0:T(8,128)(2,1)S(1)}, u32[]{:S(2)}, u32[]{:S(2)}) collective-permute-start(bf16[16,128,128]{2,1,0:T(8,128)(2,1)S(1)} %all_to_all.20.own_x_ref), channel_id=1, source_target_pairs={{0,1},{1,0},{2,3},{3,2},{4,5},{5,4},{6,7},{7,6},{8,9},{9,8},{10,11... | collective-permute-start | bytes 1572872 | tf_op jit(solution)/shard_map/ppermute | solution.py:439
  65.5 24.0 %collective-permute-start.5 = (bf16[1024,512]{1,0:T(8,128)(2,1)}, bf16[1024,512]{1,0:T(8,128)(2,1)S(1)}, u32[]{:S(2)}, u32[]{:S(2)}) collective-permute-start(bf16[1024,512]{1,0:T(8,128)(2,1)} %collective-permute-done.1.refs_2_), channel_id=1, source_target_pairs={{0,2},{1,3},{2,4},{3,5},{4,6},{5,7},{6,0},{7,1},{8,10},{9,11},{10,... | collective-permute-start | bytes 3145736 | tf_op jit(solution)/shard_map/ppermute | solution.py:427
  65.5 24.0 %collective-permute-start.6 = (bf16[1024,512]{1,0:T(8,128)(2,1)S(1)}, bf16[1024,512]{1,0:T(8,128)(2,1)S(1)}, u32[]{:S(2)}, u32[]{:S(2)}) collective-permute-start(bf16[1024,512]{1,0:T(8,128)(2,1)S(1)} %collective-permute-done.4.refs_5_), channel_id=1, source_target_pairs={{0,6},{1,7},{2,0},{3,1},{4,2},{5,3},{6,4},{7,5},{8,14},{9,15},{10,... | collective-permute-start | bytes 3145736 | tf_op jit(solution)/shard_map/ppermute | solution.py:428
  71.4 22.1 %copy-start.1 = (s32[1,128,2]{1,2,0:T(2,128)S(1)}, s32[1,128,2]{1,2,0:T(2,128)}, u32[]{:S(2)}) copy-start(s32[1,128,2]{1,2,0:T(2,128)} %param.23) | copy-start | bytes 3076
  71.4 23.3 %copy-start.3 = (bf16[1,128,4096]{2,1,0:T(8,128)(2,1)S(1)}, bf16[1,128,4096]{2,1,0:T(8,128)(2,1)}, u32[]{:S(2)}) copy-start(bf16[1,128,4096]{2,1,0:T(8,128)(2,1)} %param.16) | copy-start | bytes 3145732
  71.4 23.3 %copy-start.6 = (f32[4096]{0:T(1024)S(1)}, f32[4096]{0:T(1024)}, u32[]{:S(2)}) copy-start(f32[4096]{0:T(1024)} %param.18) | copy-start | bytes 49156
  71.4 23.3 %copy-start.7 = (f32[4096]{0:T(1024)S(1)}, f32[4096]{0:T(1024)}, u32[]{:S(2)}) copy-start(f32[4096]{0:T(1024)} %param.19) | copy-start | bytes 49156
  71.5 23.3 %collective-permute-start.7 = (f32[3,128,512]{2,1,0:T(8,128)S(1)}, f32[3,128,512]{2,1,0:T(8,128)S(1)}, u32[]{:S(2)}, u32[]{:S(2)}) collective-permute-start(f32[3,128,512]{2,1,0:T(8,128)S(1)} %get-tuple-element.21), channel_id=1, source_target_pairs={{0,1},{1,0},{2,3},{3,2},{4,5},{5,4},{6,7},{7,6},{8,9},{9,8},{10,11... | collective-permute-start | bytes 2359304 | tf_op jit(solution)/shard_map/ppermute | solution.py:443
  90.5 4.2 %collective-permute-start.8 = (f32[1,128,512]{2,1,0:T(8,128)S(1)}, f32[1,128,512]{2,1,0:T(8,128)S(1)}, u32[]{:S(2)}, u32[]{:S(2)}) collective-permute-start(f32[1,128,512]{2,1,0:T(8,128)S(1)} %get-tuple-element.22), channel_id=1, source_target_pairs={{0,1},{1,0},{2,3},{3,2},{4,5},{5,4},{6,7},{7,6},{8,9},{9,8},{10,11... | collective-permute-start | bytes 786440 | tf_op jit(solution)/shard_map/ppermute | solution.py:445
  159.7 46.6 %copy-start = (f32[4096]{0:T(1024)S(1)}, f32[4096]{0:T(1024)}, u32[]{:S(2)}) copy-start(f32[4096]{0:T(1024)} %param.25) | copy-start | bytes 49156
  159.7 46.5 %copy-start.2 = (f32[1,128,2]{1,2,0:T(2,128)S(1)}, f32[1,128,2]{1,2,0:T(2,128)}, u32[]{:S(2)}) copy-start(f32[1,128,2]{1,2,0:T(2,128)} %param.24) | copy-start | bytes 3076

commit v5 on v4

--- a/solution.py
+++ b/solution.py
@@ -1,4 +1,3 @@
-import functools
 import math
 
 import jax
@@ -86,32 +85,6 @@
     )(x)
 
 
-def split_kernel(w_hbm, top_ref, bottom_ref, sem):
-    half = top_ref.shape[0]
-    copies = [
-        pltpu.make_async_copy(w_hbm.at[pl.ds(k * half, half), :], ref, sem.at[k])
-        for k, ref in enumerate((top_ref, bottom_ref))
-    ]
-    for copy in copies:
-        copy.start()
-    for copy in copies:
-        copy.wait()
-
-
-def split(w):
-    shape = jax.ShapeDtypeStruct((w.shape[0] // 2, w.shape[1]), w.dtype)
-    return pl.pallas_call(
-        split_kernel,
-        out_shape=(shape, shape),
-        in_specs=[HBM],
-        out_specs=(VMEM, VMEM),
-        scratch_shapes=[pltpu.SemaphoreType.DMA((2,))],
-        compiler_params=pltpu.CompilerParams(vmem_limit_bytes=60 << 20),
-        cost_estimate=pl.CostEstimate(flops=10**6, bytes_accessed=4 * 10**6, transcendentals=0),
-        name="split",
-    )(w)
-
-
 def route_kernel(picks_ref, rank_ref, slot_ref):
     tokens = picks_ref.shape[1]
     experts = 128
@@ -157,16 +130,11 @@
     )(picks)
 
 
-def project_kernel(own_x_ref, other_x_ref, *refs, parts):
-    count = sum(parts)
-    weights, (own_ref, other_ref, w_ref, sem) = refs[:count], refs[count:]
-    copies, at = [], 0
-    for k, number in enumerate(parts):
-        rows = w_ref.shape[1] // number
-        for n in range(number):
-            target = w_ref.at[k, pl.ds(n * rows, rows), :]
-            copies.append(pltpu.make_async_copy(weights[at], target, sem.at[at]))
-            at += 1
+def project_kernel(own_x_ref, other_x_ref, *refs):
+    *weights, own_ref, other_ref, w_ref, sem = refs
+    copies = [
+        pltpu.make_async_copy(ref, w_ref.at[k], sem.at[k]) for k, ref in enumerate(weights)
+    ]
     for copy in copies:
         copy.start()
     heads = own_x_ref.shape[0]
@@ -174,30 +142,25 @@
         jnp.concatenate([ref[h] for h in range(heads)], axis=1) for ref in (own_x_ref, other_x_ref)
     ]
     both = jnp.concatenate(rows, axis=0)
-    at = 0
-    for k, number in enumerate(parts):
-        for copy in copies[at : at + number]:
-            copy.wait()
-        at += number
+    for k, copy in enumerate(copies):
+        copy.wait()
         for n in range(0, 512, 256):
             out = jnp.dot(both, w_ref[k, :, n : n + 256], preferred_element_type=F32)
             own_ref[k, :, n : n + 256] = out[:128]
             other_ref[k, :, n : n + 256] = out[128:]
 
 
-def project(own_x, other_x, shards):
-    parts = tuple(len(shard) for shard in shards)
-    weights = [part for shard in shards for part in shard]
-    count = len(parts)
+def project(own_x, other_x, weights):
+    count = len(weights)
     shape = jax.ShapeDtypeStruct((count, 128, 512), F32)
     return pl.pallas_call(
-        functools.partial(project_kernel, parts=parts),
+        project_kernel,
         out_shape=(shape, shape),
-        in_specs=[VMEM, VMEM] + [ANY] * len(weights),
+        in_specs=[VMEM, VMEM] + [ANY] * count,
         out_specs=(VMEM, VMEM),
         scratch_shapes=[
             pltpu.VMEM((count, 2048, 512), BF16),
-            pltpu.SemaphoreType.DMA((len(weights),)),
+            pltpu.SemaphoreType.DMA((count,)),
         ],
         compiler_params=pltpu.CompilerParams(vmem_limit_bytes=(5 + 3 * count) << 20),
         cost_estimate=pl.CostEstimate(
@@ -224,7 +187,7 @@
 ):
     chip, core = lax.axis_index("yh") * 2 + lax.axis_index("yl"), lax.axis_index("c")
     for member, near, far in ((core, own_ref, own_far_ref), (1 - core, got_ref, got_far_ref)):
-        for k, step in enumerate((0, 3, 1, 2)):
+        for k, step in enumerate((0, 3 - 2 * member, 1 + 2 * member, 2)):
             at = lax.rem(chip + step, 4) * 1024 + member * 512
             block = near[k] if k < 3 else far[0]
             proj_ref[:, pl.ds(pl.multiple_of(at, 512), 512)] = block
@@ -416,16 +379,12 @@
     queries, key_rows, values, residual, out_weight, mixer_gain, expert_gain,
     gate_weight, up_weight, expert_down_matrix, routes, route_weight, output_gain,
 ):
-    right = [(d, (d + 2) % 8) for d in range(8)]
-    left = [(d, (d + 6) % 8) for d in range(8)]
+    onward = [(d, (d + (2, 6)[d % 2]) % 8) for d in range(8)]
+    back = [(d, (d + (6, 2)[d % 2]) % 8) for d in range(8)]
     swap = [(0, 1), (1, 0)]
-    top, bottom = split(out_weight)
-    before_top = lax.ppermute(top, DP, right)
-    after_bottom = lax.ppermute(bottom, DP, left)
-    before_bottom = lax.ppermute(bottom, DP, right)
-    after_top = lax.ppermute(top, DP, left)
-    far_top = lax.ppermute(before_top, DP, right)
-    far_bottom = lax.ppermute(after_bottom, DP, left)
+    w_first = lax.ppermute(out_weight, DP, onward)
+    w_second = lax.ppermute(out_weight, DP, back)
+    w_far = lax.ppermute(w_first, DP, onward)
 
     picks = jnp.transpose(routes[0])
     rank, slots = route(picks)
@@ -437,11 +396,9 @@
     attended = attend(by_head)
     own_x = lax.all_to_all(attended, "sp", split_axis=0, concat_axis=0, tiled=True)
     other_x = lax.ppermute(own_x, "c", swap)
-    own, other = project(
-        own_x, other_x, ((top, bottom), (before_top, before_bottom), (after_top, after_bottom))
-    )
+    own, other = project(own_x, other_x, (out_weight, w_first, w_second))
     got = lax.ppermute(other, "c", swap)
-    own_far, other_far = project(own_x, other_x, ((far_top, far_bottom),))
+    own_far, other_far = project(own_x, other_x, (w_far,))
     got_far = lax.ppermute(other_far, "c", swap)
     stream, outgoing = mix(
         slots, (own, own_far, got, got_far), residual[0], mixer_gain.reshape(1, -1),

time: 210 us -> 193 us (0.919)
  waiting for transfers between devices: 34.3 us -> 26 us
  starting transfers between devices: 24.1 us -> 17.6 us
    all_to_all x1, waiting for transfers between devices: 14.7 us -> 2.47 us  [layer(): lax.all_to_all(packed, 'sp', split_axis=0, concat_axis=0, tiled=True)]
    ppermute x1, starting transfers between devices: 3.03 us -> 0.31 us  [layer(): got_far = lax.ppermute(other_far, 'c', swap)]
    ppermute x1, starting transfers between devices: 2.73 us -> 0.45 us  [layer(): got = lax.ppermute(other, 'c', swap)]
    ppermute x6 -> x3, waiting for transfers between devices: 18.7 us -> 20.9 us  [the longest x1 20.9 us: layer(): w_first = lax.ppermute(out_weight, DP, onward)]
    pallas_call x3 -> x2, Pallas kernels: 6.98 us -> 5.47 us  [project(): pl.pallas_call(project_kernel, out_shape=(shape, shape), in_specs=[VMEM,...]
    ppermute x6 -> x3, starting transfers between devices: 8.18 us -> 7.04 us  [the longest x1 3.55 us: layer(): w_first = lax.ppermute(out_weight, DP, onward)]
  transfers between devices with their start and end apart: 10 -> 7, of which waited for: 4 -> 4; matrix products, arithmetic and copies ran while one was open for 0% -> 2% of each run, Pallas kernels for 8% -> 8%
where the time goes in v5:
time: 193 us
  blocking collectives  112 us (58%)
  Pallas kernels  33.9 us (18%)
  waiting for transfers between devices  26 us (13%)
  starting transfers between devices  17.6 us (9%)
  local copies, waits for them, and re-layouts  2.69 us (1%)
    all_to_all x1, blocking collectives, layer(): lax.all_to_all(outgoing, ALL, split_axis=0, concat_axis=0, tiled=True)  48.8 us
    all_to_all x1, blocking collectives, layer(): lax.all_to_all(result, ALL, split_axis=0, concat_axis=0, tiled=True)  46.5 us
    ppermute x1, waiting for transfers between devices, layer(): w_first = lax.ppermute(out_weight, DP, onward)  20.9 us
    all_to_all x1, blocking collectives, layer(): lax.all_to_all(attended, 'sp', split_axis=0, concat_axis=0, tiled=True)  16.2 us
    pallas_call x1, Pallas kernels, run_experts(): pl.pallas_call(expert_kernel, out_shape=pltpu.HBM(x.shape, BF16), in_spec...  11.7 us
    pallas_call x1, Pallas kernels, attend(): pl.pallas_call(attend_kernel, out_shape=jax.ShapeDtypeStruct((blocks, 128...  9.94 us
    all_to_all x1, starting transfers between devices, layer(): lax.all_to_all(packed, 'sp', split_axis=0, concat_axis=0, tiled=True)  7.6 us
    pallas_call x2, Pallas kernels, project(): pl.pallas_call(project_kernel, out_shape=(shape, shape), in_specs=[VMEM,...  5.47 us
  transfers between devices with their start and end apart: 7, of which 4 were waited for; matrix products, arithmetic and copies ran while one was open for 2% of the time, Pallas kernels for 8%

profile of v5, /device:TPU:1, one launch (start us, length us, event | category | flops | bytes accessed | tf_op | source)
XLA Modules:
  0.0 193.0 jit_solution(18304892563708681793)
XLA Ops:
  0.0 3.6 %collective-permute-start.1 = (bf16[2048,512]{1,0:T(8,128)(2,1)}, bf16[2048,512]{1,0:T(8,128)(2,1)}, u32[]{:S(2)}, u32[]{:S(2)}) collective-permute-start(bf16[2048,512]{1,0:T(8,128)(2,1)} %refs_0_.1), channel_id=1, source_target_pairs={{0,2},{1,7},{2,4},{3,1},{4,6},{5,3},{6,0},{7,5},{8,10},{9,15},{10,... | collective-permute-start | bytes 6291464 | tf_op jit(solution)/shard_map/ppermute | solution.py:385
  3.6 1.2 copy.20
  4.7 1.5 copy_bitcast_fusion
  6.2 1.3 pad_maximum_fusion
  7.5 7.6 %all-to-all-start = ((bf16[16,384,128]{2,1,0:T(8,128)(2,1)}), bf16[16,384,128]{2,1,0:T(8,128)(2,1)S(1)}, u32[]{:S(2)}, u32[]{:S(2)}) async-start(bf16[16,384,128]{2,1,0:T(8,128)(2,1)} %pad_maximum_fusion), calls=%async_computation | async-start | bytes 3145728 | tf_op jit(solution)/shard_map/all_to_all | solution.py:395
  15.1 0.1 collective-permute-start.2
  15.2 20.9 %collective-permute-done.1.refs_1_ = bf16[2048,512]{1,0:T(8,128)(2,1)} collective-permute-done((bf16[2048,512]{1,0:T(8,128)(2,1)}, bf16[2048,512]{1,0:T(8,128)(2,1)}, u32[]{:S(2)}, u32[]{:S(2)}) %collective-permute-start.1) | collective-permute-done | bytes 2097184 | tf_op jit(solution)/shard_map/ppermute | solution.py:385
  36.1 3.4 %collective-permute-start.3 = (bf16[2048,512]{1,0:T(8,128)(2,1)}, bf16[2048,512]{1,0:T(8,128)(2,1)}, u32[]{:S(2)}, u32[]{:S(2)}) collective-permute-start(bf16[2048,512]{1,0:T(8,128)(2,1)} %collective-permute-done.1.refs_1_), channel_id=1, source_target_pairs={{0,2},{1,7},{2,4},{3,1},{4,6},{5,3},{6,0},{7,5},{8,10},{9,15},{10,... | collective-permute-start | bytes 6291464 | tf_op jit(solution)/shard_map/ppermute | solution.py:387
  39.5 2.5 %all-to-all-done.x_ref = bf16[16,384,128]{2,1,0:T(8,128)(2,1)S(1)} async-done(((bf16[16,384,128]{2,1,0:T(8,128)(2,1)}), bf16[16,384,128]{2,1,0:T(8,128)(2,1)S(1)}, u32[]{:S(2)}, u32[]{:S(2)}) %all-to-all-start) | async-done | bytes 1572896 | tf_op jit(solution)/shard_map/all_to_all | solution.py:395
  42.0 0.0 copy-start.3
  42.0 9.9 %attend.1 = bf16[16,128,128]{2,1,0:T(8,128)(2,1)S(1)} custom-call(bf16[16,384,128]{2,1,0:T(8,128)(2,1)S(1)} %all-to-all-done.x_ref), custom_call_target="tpu_custom_call" | custom-call | flops 12000000000 | bytes 3000000 | tf_op jit(solution)/shard_map/attend/pallas_call | solution.py:75
  51.9 16.2 %all_to_all.20.own_x_ref = bf16[16,128,128]{2,1,0:T(8,128)(2,1)S(1)} all-to-all(bf16[16,128,128]{2,1,0:T(8,128)(2,1)S(1)} %attend.1), channel_id=1, replica_groups=mesh['sp'=16,'yh'=2,'yl'=2,'c'=2] {'sp'}, dimensions={0} | all-to-all | bytes 1048576 | tf_op jit(solution)/shard_map/all_to_all | solution.py:397
  68.1 2.2 %collective-permute-start = (bf16[16,128,128]{2,1,0:T(8,128)(2,1)S(1)}, bf16[16,128,128]{2,1,0:T(8,128)(2,1)S(1)}, u32[]{:S(2)}, u32[]{:S(2)}) collective-permute-start(bf16[16,128,128]{2,1,0:T(8,128)(2,1)S(1)} %all_to_all.20.own_x_ref), channel_id=1, source_target_pairs={{0,1},{1,0},{2,3},{3,2},{4,5},{5,4},{6,7},{7,6},{8,9},{9,8},{10,11... | collective-permute-start | bytes 1572872 | tf_op jit(solution)/shard_map/ppermute | solution.py:398
  70.4 0.0 collective-permute-done.2.refs_2_
  70.4 1.5 collective-permute-done.other_x_ref
  71.9 0.0 copy-done.3
  71.9 3.2 %shard_map.127 = (f32[3,128,512]{2,1,0:T(8,128)S(1)}, f32[3,128,512]{2,1,0:T(8,128)S(1)}) custom-call(bf16[16,128,128]{2,1,0:T(8,128)(2,1)S(1)} %all_to_all.20.own_x_ref, bf16[16,128,128]{2,1,0:T(8,128)(2,1)S(1)} %collective-permute-done.other_x_ref, bf16[2048,512]{1,0:T(8,128)(2,1)S(1)} %copy-done.3, bf16[2048,512]{1,0:T(8,128)(2,1)} %collective-permute-done.1.refs_1_, ...), custom_call_target="tpu_custom_call" | custom-call | flops 3000000000 | bytes 9000000 | tf_op jit(solution)/shard_map/pallas_call | solution.py:156
  75.1 0.0 copy-start.1
  75.1 0.0 copy-start.4
  75.1 0.0 copy-start.5
  75.1 0.0 copy-start.6
  75.1 0.5 collective-permute-start.4
  75.6 0.0 collective-permute-done.3.refs_0_
  75.6 2.3 %shard_map.128 = (f32[1,128,512]{2,1,0:T(8,128)S(1)}, f32[1,128,512]{2,1,0:T(8,128)S(1)}) custom-call(bf16[16,128,128]{2,1,0:T(8,128)(2,1)S(1)} %all_to_all.20.own_x_ref, bf16[16,128,128]{2,1,0:T(8,128)(2,1)S(1)} %collective-permute-done.other_x_ref, bf16[2048,512]{1,0:T(8,128)(2,1)} %collective-permute-done.3.refs_0_), custom_call_target="tpu_custom_call" | custom-call | flops 1000000000 | bytes 3000000 | tf_op jit(solution)/shard_map/pallas_call | solution.py:156
  77.9 0.3 collective-permute-start.5
  78.2 0.0 copy-done.1
  78.2 0.3 route.1
  78.5 0.0 collective-permute-done.4.got_ref
  78.5 1.0 collective-permute-done.5.got_far_ref
  79.5 0.0 copy-done.4
  79.5 0.0 copy-done.5
  79.5 0.0 copy-done.6
  79.5 2.8 %mix.1 = (bf16[128,32,128]{2,1,0:T(8,128)(2,1)S(1)}, bf16[128,96,128]{2,1,0:T(8,128)(2,1)S(1)}) custom-call(s32[8,128]{1,0:T(8,128)S(1)} %get-tuple-element.14.slot_ref, f32[3,128,512]{2,1,0:T(8,128)S(1)} %get-tuple-element.15.own_ref, f32[1,128,512]{2,1,0:T(8,128)S(1)} %get-tuple-element.16.own_far_ref, f32[3,128,512]{2,1,0:T(8,128)S(1)} %collective-permute-done.4.got_ref, ...), custom_call_target="tpu_custom_call" | custom-call | flops 1000000000 | bytes 8000000 | tf_op jit(solution)/shard_map/mix/pallas_call | solution.py:223
  82.3 48.8 %all_to_all.21.x_hbm = bf16[128,96,128]{2,1,0:T(8,128)(2,1)} all-to-all(bf16[128,96,128]{2,1,0:T(8,128)(2,1)S(1)} %get-tuple-element.19), channel_id=1, replica_groups=mesh['sp'=16,'yh'=2,'yl'=2,'c'=2] {'sp','yh','yl','c'}, dimensions={0} | all-to-all | bytes 6291456 | tf_op jit(solution)/shard_map/all_to_all | solution.py:407
  131.1 11.7 %experts.1 = bf16[128,96,128]{2,1,0:T(8,128)(2,1)} custom-call(bf16[128,96,128]{2,1,0:T(8,128)(2,1)} %all_to_all.21.x_hbm, bf16[4096,512]{1,0:T(8,128)(2,1)} %bitcast.35, bf16[4096,512]{1,0:T(8,128)(2,1)} %bitcast.36, bf16[512,4096]{1,0:T(8,128)(2,1)} %bitcast.37), custom_call_target="tpu_custom_call" | custom-call | flops 6000000000 | bytes 19000000 | tf_op jit(solution)/shard_map/experts/pallas_call | solution.py:313
  142.9 0.0 copy-start
  142.9 0.0 copy-start.2
  142.9 46.5 %all_to_all.22.x_ref = bf16[128,96,128]{2,1,0:T(8,128)(2,1)S(1)} all-to-all(bf16[128,96,128]{2,1,0:T(8,128)(2,1)} %experts.1), channel_id=1, replica_groups=mesh['sp'=16,'yh'=2,'yl'=2,'c'=2] {'sp','yh','yl','c'}, dimensions={0} | all-to-all | bytes 6291456 | tf_op jit(solution)/shard_map/all_to_all | solution.py:409
  189.4 0.0 copy-done
  189.4 0.0 copy-done.2
  189.4 3.6 %combine.1 = bf16[128,4096]{1,0:T(8,128)(2,1)} custom-call(s32[2,128]{1,0:T(2,128)S(1)} %bitcast.29, s32[2,128]{1,0:T(2,128)S(1)} %get-tuple-element.13.rank_ref, f32[2,128]{1,0:T(2,128)S(1)} %bitcast.30, bf16[128,96,128]{2,1,0:T(8,128)(2,1)S(1)} %all_to_all.22.x_ref, bf16[128,32,128]{2,1,0:T(8,128)(2,1)S(1)} %get-tuple-element.20.stream_ref, ...), custom_call_target="tpu_custom_call" | custom-call | flops 1000000000 | bytes 6000000 | tf_op jit(solution)/shard_map/combine/pallas_call | solution.py:366
Async XLA Ops:
  0.0 36.1 %collective-permute-start.1 = (bf16[2048,512]{1,0:T(8,128)(2,1)}, bf16[2048,512]{1,0:T(8,128)(2,1)}, u32[]{:S(2)}, u32[]{:S(2)}) collective-permute-start(bf16[2048,512]{1,0:T(8,128)(2,1)} %refs_0_.1), channel_id=1, source_target_pairs={{0,2},{1,7},{2,4},{3,1},{4,6},{5,3},{6,0},{7,5},{8,10},{9,15},{10,... | collective-permute-start | bytes 6291464 | tf_op jit(solution)/shard_map/ppermute | solution.py:385
  7.5 34.5 %all-to-all-start = ((bf16[16,384,128]{2,1,0:T(8,128)(2,1)}), bf16[16,384,128]{2,1,0:T(8,128)(2,1)S(1)}, u32[]{:S(2)}, u32[]{:S(2)}) async-start(bf16[16,384,128]{2,1,0:T(8,128)(2,1)} %pad_maximum_fusion), calls=%async_computation | async-start | bytes 3145728 | tf_op jit(solution)/shard_map/all_to_all | solution.py:395
  15.1 55.3 %collective-permute-start.2 = (bf16[2048,512]{1,0:T(8,128)(2,1)}, bf16[2048,512]{1,0:T(8,128)(2,1)}, u32[]{:S(2)}, u32[]{:S(2)}) collective-permute-start(bf16[2048,512]{1,0:T(8,128)(2,1)} %refs_0_.1), channel_id=1, source_target_pairs={{0,6},{1,3},{2,0},{3,5},{4,2},{5,7},{6,4},{7,1},{8,14},{9,11},{10,... | collective-permute-start | bytes 6291464 | tf_op jit(solution)/shard_map/ppermute | solution.py:386
  36.1 39.5 %collective-permute-start.3 = (bf16[2048,512]{1,0:T(8,128)(2,1)}, bf16[2048,512]{1,0:T(8,128)(2,1)}, u32[]{:S(2)}, u32[]{:S(2)}) collective-permute-start(bf16[2048,512]{1,0:T(8,128)(2,1)} %collective-permute-done.1.refs_1_), channel_id=1, source_target_pairs={{0,2},{1,7},{2,4},{3,1},{4,6},{5,3},{6,0},{7,5},{8,10},{9,15},{10,... | collective-permute-start | bytes 6291464 | tf_op jit(solution)/shard_map/ppermute | solution.py:387
  42.0 29.9 %copy-start.3 = (bf16[2048,512]{1,0:T(8,128)(2,1)S(1)}, bf16[2048,512]{1,0:T(8,128)(2,1)}, u32[]{:S(2)}) copy-start(bf16[2048,512]{1,0:T(8,128)(2,1)} %refs_0_.1) | copy-start | bytes 6291460
  68.1 3.8 %collective-permute-start = (bf16[16,128,128]{2,1,0:T(8,128)(2,1)S(1)}, bf16[16,128,128]{2,1,0:T(8,128)(2,1)S(1)}, u32[]{:S(2)}, u32[]{:S(2)}) collective-permute-start(bf16[16,128,128]{2,1,0:T(8,128)(2,1)S(1)} %all_to_all.20.own_x_ref), channel_id=1, source_target_pairs={{0,1},{1,0},{2,3},{3,2},{4,5},{5,4},{6,7},{7,6},{8,9},{9,8},{10,11... | collective-permute-start | bytes 1572872 | tf_op jit(solution)/shard_map/ppermute | solution.py:398
  75.1 3.1 %copy-start.1 = (s32[1,128,2]{1,2,0:T(2,128)S(1)}, s32[1,128,2]{1,2,0:T(2,128)}, u32[]{:S(2)}) copy-start(s32[1,128,2]{1,2,0:T(2,128)} %param.23) | copy-start | bytes 3076
  75.1 4.4 %copy-start.4 = (bf16[1,128,4096]{2,1,0:T(8,128)(2,1)S(1)}, bf16[1,128,4096]{2,1,0:T(8,128)(2,1)}, u32[]{:S(2)}) copy-start(bf16[1,128,4096]{2,1,0:T(8,128)(2,1)} %param.16) | copy-start | bytes 3145732
  75.1 4.4 %copy-start.5 = (f32[4096]{0:T(1024)S(1)}, f32[4096]{0:T(1024)}, u32[]{:S(2)}) copy-start(f32[4096]{0:T(1024)} %param.18) | copy-start | bytes 49156
  75.1 4.4 %copy-start.6 = (f32[4096]{0:T(1024)S(1)}, f32[4096]{0:T(1024)}, u32[]{:S(2)}) copy-start(f32[4096]{0:T(1024)} %param.19) | copy-start | bytes 49156
  75.1 3.4 %collective-permute-start.4 = (f32[3,128,512]{2,1,0:T(8,128)S(1)}, f32[3,128,512]{2,1,0:T(8,128)S(1)}, u32[]{:S(2)}, u32[]{:S(2)}) collective-permute-start(f32[3,128,512]{2,1,0:T(8,128)S(1)} %get-tuple-element.17), channel_id=1, source_target_pairs={{0,1},{1,0},{2,3},{3,2},{4,5},{5,4},{6,7},{7,6},{8,9},{9,8},{10,11... | collective-permute-start | bytes 2359304 | tf_op jit(solution)/shard_map/ppermute | solution.py:400
  77.9 1.6 collective-permute-start.5
  142.9 46.6 %copy-start = (f32[4096]{0:T(1024)S(1)}, f32[4096]{0:T(1024)}, u32[]{:S(2)}) copy-start(f32[4096]{0:T(1024)} %param.25) | copy-start | bytes 49156
  142.9 46.5 %copy-start.2 = (f32[1,128,2]{1,2,0:T(2,128)S(1)}, f32[1,128,2]{1,2,0:T(2,128)}, u32[]{:S(2)}) copy-start(f32[1,128,2]{1,2,0:T(2,128)} %param.24) | copy-start | bytes 3076

commit v6 on v5

--- a/solution.py
+++ b/solution.py
@@ -235,30 +235,13 @@
     )(slots, *projected, residual, mixer_gain, expert_gain)
 
 
-def expert_kernel(
-    x_hbm, gate_hbm, up_hbm, down_hbm, o_hbm,
-    x_ref, gate_ref, up_ref, down_ref, o_ref, rows_ref, hidden_ref, result_ref, in_sem, out_sem,
-):
+def expert_kernel(x_ref, gate_ref, up_ref, down_ref, o_ref, rows_ref, hidden_ref, result_ref):
     sources = x_ref.shape[0]
     slots = x_ref.shape[1] // 32
     gather = to_rows(8, 32)
     spread = to_rows(32, 8)
-    weights = ((gate_hbm, gate_ref), (up_hbm, up_ref), (down_hbm, down_ref))
-
-    def slot_copy(source, target, sem, slot):
-        at = pl.ds(slot * 32, 32)
-        return pltpu.make_async_copy(source.at[:, at, :], target.at[:, at, :], sem.at[slot])
-
-    x_copies = [slot_copy(x_hbm, x_ref, in_sem, slot) for slot in range(slots)]
-    w_copies = [
-        pltpu.make_async_copy(source, target, in_sem.at[slots + k])
-        for k, (source, target) in enumerate(weights)
-    ]
-    for copy in x_copies + w_copies:
-        copy.start()
 
     for slot in range(slots):
-        x_copies[slot].wait()
 
         @pl.loop(0, sources // 16, unroll=8)
         def _(g):
@@ -274,20 +257,16 @@
                     [got[c * 8 : c * 8 + 8, :128], got[c * 8 : c * 8 + 8, 128:]], axis=0
                 ).astype(BF16)
 
-    w_copies[0].wait()
-    w_copies[1].wait()
     for n in range(0, 512, 256):
         a = jnp.dot(rows_ref[...], gate_ref[:, n : n + 256], preferred_element_type=F32)
         b = jnp.dot(rows_ref[...], up_ref[:, n : n + 256], preferred_element_type=F32)
         hidden_ref[:, n : n + 256] = (a / (1.0 + jnp.exp(-a)) * b).astype(BF16)
 
-    w_copies[2].wait()
     for n in range(0, 4096, 1024):
         result_ref[:, n : n + 1024] = jnp.dot(
             hidden_ref[...], down_ref[:, n : n + 1024], preferred_element_type=F32
         )
 
-    o_copies = [slot_copy(o_ref, o_hbm, out_sem, slot) for slot in range(slots)]
     for slot in range(slots):
 
         @pl.loop(0, sources // 16, unroll=8)
@@ -302,32 +281,20 @@
             o_ref[pl.ds(g * 16, 8), at, :] = out[:, :128].reshape(8, 32, 128)
             o_ref[pl.ds(g * 16 + 8, 8), at, :] = out[:, 128:].reshape(8, 32, 128)
 
-        o_copies[slot].start()
-    for copy in o_copies:
-        copy.wait()
-
 
 def run_experts(x, gate, up, down):
-    slots = x.shape[1] // 32
-    rows = x.shape[0] * slots
+    rows = x.shape[0] * (x.shape[1] // 32)
     return pl.pallas_call(
         expert_kernel,
-        out_shape=pltpu.HBM(x.shape, BF16),
-        in_specs=[HBM] * 4,
-        out_specs=HBM,
+        out_shape=jax.ShapeDtypeStruct(x.shape, BF16),
+        in_specs=[VMEM] * 4,
+        out_specs=VMEM,
         scratch_shapes=[
-            pltpu.VMEM(x.shape, BF16),
-            pltpu.VMEM(gate.shape, BF16),
-            pltpu.VMEM(up.shape, BF16),
-            pltpu.VMEM(down.shape, BF16),
-            pltpu.VMEM(x.shape, BF16),
             pltpu.VMEM((rows, 4096), BF16),
             pltpu.VMEM((rows, 512), BF16),
             pltpu.VMEM((rows, 4096), F32),
-            pltpu.SemaphoreType.DMA((slots + 3,)),
-            pltpu.SemaphoreType.DMA((slots,)),
         ],
-        compiler_params=pltpu.CompilerParams(vmem_limit_bytes=56 << 20),
+        compiler_params=pltpu.CompilerParams(vmem_limit_bytes=18 << 20),
         cost_estimate=pl.CostEstimate(flops=6 * 10**9, bytes_accessed=19 * 10**6, transcendentals=0),
         name="experts",
     )(x, gate, up, down)

time: 193 us -> 188 us (0.974)
  Pallas kernels: 33.9 us -> 29.1 us
  blocking collectives: 112 us -> 110 us
    pallas_call x1, Pallas kernels: 11.7 us -> 6.73 us  [run_experts(): pl.pallas_call(expert_kernel, out_shape=jax.ShapeDtypeStruct(x.shape, BF1...]
where the time goes in v6:
time: 188 us; the launch traced here: 187 us
  blocking collectives  110 us (59%)
  Pallas kernels  29.1 us (15%)
  waiting for transfers between devices  26 us (14%)
  starting transfers between devices  17.5 us (9%)
  local copies, waits for them, and re-layouts  2.71 us (1%)
    all_to_all x1, blocking collectives, layer(): lax.all_to_all(outgoing, ALL, split_axis=0, concat_axis=0, tiled=True)  48.7 us
    all_to_all x1, blocking collectives, layer(): lax.all_to_all(result, ALL, split_axis=0, concat_axis=0, tiled=True)  45.6 us
    ppermute x1, waiting for transfers between devices, layer(): w_first = lax.ppermute(out_weight, DP, onward)  20.9 us
    all_to_all x1, blocking collectives, layer(): lax.all_to_all(attended, 'sp', split_axis=0, concat_axis=0, tiled=True)  16.2 us
    pallas_call x1, Pallas kernels, attend(): pl.pallas_call(attend_kernel, out_shape=jax.ShapeDtypeStruct((blocks, 128...  9.94 us
    all_to_all x1, starting transfers between devices, layer(): lax.all_to_all(packed, 'sp', split_axis=0, concat_axis=0, tiled=True)  7.6 us
    pallas_call x1, Pallas kernels, run_experts(): pl.pallas_call(expert_kernel, out_shape=jax.ShapeDtypeStruct(x.shape, BF1...  6.73 us
    pallas_call x2, Pallas kernels, project(): pl.pallas_call(project_kernel, out_shape=(shape, shape), in_specs=[VMEM,...  5.63 us
  transfers between devices with their start and end apart: 7, of which 4 were waited for; matrix products, arithmetic and copies ran while one was open for 2% of the time, Pallas kernels for 8%

profile of v6, /device:TPU:1, one launch (start us, length us, event | category | flops | bytes accessed | tf_op | source)
XLA Modules:
  0.0 187.3 jit_solution(16397248600375925565)
XLA Ops:
  0.0 3.6 %collective-permute-start.1 = (bf16[2048,512]{1,0:T(8,128)(2,1)}, bf16[2048,512]{1,0:T(8,128)(2,1)}, u32[]{:S(2)}, u32[]{:S(2)}) collective-permute-start(bf16[2048,512]{1,0:T(8,128)(2,1)} %refs_0_.1), channel_id=1, source_target_pairs={{0,2},{1,7},{2,4},{3,1},{4,6},{5,3},{6,0},{7,5},{8,10},{9,15},{10,... | collective-permute-start | bytes 6291464 | tf_op jit(solution)/shard_map/ppermute | solution.py:352
  3.6 1.2 copy.20
  4.7 1.5 copy_bitcast_fusion
  6.2 1.3 pad_maximum_fusion
  7.5 7.6 %all-to-all-start = ((bf16[16,384,128]{2,1,0:T(8,128)(2,1)}), bf16[16,384,128]{2,1,0:T(8,128)(2,1)S(1)}, u32[]{:S(2)}, u32[]{:S(2)}) async-start(bf16[16,384,128]{2,1,0:T(8,128)(2,1)} %pad_maximum_fusion), calls=%async_computation | async-start | bytes 3145728 | tf_op jit(solution)/shard_map/all_to_all | solution.py:362
  15.1 0.1 collective-permute-start.2
  15.2 20.9 %collective-permute-done.1.refs_1_ = bf16[2048,512]{1,0:T(8,128)(2,1)} collective-permute-done((bf16[2048,512]{1,0:T(8,128)(2,1)}, bf16[2048,512]{1,0:T(8,128)(2,1)}, u32[]{:S(2)}, u32[]{:S(2)}) %collective-permute-start.1) | collective-permute-done | bytes 2097184 | tf_op jit(solution)/shard_map/ppermute | solution.py:352
  36.1 3.4 %collective-permute-start.3 = (bf16[2048,512]{1,0:T(8,128)(2,1)}, bf16[2048,512]{1,0:T(8,128)(2,1)}, u32[]{:S(2)}, u32[]{:S(2)}) collective-permute-start(bf16[2048,512]{1,0:T(8,128)(2,1)} %collective-permute-done.1.refs_1_), channel_id=1, source_target_pairs={{0,2},{1,7},{2,4},{3,1},{4,6},{5,3},{6,0},{7,5},{8,10},{9,15},{10,... | collective-permute-start | bytes 6291464 | tf_op jit(solution)/shard_map/ppermute | solution.py:354
  39.5 2.5 %all-to-all-done.x_ref = bf16[16,384,128]{2,1,0:T(8,128)(2,1)S(1)} async-done(((bf16[16,384,128]{2,1,0:T(8,128)(2,1)}), bf16[16,384,128]{2,1,0:T(8,128)(2,1)S(1)}, u32[]{:S(2)}, u32[]{:S(2)}) %all-to-all-start) | async-done | bytes 1572896 | tf_op jit(solution)/shard_map/all_to_all | solution.py:362
  42.0 0.0 copy-start.6
  42.0 9.9 %attend.1 = bf16[16,128,128]{2,1,0:T(8,128)(2,1)S(1)} custom-call(bf16[16,384,128]{2,1,0:T(8,128)(2,1)S(1)} %all-to-all-done.x_ref), custom_call_target="tpu_custom_call" | custom-call | flops 12000000000 | bytes 3000000 | tf_op jit(solution)/shard_map/attend/pallas_call | solution.py:75
  51.9 16.2 %all_to_all.20.own_x_ref = bf16[16,128,128]{2,1,0:T(8,128)(2,1)S(1)} all-to-all(bf16[16,128,128]{2,1,0:T(8,128)(2,1)S(1)} %attend.1), channel_id=1, replica_groups=mesh['sp'=16,'yh'=2,'yl'=2,'c'=2] {'sp'}, dimensions={0} | all-to-all | bytes 1048576 | tf_op jit(solution)/shard_map/all_to_all | solution.py:364
  68.1 2.2 %collective-permute-start = (bf16[16,128,128]{2,1,0:T(8,128)(2,1)S(1)}, bf16[16,128,128]{2,1,0:T(8,128)(2,1)S(1)}, u32[]{:S(2)}, u32[]{:S(2)}) collective-permute-start(bf16[16,128,128]{2,1,0:T(8,128)(2,1)S(1)} %all_to_all.20.own_x_ref), channel_id=1, source_target_pairs={{0,1},{1,0},{2,3},{3,2},{4,5},{5,4},{6,7},{7,6},{8,9},{9,8},{10,11... | collective-permute-start | bytes 1572872 | tf_op jit(solution)/shard_map/ppermute | solution.py:365
  70.3 0.0 collective-permute-done.2.refs_2_
  70.3 1.5 collective-permute-done.other_x_ref
  71.9 0.0 copy-done.6
  71.9 3.2 %shard_map.127 = (f32[3,128,512]{2,1,0:T(8,128)S(1)}, f32[3,128,512]{2,1,0:T(8,128)S(1)}) custom-call(bf16[16,128,128]{2,1,0:T(8,128)(2,1)S(1)} %all_to_all.20.own_x_ref, bf16[16,128,128]{2,1,0:T(8,128)(2,1)S(1)} %collective-permute-done.other_x_ref, bf16[2048,512]{1,0:T(8,128)(2,1)S(1)} %copy-done.6, bf16[2048,512]{1,0:T(8,128)(2,1)} %collective-permute-done.1.refs_1_, ...), custom_call_target="tpu_custom_call" | custom-call | flops 3000000000 | bytes 9000000 | tf_op jit(solution)/shard_map/pallas_call | solution.py:156
  75.1 0.0 copy-start.1
  75.1 0.0 copy-start.7
  75.1 0.0 copy-start.8
  75.1 0.0 copy-start.9
  75.1 0.5 collective-permute-start.4
  75.6 0.0 collective-permute-done.3.refs_0_
  75.6 0.0 copy-start.5
  75.6 2.5 %shard_map.128 = (f32[1,128,512]{2,1,0:T(8,128)S(1)}, f32[1,128,512]{2,1,0:T(8,128)S(1)}) custom-call(bf16[16,128,128]{2,1,0:T(8,128)(2,1)S(1)} %all_to_all.20.own_x_ref, bf16[16,128,128]{2,1,0:T(8,128)(2,1)S(1)} %collective-permute-done.other_x_ref, bf16[2048,512]{1,0:T(8,128)(2,1)} %collective-permute-done.3.refs_0_), custom_call_target="tpu_custom_call" | custom-call | flops 1000000000 | bytes 3000000 | tf_op jit(solution)/shard_map/pallas_call | solution.py:156
  78.0 0.2 collective-permute-start.5
  78.2 0.0 copy-done.1
  78.3 0.3 route.1
  78.5 0.0 collective-permute-done.4.got_ref
  78.5 1.1 collective-permute-done.5.got_far_ref
  79.6 0.0 copy-done.7
  79.7 0.0 copy-done.8
  79.7 0.0 copy-done.9
  79.7 0.0 copy-start.4
  79.7 2.9 %mix.1 = (bf16[128,32,128]{2,1,0:T(8,128)(2,1)S(1)}, bf16[128,96,128]{2,1,0:T(8,128)(2,1)S(1)}) custom-call(s32[8,128]{1,0:T(8,128)S(1)} %get-tuple-element.14.slot_ref, f32[3,128,512]{2,1,0:T(8,128)S(1)} %get-tuple-element.15.own_ref, f32[1,128,512]{2,1,0:T(8,128)S(1)} %get-tuple-element.16.own_far_ref, f32[3,128,512]{2,1,0:T(8,128)S(1)} %collective-permute-done.4.got_ref, ...), custom_call_target="tpu_custom_call" | custom-call | flops 1000000000 | bytes 8000000 | tf_op jit(solution)/shard_map/mix/pallas_call | solution.py:223
  82.6 0.0 copy-start.3
  82.6 48.7 %all_to_all.21.x_ref = bf16[128,96,128]{2,1,0:T(8,128)(2,1)S(1)} all-to-all(bf16[128,96,128]{2,1,0:T(8,128)(2,1)S(1)} %get-tuple-element.19), channel_id=1, replica_groups=mesh['sp'=16,'yh'=2,'yl'=2,'c'=2] {'sp','yh','yl','c'}, dimensions={0} | all-to-all | bytes 6291456 | tf_op jit(solution)/shard_map/all_to_all | solution.py:374
  131.3 0.0 copy-done.5
  131.3 0.0 copy-done.4
  131.3 0.0 copy-done.3
  131.3 6.7 %experts.1 = bf16[128,96,128]{2,1,0:T(8,128)(2,1)S(1)} custom-call(bf16[128,96,128]{2,1,0:T(8,128)(2,1)S(1)} %all_to_all.21.x_ref, bf16[4096,512]{1,0:T(8,128)(2,1)S(1)} %bitcast.31, bf16[4096,512]{1,0:T(8,128)(2,1)S(1)} %bitcast.32, bf16[512,4096]{1,0:T(8,128)(2,1)S(1)} %bitcast.33), custom_call_target="tpu_custom_call" | custom-call | flops 6000000000 | bytes 19000000 | tf_op jit(solution)/shard_map/experts/pallas_call | solution.py:287
  138.0 0.0 copy-start
  138.0 0.0 copy-start.2
  138.0 45.6 %all_to_all.22.x_ref = bf16[128,96,128]{2,1,0:T(8,128)(2,1)S(1)} all-to-all(bf16[128,96,128]{2,1,0:T(8,128)(2,1)S(1)} %experts.1), channel_id=1, replica_groups=mesh['sp'=16,'yh'=2,'yl'=2,'c'=2] {'sp','yh','yl','c'}, dimensions={0} | all-to-all | bytes 6291456 | tf_op jit(solution)/shard_map/all_to_all | solution.py:376
  183.7 0.0 copy-done
  183.7 0.0 copy-done.2
  183.7 3.6 %combine.1 = bf16[128,4096]{1,0:T(8,128)(2,1)} custom-call(s32[2,128]{1,0:T(2,128)S(1)} %bitcast.29, s32[2,128]{1,0:T(2,128)S(1)} %get-tuple-element.13.rank_ref, f32[2,128]{1,0:T(2,128)S(1)} %bitcast.30, bf16[128,96,128]{2,1,0:T(8,128)(2,1)S(1)} %all_to_all.22.x_ref, bf16[128,32,128]{2,1,0:T(8,128)(2,1)S(1)} %get-tuple-element.20.stream_ref, ...), custom_call_target="tpu_custom_call" | custom-call | flops 1000000000 | bytes 6000000 | tf_op jit(solution)/shard_map/combine/pallas_call | solution.py:333
Async XLA Ops:
  0.0 36.1 %collective-permute-start.1 = (bf16[2048,512]{1,0:T(8,128)(2,1)}, bf16[2048,512]{1,0:T(8,128)(2,1)}, u32[]{:S(2)}, u32[]{:S(2)}) collective-permute-start(bf16[2048,512]{1,0:T(8,128)(2,1)} %refs_0_.1), channel_id=1, source_target_pairs={{0,2},{1,7},{2,4},{3,1},{4,6},{5,3},{6,0},{7,5},{8,10},{9,15},{10,... | collective-permute-start | bytes 6291464 | tf_op jit(solution)/shard_map/ppermute | solution.py:352
  7.5 34.5 %all-to-all-start = ((bf16[16,384,128]{2,1,0:T(8,128)(2,1)}), bf16[16,384,128]{2,1,0:T(8,128)(2,1)S(1)}, u32[]{:S(2)}, u32[]{:S(2)}) async-start(bf16[16,384,128]{2,1,0:T(8,128)(2,1)} %pad_maximum_fusion), calls=%async_computation | async-start | bytes 3145728 | tf_op jit(solution)/shard_map/all_to_all | solution.py:362
  15.1 55.3 %collective-permute-start.2 = (bf16[2048,512]{1,0:T(8,128)(2,1)}, bf16[2048,512]{1,0:T(8,128)(2,1)}, u32[]{:S(2)}, u32[]{:S(2)}) collective-permute-start(bf16[2048,512]{1,0:T(8,128)(2,1)} %refs_0_.1), channel_id=1, source_target_pairs={{0,6},{1,3},{2,0},{3,5},{4,2},{5,7},{6,4},{7,1},{8,14},{9,11},{10,... | collective-permute-start | bytes 6291464 | tf_op jit(solution)/shard_map/ppermute | solution.py:353
  36.1 39.5 %collective-permute-start.3 = (bf16[2048,512]{1,0:T(8,128)(2,1)}, bf16[2048,512]{1,0:T(8,128)(2,1)}, u32[]{:S(2)}, u32[]{:S(2)}) collective-permute-start(bf16[2048,512]{1,0:T(8,128)(2,1)} %collective-permute-done.1.refs_1_), channel_id=1, source_target_pairs={{0,2},{1,7},{2,4},{3,1},{4,6},{5,3},{6,0},{7,5},{8,10},{9,15},{10,... | collective-permute-start | bytes 6291464 | tf_op jit(solution)/shard_map/ppermute | solution.py:354
  42.0 29.9 %copy-start.6 = (bf16[2048,512]{1,0:T(8,128)(2,1)S(1)}, bf16[2048,512]{1,0:T(8,128)(2,1)}, u32[]{:S(2)}) copy-start(bf16[2048,512]{1,0:T(8,128)(2,1)} %refs_0_.1) | copy-start | bytes 6291460
  68.1 3.8 %collective-permute-start = (bf16[16,128,128]{2,1,0:T(8,128)(2,1)S(1)}, bf16[16,128,128]{2,1,0:T(8,128)(2,1)S(1)}, u32[]{:S(2)}, u32[]{:S(2)}) collective-permute-start(bf16[16,128,128]{2,1,0:T(8,128)(2,1)S(1)} %all_to_all.20.own_x_ref), channel_id=1, source_target_pairs={{0,1},{1,0},{2,3},{3,2},{4,5},{5,4},{6,7},{7,6},{8,9},{9,8},{10,11... | collective-permute-start | bytes 1572872 | tf_op jit(solution)/shard_map/ppermute | solution.py:365
  75.1 3.2 %copy-start.1 = (s32[1,128,2]{1,2,0:T(2,128)S(1)}, s32[1,128,2]{1,2,0:T(2,128)}, u32[]{:S(2)}) copy-start(s32[1,128,2]{1,2,0:T(2,128)} %param.23) | copy-start | bytes 3076
  75.1 4.6 %copy-start.7 = (bf16[1,128,4096]{2,1,0:T(8,128)(2,1)S(1)}, bf16[1,128,4096]{2,1,0:T(8,128)(2,1)}, u32[]{:S(2)}) copy-start(bf16[1,128,4096]{2,1,0:T(8,128)(2,1)} %param.16) | copy-start | bytes 3145732
  75.1 4.6 %copy-start.8 = (f32[4096]{0:T(1024)S(1)}, f32[4096]{0:T(1024)}, u32[]{:S(2)}) copy-start(f32[4096]{0:T(1024)} %param.18) | copy-start | bytes 49156
  75.1 4.6 %copy-start.9 = (f32[4096]{0:T(1024)S(1)}, f32[4096]{0:T(1024)}, u32[]{:S(2)}) copy-start(f32[4096]{0:T(1024)} %param.19) | copy-start | bytes 49156
  75.1 3.4 %collective-permute-start.4 = (f32[3,128,512]{2,1,0:T(8,128)S(1)}, f32[3,128,512]{2,1,0:T(8,128)S(1)}, u32[]{:S(2)}, u32[]{:S(2)}) collective-permute-start(f32[3,128,512]{2,1,0:T(8,128)S(1)} %get-tuple-element.17), channel_id=1, source_target_pairs={{0,1},{1,0},{2,3},{3,2},{4,5},{5,4},{6,7},{7,6},{8,9},{9,8},{10,11... | collective-permute-start | bytes 2359304 | tf_op jit(solution)/shard_map/ppermute | solution.py:367
  75.6 55.7 %copy-start.5 = (bf16[1,512,4096]{2,1,0:T(8,128)(2,1)S(1)}, bf16[1,512,4096]{2,1,0:T(8,128)(2,1)}, u32[]{:S(2)}) copy-start(bf16[1,512,4096]{2,1,0:T(8,128)(2,1)} %param.22) | copy-start | bytes 12582916
  78.0 1.6 collective-permute-start.5
  79.7 51.6 %copy-start.4 = (bf16[1,4096,512]{2,1,0:T(8,128)(2,1)S(1)}, bf16[1,4096,512]{2,1,0:T(8,128)(2,1)}, u32[]{:S(2)}) copy-start(bf16[1,4096,512]{2,1,0:T(8,128)(2,1)} %param.21) | copy-start | bytes 12582916
  82.6 48.7 %copy-start.3 = (bf16[1,4096,512]{2,1,0:T(8,128)(2,1)S(1)}, bf16[1,4096,512]{2,1,0:T(8,128)(2,1)}, u32[]{:S(2)}) copy-start(bf16[1,4096,512]{2,1,0:T(8,128)(2,1)} %param.20) | copy-start | bytes 12582916
  138.0 45.7 %copy-start = (f32[4096]{0:T(1024)S(1)}, f32[4096]{0:T(1024)}, u32[]{:S(2)}) copy-start(f32[4096]{0:T(1024)} %param.25) | copy-start | bytes 49156
  138.0 45.6 %copy-start.2 = (f32[1,128,2]{1,2,0:T(2,128)S(1)}, f32[1,128,2]{1,2,0:T(2,128)}, u32[]{:S(2)}) copy-start(f32[1,128,2]{1,2,0:T(2,128)} %param.24) | copy-start | bytes 3076

commit v7 on v6

--- a/solution.py
+++ b/solution.py
@@ -16,6 +16,7 @@
 VMEM = pl.BlockSpec(memory_space=pltpu.VMEM)
 ANY = pl.BlockSpec(memory_space=pl.ANY)
 HBM = pl.BlockSpec(memory_space=pltpu.HBM)
+CHUNKS = 4
 SMEM = pl.BlockSpec(memory_space=pltpu.SMEM)
 
 
@@ -300,13 +301,14 @@
     )(x, gate, up, down)
 
 
-def combine_kernel(expert_ref, rank_ref, weight_ref, x_ref, stream_ref, gain_ref, o_ref, out_ref):
+def combine_kernel(
+    expert_ref, rank_ref, weight_ref, x_ref, stream_ref, gain_ref, o_hbm, o_ref, sem
+):
     tokens = stream_ref.shape[0]
     gather = to_rows(8, 32)
     gain = gain_ref[...]
 
-    @pl.loop(0, tokens, unroll=16)
-    def _(t):
+    def one(t):
         total = None
         for k in range(2):
             rank = pl.multiple_of(rank_ref[k, t] * 32, 32)
@@ -314,18 +316,30 @@
             total = part if total is None else total + part
         square = jnp.sum(jnp.sum(total * total, axis=0, keepdims=True), axis=1, keepdims=True)
         r = lax.rsqrt(square * (1.0 / 4096) + EPSILON)
-        out_ref[t] = (stream_ref[t].astype(F32) + total * r * gain).astype(BF16)
-
-    @pl.loop(0, tokens // 16, unroll=8)
-    def _(g):
-        left = out_ref[pl.ds(g * 16, 8)].reshape(256, 128)
-        right = out_ref[pl.ds(g * 16 + 8, 8)].reshape(256, 128)
-        got = jnp.dot(gather, jnp.concatenate([left, right], axis=1), preferred_element_type=F32)
-        to = pl.ds(pl.multiple_of(g * 16, 16), 16)
-        for c in range(32):
-            o_ref[to, c * 128 : c * 128 + 128] = jnp.concatenate(
-                [got[c * 8 : c * 8 + 8, :128], got[c * 8 : c * 8 + 8, 128:]], axis=0
-            ).astype(BF16)
+        return (stream_ref[t].astype(F32) + total * r * gain).astype(BF16)
+
+    copies = []
+    for chunk in range(CHUNKS):
+        size = tokens // CHUNKS
+
+        @pl.loop(0, size // 16, unroll=size // 16)
+        def _(g):
+            start = chunk * size + g * 16
+            left = jnp.concatenate([one(start + t) for t in range(8)], axis=0)
+            right = jnp.concatenate([one(start + 8 + t) for t in range(8)], axis=0)
+            got = jnp.dot(gather, jnp.concatenate([left, right], axis=1), preferred_element_type=F32)
+            to = pl.ds(pl.multiple_of(start, 16), 16)
+            for c in range(32):
+                o_ref[to, c * 128 : c * 128 + 128] = jnp.concatenate(
+                    [got[c * 8 : c * 8 + 8, :128], got[c * 8 : c * 8 + 8, 128:]], axis=0
+                ).astype(BF16)
+
+        at = pl.ds(chunk * size, size)
+        copy = pltpu.make_async_copy(o_ref.at[at, :], o_hbm.at[at, :], sem.at[chunk])
+        copy.start()
+        copies.append(copy)
+    for copy in copies:
+        copy.wait()
 
 
 def combine(expert, rank, weight, x, stream, gain):
@@ -334,8 +348,8 @@
         combine_kernel,
         out_shape=jax.ShapeDtypeStruct((tokens, 4096), BF16),
         in_specs=[SMEM, SMEM, SMEM, VMEM, VMEM, VMEM],
-        out_specs=VMEM,
-        scratch_shapes=[pltpu.VMEM((tokens, 32, 128), BF16)],
+        out_specs=pl.BlockSpec(memory_space=pl.ANY),
+        scratch_shapes=[pltpu.VMEM((tokens, 4096), BF16), pltpu.SemaphoreType.DMA((CHUNKS,))],
         compiler_params=pltpu.CompilerParams(vmem_limit_bytes=14 << 20),
         cost_estimate=pl.CostEstimate(flops=10**9, bytes_accessed=6 * 10**6, transcendentals=0),
         name="combine",

time: 188 us -> 187 us (level)
  no operation moved by 1% of the time
where the time goes in v7:
time: 187 us; the launch traced here: 186 us
  blocking collectives  110 us (59%)
  Pallas kernels  28.1 us (15%)
  waiting for transfers between devices  26 us (14%)
  starting transfers between devices  17.5 us (9%)
  local copies, waits for them, and re-layouts  2.71 us (1%)
    all_to_all x1, blocking collectives, layer(): lax.all_to_all(outgoing, ALL, split_axis=0, concat_axis=0, tiled=True)  48.7 us
    all_to_all x1, blocking collectives, layer(): lax.all_to_all(result, ALL, split_axis=0, concat_axis=0, tiled=True)  45.6 us
    ppermute x1, waiting for transfers between devices, layer(): w_first = lax.ppermute(out_weight, DP, onward)  20.9 us
    all_to_all x1, blocking collectives, layer(): lax.all_to_all(attended, 'sp', split_axis=0, concat_axis=0, tiled=True)  16.2 us
    pallas_call x1, Pallas kernels, attend(): pl.pallas_call(attend_kernel, out_shape=jax.ShapeDtypeStruct((blocks, 128...  9.94 us
    all_to_all x1, starting transfers between devices, layer(): lax.all_to_all(packed, 'sp', split_axis=0, concat_axis=0, tiled=True)  7.6 us
    pallas_call x1, Pallas kernels, run_experts(): pl.pallas_call(expert_kernel, out_shape=jax.ShapeDtypeStruct(x.shape, BF1...  6.73 us
    pallas_call x2, Pallas kernels, project(): pl.pallas_call(project_kernel, out_shape=(shape, shape), in_specs=[VMEM,...  5.63 us
  transfers between devices with their start and end apart: 7, of which 4 were waited for; matrix products, arithmetic and copies ran while one was open for 2% of the time, Pallas kernels for 8%

profile of v7, /device:TPU:1, one launch (start us, length us, event | category | flops | bytes accessed | tf_op | source)
XLA Modules:
  0.0 186.5 jit_solution(1292906586959245917)
XLA Ops:
  0.0 3.6 %collective-permute-start.1 = (bf16[2048,512]{1,0:T(8,128)(2,1)}, bf16[2048,512]{1,0:T(8,128)(2,1)}, u32[]{:S(2)}, u32[]{:S(2)}) collective-permute-start(bf16[2048,512]{1,0:T(8,128)(2,1)} %refs_0_.1), channel_id=1, source_target_pairs={{0,2},{1,7},{2,4},{3,1},{4,6},{5,3},{6,0},{7,5},{8,10},{9,15},{10,... | collective-permute-start | bytes 6291464 | tf_op jit(solution)/shard_map/ppermute | solution.py:366
  3.6 1.2 copy.20
  4.7 1.5 copy_bitcast_fusion
  6.2 1.3 pad_maximum_fusion
  7.5 7.6 %all-to-all-start = ((bf16[16,384,128]{2,1,0:T(8,128)(2,1)}), bf16[16,384,128]{2,1,0:T(8,128)(2,1)S(1)}, u32[]{:S(2)}, u32[]{:S(2)}) async-start(bf16[16,384,128]{2,1,0:T(8,128)(2,1)} %pad_maximum_fusion), calls=%async_computation | async-start | bytes 3145728 | tf_op jit(solution)/shard_map/all_to_all | solution.py:376
  15.1 0.1 collective-permute-start.2
  15.2 20.9 %collective-permute-done.1.refs_1_ = bf16[2048,512]{1,0:T(8,128)(2,1)} collective-permute-done((bf16[2048,512]{1,0:T(8,128)(2,1)}, bf16[2048,512]{1,0:T(8,128)(2,1)}, u32[]{:S(2)}, u32[]{:S(2)}) %collective-permute-start.1) | collective-permute-done | bytes 2097184 | tf_op jit(solution)/shard_map/ppermute | solution.py:366
  36.1 3.4 %collective-permute-start.3 = (bf16[2048,512]{1,0:T(8,128)(2,1)}, bf16[2048,512]{1,0:T(8,128)(2,1)}, u32[]{:S(2)}, u32[]{:S(2)}) collective-permute-start(bf16[2048,512]{1,0:T(8,128)(2,1)} %collective-permute-done.1.refs_1_), channel_id=1, source_target_pairs={{0,2},{1,7},{2,4},{3,1},{4,6},{5,3},{6,0},{7,5},{8,10},{9,15},{10,... | collective-permute-start | bytes 6291464 | tf_op jit(solution)/shard_map/ppermute | solution.py:368
  39.5 2.5 %all-to-all-done.x_ref = bf16[16,384,128]{2,1,0:T(8,128)(2,1)S(1)} async-done(((bf16[16,384,128]{2,1,0:T(8,128)(2,1)}), bf16[16,384,128]{2,1,0:T(8,128)(2,1)S(1)}, u32[]{:S(2)}, u32[]{:S(2)}) %all-to-all-start) | async-done | bytes 1572896 | tf_op jit(solution)/shard_map/all_to_all | solution.py:376
  42.0 0.0 copy-start.6
  42.0 9.9 %attend.1 = bf16[16,128,128]{2,1,0:T(8,128)(2,1)S(1)} custom-call(bf16[16,384,128]{2,1,0:T(8,128)(2,1)S(1)} %all-to-all-done.x_ref), custom_call_target="tpu_custom_call" | custom-call | flops 12000000000 | bytes 3000000 | tf_op jit(solution)/shard_map/attend/pallas_call | solution.py:76
  51.9 16.2 %all_to_all.20.own_x_ref = bf16[16,128,128]{2,1,0:T(8,128)(2,1)S(1)} all-to-all(bf16[16,128,128]{2,1,0:T(8,128)(2,1)S(1)} %attend.1), channel_id=1, replica_groups=mesh['sp'=16,'yh'=2,'yl'=2,'c'=2] {'sp'}, dimensions={0} | all-to-all | bytes 1048576 | tf_op jit(solution)/shard_map/all_to_all | solution.py:378
  68.1 2.2 %collective-permute-start = (bf16[16,128,128]{2,1,0:T(8,128)(2,1)S(1)}, bf16[16,128,128]{2,1,0:T(8,128)(2,1)S(1)}, u32[]{:S(2)}, u32[]{:S(2)}) collective-permute-start(bf16[16,128,128]{2,1,0:T(8,128)(2,1)S(1)} %all_to_all.20.own_x_ref), channel_id=1, source_target_pairs={{0,1},{1,0},{2,3},{3,2},{4,5},{5,4},{6,7},{7,6},{8,9},{9,8},{10,11... | collective-permute-start | bytes 1572872 | tf_op jit(solution)/shard_map/ppermute | solution.py:379
  70.3 0.0 collective-permute-done.2.refs_2_
  70.3 1.5 collective-permute-done.other_x_ref
  71.9 0.0 copy-done.6
  71.9 3.2 %shard_map.127 = (f32[3,128,512]{2,1,0:T(8,128)S(1)}, f32[3,128,512]{2,1,0:T(8,128)S(1)}) custom-call(bf16[16,128,128]{2,1,0:T(8,128)(2,1)S(1)} %all_to_all.20.own_x_ref, bf16[16,128,128]{2,1,0:T(8,128)(2,1)S(1)} %collective-permute-done.other_x_ref, bf16[2048,512]{1,0:T(8,128)(2,1)S(1)} %copy-done.6, bf16[2048,512]{1,0:T(8,128)(2,1)} %collective-permute-done.1.refs_1_, ...), custom_call_target="tpu_custom_call" | custom-call | flops 3000000000 | bytes 9000000 | tf_op jit(solution)/shard_map/pallas_call | solution.py:157
  75.1 0.0 copy-start.1
  75.1 0.0 copy-start.7
  75.1 0.0 copy-start.8
  75.1 0.0 copy-start.9
  75.1 0.5 collective-permute-start.4
  75.6 0.0 collective-permute-done.3.refs_0_
  75.6 0.0 copy-start.5
  75.6 2.5 %shard_map.128 = (f32[1,128,512]{2,1,0:T(8,128)S(1)}, f32[1,128,512]{2,1,0:T(8,128)S(1)}) custom-call(bf16[16,128,128]{2,1,0:T(8,128)(2,1)S(1)} %all_to_all.20.own_x_ref, bf16[16,128,128]{2,1,0:T(8,128)(2,1)S(1)} %collective-permute-done.other_x_ref, bf16[2048,512]{1,0:T(8,128)(2,1)} %collective-permute-done.3.refs_0_), custom_call_target="tpu_custom_call" | custom-call | flops 1000000000 | bytes 3000000 | tf_op jit(solution)/shard_map/pallas_call | solution.py:157
  78.0 0.2 collective-permute-start.5
  78.2 0.0 copy-done.1
  78.3 0.3 route.1
  78.5 0.0 collective-permute-done.4.got_ref
  78.5 1.1 collective-permute-done.5.got_far_ref
  79.6 0.0 copy-done.7
  79.7 0.0 copy-done.8
  79.7 0.0 copy-done.9
  79.7 0.0 copy-start.4
  79.7 2.9 %mix.1 = (bf16[128,32,128]{2,1,0:T(8,128)(2,1)S(1)}, bf16[128,96,128]{2,1,0:T(8,128)(2,1)S(1)}) custom-call(s32[8,128]{1,0:T(8,128)S(1)} %get-tuple-element.14.slot_ref, f32[3,128,512]{2,1,0:T(8,128)S(1)} %get-tuple-element.15.own_ref, f32[1,128,512]{2,1,0:T(8,128)S(1)} %get-tuple-element.16.own_far_ref, f32[3,128,512]{2,1,0:T(8,128)S(1)} %collective-permute-done.4.got_ref, ...), custom_call_target="tpu_custom_call" | custom-call | flops 1000000000 | bytes 8000000 | tf_op jit(solution)/shard_map/mix/pallas_call | solution.py:224
  82.6 0.0 copy-start.3
  82.6 48.7 %all_to_all.21.x_ref = bf16[128,96,128]{2,1,0:T(8,128)(2,1)S(1)} all-to-all(bf16[128,96,128]{2,1,0:T(8,128)(2,1)S(1)} %get-tuple-element.19), channel_id=1, replica_groups=mesh['sp'=16,'yh'=2,'yl'=2,'c'=2] {'sp','yh','yl','c'}, dimensions={0} | all-to-all | bytes 6291456 | tf_op jit(solution)/shard_map/all_to_all | solution.py:388
  131.3 0.0 copy-done.5
  131.3 0.0 copy-done.4
  131.3 0.0 copy-done.3
  131.3 6.7 %experts.1 = bf16[128,96,128]{2,1,0:T(8,128)(2,1)S(1)} custom-call(bf16[128,96,128]{2,1,0:T(8,128)(2,1)S(1)} %all_to_all.21.x_ref, bf16[4096,512]{1,0:T(8,128)(2,1)S(1)} %bitcast.31, bf16[4096,512]{1,0:T(8,128)(2,1)S(1)} %bitcast.32, bf16[512,4096]{1,0:T(8,128)(2,1)S(1)} %bitcast.33), custom_call_target="tpu_custom_call" | custom-call | flops 6000000000 | bytes 19000000 | tf_op jit(solution)/shard_map/experts/pallas_call | solution.py:288
  138.0 0.0 copy-start
  138.0 0.0 copy-start.2
  138.0 45.6 %all_to_all.22.x_ref = bf16[128,96,128]{2,1,0:T(8,128)(2,1)S(1)} all-to-all(bf16[128,96,128]{2,1,0:T(8,128)(2,1)S(1)} %experts.1), channel_id=1, replica_groups=mesh['sp'=16,'yh'=2,'yl'=2,'c'=2] {'sp','yh','yl','c'}, dimensions={0} | all-to-all | bytes 6291456 | tf_op jit(solution)/shard_map/all_to_all | solution.py:390
  183.7 0.0 copy-done
  183.7 0.0 copy-done.2
  183.7 2.6 %combine.1 = bf16[128,4096]{1,0:T(8,128)(2,1)} custom-call(s32[2,128]{1,0:T(2,128)S(1)} %bitcast.29, s32[2,128]{1,0:T(2,128)S(1)} %get-tuple-element.13.rank_ref, f32[2,128]{1,0:T(2,128)S(1)} %bitcast.30, bf16[128,96,128]{2,1,0:T(8,128)(2,1)S(1)} %all_to_all.22.x_ref, bf16[128,32,128]{2,1,0:T(8,128)(2,1)S(1)} %get-tuple-element.20.stream_ref, ...), custom_call_target="tpu_custom_call" | custom-call | flops 1000000000 | bytes 6000000 | tf_op jit(solution)/shard_map/combine/pallas_call | solution.py:347
Async XLA Ops:
  0.0 36.1 %collective-permute-start.1 = (bf16[2048,512]{1,0:T(8,128)(2,1)}, bf16[2048,512]{1,0:T(8,128)(2,1)}, u32[]{:S(2)}, u32[]{:S(2)}) collective-permute-start(bf16[2048,512]{1,0:T(8,128)(2,1)} %refs_0_.1), channel_id=1, source_target_pairs={{0,2},{1,7},{2,4},{3,1},{4,6},{5,3},{6,0},{7,5},{8,10},{9,15},{10,... | collective-permute-start | bytes 6291464 | tf_op jit(solution)/shard_map/ppermute | solution.py:366
  7.5 34.5 %all-to-all-start = ((bf16[16,384,128]{2,1,0:T(8,128)(2,1)}), bf16[16,384,128]{2,1,0:T(8,128)(2,1)S(1)}, u32[]{:S(2)}, u32[]{:S(2)}) async-start(bf16[16,384,128]{2,1,0:T(8,128)(2,1)} %pad_maximum_fusion), calls=%async_computation | async-start | bytes 3145728 | tf_op jit(solution)/shard_map/all_to_all | solution.py:376
  15.1 55.3 %collective-permute-start.2 = (bf16[2048,512]{1,0:T(8,128)(2,1)}, bf16[2048,512]{1,0:T(8,128)(2,1)}, u32[]{:S(2)}, u32[]{:S(2)}) collective-permute-start(bf16[2048,512]{1,0:T(8,128)(2,1)} %refs_0_.1), channel_id=1, source_target_pairs={{0,6},{1,3},{2,0},{3,5},{4,2},{5,7},{6,4},{7,1},{8,14},{9,11},{10,... | collective-permute-start | bytes 6291464 | tf_op jit(solution)/shard_map/ppermute | solution.py:367
  36.1 39.5 %collective-permute-start.3 = (bf16[2048,512]{1,0:T(8,128)(2,1)}, bf16[2048,512]{1,0:T(8,128)(2,1)}, u32[]{:S(2)}, u32[]{:S(2)}) collective-permute-start(bf16[2048,512]{1,0:T(8,128)(2,1)} %collective-permute-done.1.refs_1_), channel_id=1, source_target_pairs={{0,2},{1,7},{2,4},{3,1},{4,6},{5,3},{6,0},{7,5},{8,10},{9,15},{10,... | collective-permute-start | bytes 6291464 | tf_op jit(solution)/shard_map/ppermute | solution.py:368
  42.0 29.9 %copy-start.6 = (bf16[2048,512]{1,0:T(8,128)(2,1)S(1)}, bf16[2048,512]{1,0:T(8,128)(2,1)}, u32[]{:S(2)}) copy-start(bf16[2048,512]{1,0:T(8,128)(2,1)} %refs_0_.1) | copy-start | bytes 6291460
  68.1 3.8 %collective-permute-start = (bf16[16,128,128]{2,1,0:T(8,128)(2,1)S(1)}, bf16[16,128,128]{2,1,0:T(8,128)(2,1)S(1)}, u32[]{:S(2)}, u32[]{:S(2)}) collective-permute-start(bf16[16,128,128]{2,1,0:T(8,128)(2,1)S(1)} %all_to_all.20.own_x_ref), channel_id=1, source_target_pairs={{0,1},{1,0},{2,3},{3,2},{4,5},{5,4},{6,7},{7,6},{8,9},{9,8},{10,11... | collective-permute-start | bytes 1572872 | tf_op jit(solution)/shard_map/ppermute | solution.py:379
  75.1 3.2 %copy-start.1 = (s32[1,128,2]{1,2,0:T(2,128)S(1)}, s32[1,128,2]{1,2,0:T(2,128)}, u32[]{:S(2)}) copy-start(s32[1,128,2]{1,2,0:T(2,128)} %param.23) | copy-start | bytes 3076
  75.1 4.6 %copy-start.7 = (bf16[1,128,4096]{2,1,0:T(8,128)(2,1)S(1)}, bf16[1,128,4096]{2,1,0:T(8,128)(2,1)}, u32[]{:S(2)}) copy-start(bf16[1,128,4096]{2,1,0:T(8,128)(2,1)} %param.16) | copy-start | bytes 3145732
  75.1 4.6 %copy-start.8 = (f32[4096]{0:T(1024)S(1)}, f32[4096]{0:T(1024)}, u32[]{:S(2)}) copy-start(f32[4096]{0:T(1024)} %param.18) | copy-start | bytes 49156
  75.1 4.6 %copy-start.9 = (f32[4096]{0:T(1024)S(1)}, f32[4096]{0:T(1024)}, u32[]{:S(2)}) copy-start(f32[4096]{0:T(1024)} %param.19) | copy-start | bytes 49156
  75.1 3.4 %collective-permute-start.4 = (f32[3,128,512]{2,1,0:T(8,128)S(1)}, f32[3,128,512]{2,1,0:T(8,128)S(1)}, u32[]{:S(2)}, u32[]{:S(2)}) collective-permute-start(f32[3,128,512]{2,1,0:T(8,128)S(1)} %get-tuple-element.17), channel_id=1, source_target_pairs={{0,1},{1,0},{2,3},{3,2},{4,5},{5,4},{6,7},{7,6},{8,9},{9,8},{10,11... | collective-permute-start | bytes 2359304 | tf_op jit(solution)/shard_map/ppermute | solution.py:381
  75.6 55.7 %copy-start.5 = (bf16[1,512,4096]{2,1,0:T(8,128)(2,1)S(1)}, bf16[1,512,4096]{2,1,0:T(8,128)(2,1)}, u32[]{:S(2)}) copy-start(bf16[1,512,4096]{2,1,0:T(8,128)(2,1)} %param.22) | copy-start | bytes 12582916
  78.0 1.6 collective-permute-start.5
  79.7 51.6 %copy-start.4 = (bf16[1,4096,512]{2,1,0:T(8,128)(2,1)S(1)}, bf16[1,4096,512]{2,1,0:T(8,128)(2,1)}, u32[]{:S(2)}) copy-start(bf16[1,4096,512]{2,1,0:T(8,128)(2,1)} %param.21) | copy-start | bytes 12582916
  82.6 48.7 %copy-start.3 = (bf16[1,4096,512]{2,1,0:T(8,128)(2,1)S(1)}, bf16[1,4096,512]{2,1,0:T(8,128)(2,1)}, u32[]{:S(2)}) copy-start(bf16[1,4096,512]{2,1,0:T(8,128)(2,1)} %param.20) | copy-start | bytes 12582916
  138.0 45.7 %copy-start = (f32[4096]{0:T(1024)S(1)}, f32[4096]{0:T(1024)}, u32[]{:S(2)}) copy-start(f32[4096]{0:T(1024)} %param.25) | copy-start | bytes 49156
  138.0 45.6 %copy-start.2 = (f32[1,128,2]{1,2,0:T(2,128)S(1)}, f32[1,128,2]{1,2,0:T(2,128)}, u32[]{:S(2)}) copy-start(f32[1,128,2]{1,2,0:T(2,128)} %param.24) | copy-start | bytes 3076

commit v8 on v7

--- a/solution.py
+++ b/solution.py
@@ -1,3 +1,4 @@
+import functools
 import math
 
 import jax
@@ -131,10 +132,11 @@
     )(picks)
 
 
-def project_kernel(own_x_ref, other_x_ref, *refs):
+def project_kernel(own_x_ref, other_x_ref, *refs, first_rows):
     *weights, own_ref, other_ref, w_ref, sem = refs
     copies = [
-        pltpu.make_async_copy(ref, w_ref.at[k], sem.at[k]) for k, ref in enumerate(weights)
+        pltpu.make_async_copy(ref, w_ref.at[k, pl.ds(0, ref.shape[0]), :], sem.at[k])
+        for k, ref in enumerate(weights)
     ]
     for copy in copies:
         copy.start()
@@ -145,22 +147,27 @@
     both = jnp.concatenate(rows, axis=0)
     for k, copy in enumerate(copies):
         copy.wait()
+        depth = weights[k].shape[0]
+        start = 0 if first_rows is None else first_rows
         for n in range(0, 512, 256):
-            out = jnp.dot(both, w_ref[k, :, n : n + 256], preferred_element_type=F32)
+            out = jnp.dot(
+                both[:, start : start + depth], w_ref[k, :depth, n : n + 256],
+                preferred_element_type=F32,
+            )
             own_ref[k, :, n : n + 256] = out[:128]
             other_ref[k, :, n : n + 256] = out[128:]
 
 
-def project(own_x, other_x, weights):
+def project(own_x, other_x, weights, first_rows=None):
     count = len(weights)
     shape = jax.ShapeDtypeStruct((count, 128, 512), F32)
     return pl.pallas_call(
-        project_kernel,
+        functools.partial(project_kernel, first_rows=first_rows),
         out_shape=(shape, shape),
         in_specs=[VMEM, VMEM] + [ANY] * count,
         out_specs=(VMEM, VMEM),
         scratch_shapes=[
-            pltpu.VMEM((count, 2048, 512), BF16),
+            pltpu.VMEM((count, max(w.shape[0] for w in weights), 512), BF16),
             pltpu.SemaphoreType.DMA((count,)),
         ],
         compiler_params=pltpu.CompilerParams(vmem_limit_bytes=(5 + 3 * count) << 20),
@@ -188,9 +195,9 @@
 ):
     chip, core = lax.axis_index("yh") * 2 + lax.axis_index("yl"), lax.axis_index("c")
     for member, near, far in ((core, own_ref, own_far_ref), (1 - core, got_ref, got_far_ref)):
-        for k, step in enumerate((0, 3 - 2 * member, 1 + 2 * member, 2)):
+        for k, step in enumerate((0, 3 - 2 * member, 2, 1 + 2 * member)):
             at = lax.rem(chip + step, 4) * 1024 + member * 512
-            block = near[k] if k < 3 else far[0]
+            block = near[k] if k < 3 else near[k] + far[0]
             proj_ref[:, pl.ds(pl.multiple_of(at, 512), 512)] = block
     spread = to_rows(32, 8)
     width = proj_ref.shape[1]
@@ -364,8 +371,10 @@
     back = [(d, (d + (6, 2)[d % 2]) % 8) for d in range(8)]
     swap = [(0, 1), (1, 0)]
     w_first = lax.ppermute(out_weight, DP, onward)
-    w_second = lax.ppermute(out_weight, DP, back)
     w_far = lax.ppermute(w_first, DP, onward)
+    half = out_weight.shape[0] // 2
+    w_second = lax.ppermute(out_weight[:half], DP, back)
+    w_last = lax.ppermute(out_weight[half:], DP, back)
 
     picks = jnp.transpose(routes[0])
     rank, slots = route(picks)
@@ -377,9 +386,9 @@
     attended = attend(by_head)
     own_x = lax.all_to_all(attended, "sp", split_axis=0, concat_axis=0, tiled=True)
     other_x = lax.ppermute(own_x, "c", swap)
-    own, other = project(own_x, other_x, (out_weight, w_first, w_second))
+    own, other = project(own_x, other_x, (out_weight, w_first, w_far, w_second))
     got = lax.ppermute(other, "c", swap)
-    own_far, other_far = project(own_x, other_x, (w_far,))
+    own_far, other_far = project(own_x, other_x, (w_last,), half)
     got_far = lax.ppermute(other_far, "c", swap)
     stream, outgoing = mix(
         slots, (own, own_far, got, got_far), residual[0], mixer_gain.reshape(1, -1),

time: 187 us -> 192 us (1.027)
  waiting for transfers between devices: 26 us -> 33 us
  blocking collectives: 110 us -> 106 us
    ppermute x1 -> x2, waiting for transfers between devices: 0.01 us -> 9.2 us  [the longest x1 9.2 us: layer(): w_last = lax.ppermute(out_weight[half:], DP, back)]
    ppermute x1, waiting for transfers between devices: 20.9 us -> 17.8 us  [layer(): w_first = lax.ppermute(out_weight, DP, onward)]
    all_to_all x1, blocking collectives: 48.7 us -> 46.1 us  [layer(): lax.all_to_all(outgoing, ALL, split_axis=0, concat_axis=0, tiled=True)]
  transfers between devices with their start and end apart: 7 -> 8, of which waited for: 4 -> 5; matrix products, arithmetic and copies ran while one was open for 2% -> 3% of each run, Pallas kernels for 8% -> 8%
where the time goes in v8:
time: 192 us; the launch traced here: 191 us
  blocking collectives  106 us (55%)
  waiting for transfers between devices  33 us (17%)
  Pallas kernels  28.1 us (15%)
  starting transfers between devices  18.1 us (9%)
  local copies, waits for them, and re-layouts  4.26 us (2%)
    all_to_all x1, blocking collectives, layer(): lax.all_to_all(outgoing, ALL, split_axis=0, concat_axis=0, tiled=True)  46.1 us
    all_to_all x1, blocking collectives, layer(): lax.all_to_all(result, ALL, split_axis=0, concat_axis=0, tiled=True)  45.6 us
    ppermute x1, waiting for transfers between devices, layer(): w_first = lax.ppermute(out_weight, DP, onward)  17.8 us
    all_to_all x1, blocking collectives, layer(): lax.all_to_all(attended, 'sp', split_axis=0, concat_axis=0, tiled=True)  14.6 us
    pallas_call x1, Pallas kernels, attend(): pl.pallas_call(attend_kernel, out_shape=jax.ShapeDtypeStruct((blocks, 128...  11.4 us
    ppermute x1, waiting for transfers between devices, layer(): w_last = lax.ppermute(out_weight[half:], DP, back)  9.2 us
    all_to_all x1, starting transfers between devices, layer(): lax.all_to_all(packed, 'sp', split_axis=0, concat_axis=0, tiled=True)  7.64 us
    pallas_call x1, Pallas kernels, run_experts(): pl.pallas_call(expert_kernel, out_shape=jax.ShapeDtypeStruct(x.shape, BF1...  6.74 us
  transfers between devices with their start and end apart: 8, of which 5 were waited for; matrix products, arithmetic and copies ran while one was open for 3% of the time, Pallas kernels for 8%

profile of v8, /device:TPU:1, one launch (start us, length us, event | category | flops | bytes accessed | tf_op | source)
XLA Modules:
  0.0 191.4 jit_solution(2818027788307648355)
XLA Ops:
  0.0 3.6 %collective-permute-start.1 = (bf16[2048,512]{1,0:T(8,128)(2,1)}, bf16[2048,512]{1,0:T(8,128)(2,1)}, u32[]{:S(2)}, u32[]{:S(2)}) collective-permute-start(bf16[2048,512]{1,0:T(8,128)(2,1)} %refs_0_.1), channel_id=1, source_target_pairs={{0,2},{1,7},{2,4},{3,1},{4,6},{5,3},{6,0},{7,5},{8,10},{9,15},{10,... | collective-permute-start | bytes 6291464 | tf_op jit(solution)/shard_map/ppermute | solution.py:373
  3.6 1.2 copy.20
  4.7 1.5 copy_bitcast_fusion
  6.2 0.0 copy-start
  6.2 1.3 pad_maximum_fusion
  7.5 7.6 %all-to-all-start = ((bf16[16,384,128]{2,1,0:T(8,128)(2,1)}), bf16[16,384,128]{2,1,0:T(8,128)(2,1)}, u32[]{:S(2)}, u32[]{:S(2)}) async-start(bf16[16,384,128]{2,1,0:T(8,128)(2,1)} %pad_maximum_fusion), calls=%async_computation | async-start | bytes 3145728 | tf_op jit(solution)/shard_map/all_to_all | solution.py:385
  15.1 0.0 copy-done
  15.1 1.5 fusion
  16.7 0.0 collective-permute-start.3
  16.7 17.8 %collective-permute-done.1.refs_1_ = bf16[2048,512]{1,0:T(8,128)(2,1)} collective-permute-done((bf16[2048,512]{1,0:T(8,128)(2,1)}, bf16[2048,512]{1,0:T(8,128)(2,1)}, u32[]{:S(2)}, u32[]{:S(2)}) %collective-permute-start.1) | collective-permute-done | bytes 2097184 | tf_op jit(solution)/shard_map/ppermute | solution.py:373
  34.5 3.3 %collective-permute-start.2 = (bf16[2048,512]{1,0:T(8,128)(2,1)}, bf16[2048,512]{1,0:T(8,128)(2,1)}, u32[]{:S(2)}, u32[]{:S(2)}) collective-permute-start(bf16[2048,512]{1,0:T(8,128)(2,1)} %collective-permute-done.1.refs_1_), channel_id=1, source_target_pairs={{0,2},{1,7},{2,4},{3,1},{4,6},{5,3},{6,0},{7,5},{8,10},{9,15},{10,... | collective-permute-start | bytes 6291464 | tf_op jit(solution)/shard_map/ppermute | solution.py:374
  37.8 4.3 %all-to-all-done.x_ref = bf16[16,384,128]{2,1,0:T(8,128)(2,1)} async-done(((bf16[16,384,128]{2,1,0:T(8,128)(2,1)}), bf16[16,384,128]{2,1,0:T(8,128)(2,1)}, u32[]{:S(2)}, u32[]{:S(2)}) %all-to-all-start) | async-done | bytes 1572896 | tf_op jit(solution)/shard_map/all_to_all | solution.py:385
  42.1 11.4 %attend.1 = bf16[16,128,128]{2,1,0:T(8,128)(2,1)S(1)} custom-call(bf16[16,384,128]{2,1,0:T(8,128)(2,1)} %all-to-all-done.x_ref), custom_call_target="tpu_custom_call" | custom-call | flops 12000000000 | bytes 3000000 | tf_op jit(solution)/shard_map/attend/pallas_call | solution.py:77
  53.5 14.6 %all_to_all.20.own_x_ref = bf16[16,128,128]{2,1,0:T(8,128)(2,1)S(1)} all-to-all(bf16[16,128,128]{2,1,0:T(8,128)(2,1)S(1)} %attend.1), channel_id=1, replica_groups=mesh['sp'=16,'yh'=2,'yl'=2,'c'=2] {'sp'}, dimensions={0} | all-to-all | bytes 1048576 | tf_op jit(solution)/shard_map/all_to_all | solution.py:387
  68.2 2.0 %collective-permute-start = (bf16[16,128,128]{2,1,0:T(8,128)(2,1)S(1)}, bf16[16,128,128]{2,1,0:T(8,128)(2,1)S(1)}, u32[]{:S(2)}, u32[]{:S(2)}) collective-permute-start(bf16[16,128,128]{2,1,0:T(8,128)(2,1)S(1)} %all_to_all.20.own_x_ref), channel_id=1, source_target_pairs={{0,1},{1,0},{2,3},{3,2},{4,5},{5,4},{6,7},{7,6},{8,9},{9,8},{10,11... | collective-permute-start | bytes 1572872 | tf_op jit(solution)/shard_map/ppermute | solution.py:388
  70.2 0.0 copy-done.10
  70.2 1.0 collective-permute-start.4
  71.2 0.0 collective-permute-done.3.refs_3_
  71.2 0.5 collective-permute-done.other_x_ref
  71.7 0.0 collective-permute-done.2.refs_2_
  71.7 3.6 %shard_map.127 = (f32[4,128,512]{2,1,0:T(8,128)S(1)}, f32[4,128,512]{2,1,0:T(8,128)S(1)}) custom-call(bf16[16,128,128]{2,1,0:T(8,128)(2,1)S(1)} %all_to_all.20.own_x_ref, bf16[16,128,128]{2,1,0:T(8,128)(2,1)S(1)} %collective-permute-done.other_x_ref, bf16[2048,512]{1,0:T(8,128)(2,1)S(1)} %copy-done, bf16[2048,512]{1,0:T(8,128)(2,1)} %collective-permute-done.1.refs_1_, ...), custom_call_target="tpu_custom_call" | custom-call | flops 4000000000 | bytes 12000000 | tf_op jit(solution)/shard_map/pallas_call | solution.py:164
  75.3 0.0 copy-start.5
  75.3 0.0 copy-start.1
  75.4 0.0 copy-start.2
  75.4 0.0 copy-start.3
  75.4 0.5 collective-permute-start.5
  75.8 9.2 %collective-permute-done.4.refs_0_ = bf16[1024,512]{1,0:T(8,128)(2,1)S(1)} collective-permute-done((bf16[1024,512]{1,0:T(8,128)(2,1)S(1)}, bf16[1024,512]{1,0:T(8,128)(2,1)S(1)}, u32[]{:S(2)}, u32[]{:S(2)}) %collective-permute-start.4) | collective-permute-done | bytes 1048608 | tf_op jit(solution)/shard_map/ppermute | solution.py:377
  85.0 0.5 shard_map.128
  85.6 0.1 collective-permute-start.6
  85.7 0.0 copy-done.5
  85.7 0.3 route.1
  86.0 1.2 collective-permute-done.6.got_far_ref
  87.2 0.0 collective-permute-done.5.got_ref
  87.2 0.0 copy-done.1
  87.2 0.0 copy-done.2
  87.2 0.0 copy-done.3
  87.2 0.0 copy-start.8
  87.2 2.8 %mix.1 = (bf16[128,32,128]{2,1,0:T(8,128)(2,1)S(1)}, bf16[128,96,128]{2,1,0:T(8,128)(2,1)S(1)}) custom-call(s32[8,128]{1,0:T(8,128)S(1)} %get-tuple-element.14.slot_ref, f32[4,128,512]{2,1,0:T(8,128)S(1)} %get-tuple-element.15.own_ref, f32[1,128,512]{2,1,0:T(8,128)S(1)} %get-tuple-element.16.own_far_ref, f32[4,128,512]{2,1,0:T(8,128)S(1)} %collective-permute-done.5.got_ref, ...), custom_call_target="tpu_custom_call" | custom-call | flops 1000000000 | bytes 8000000 | tf_op jit(solution)/shard_map/mix/pallas_call | solution.py:231
  90.1 0.0 copy-start.7
  90.1 46.1 %all_to_all.21.x_ref = bf16[128,96,128]{2,1,0:T(8,128)(2,1)S(1)} all-to-all(bf16[128,96,128]{2,1,0:T(8,128)(2,1)S(1)} %get-tuple-element.19), channel_id=1, replica_groups=mesh['sp'=16,'yh'=2,'yl'=2,'c'=2] {'sp','yh','yl','c'}, dimensions={0} | all-to-all | bytes 6291456 | tf_op jit(solution)/shard_map/all_to_all | solution.py:397
  136.2 0.0 copy-done.9
  136.2 0.0 copy-done.8
  136.2 0.0 copy-done.7
  136.2 6.7 %experts.1 = bf16[128,96,128]{2,1,0:T(8,128)(2,1)S(1)} custom-call(bf16[128,96,128]{2,1,0:T(8,128)(2,1)S(1)} %all_to_all.21.x_ref, bf16[4096,512]{1,0:T(8,128)(2,1)S(1)} %bitcast.34, bf16[4096,512]{1,0:T(8,128)(2,1)S(1)} %bitcast.35, bf16[512,4096]{1,0:T(8,128)(2,1)S(1)} %bitcast.36), custom_call_target="tpu_custom_call" | custom-call | flops 6000000000 | bytes 19000000 | tf_op jit(solution)/shard_map/experts/pallas_call | solution.py:295
  143.0 0.0 copy-start.4
  143.0 0.0 copy-start.6
  143.0 45.6 %all_to_all.22.x_ref = bf16[128,96,128]{2,1,0:T(8,128)(2,1)S(1)} all-to-all(bf16[128,96,128]{2,1,0:T(8,128)(2,1)S(1)} %experts.1), channel_id=1, replica_groups=mesh['sp'=16,'yh'=2,'yl'=2,'c'=2] {'sp','yh','yl','c'}, dimensions={0} | all-to-all | bytes 6291456 | tf_op jit(solution)/shard_map/all_to_all | solution.py:399
  188.6 2.6 %combine.1 = bf16[128,4096]{1,0:T(8,128)(2,1)} custom-call(s32[2,128]{1,0:T(2,128)S(1)} %bitcast.32, s32[2,128]{1,0:T(2,128)S(1)} %get-tuple-element.13.rank_ref, f32[2,128]{1,0:T(2,128)S(1)} %bitcast.33, bf16[128,96,128]{2,1,0:T(8,128)(2,1)S(1)} %all_to_all.22.x_ref, bf16[128,32,128]{2,1,0:T(8,128)(2,1)S(1)} %get-tuple-element.20.stream_ref, ...), custom_call_target="tpu_custom_call" | custom-call | flops 1000000000 | bytes 6000000 | tf_op jit(solution)/shard_map/combine/pallas_call | solution.py:354
  (4 shorter events, 0.0 us)
Async XLA Ops:
  0.0 34.5 %collective-permute-start.1 = (bf16[2048,512]{1,0:T(8,128)(2,1)}, bf16[2048,512]{1,0:T(8,128)(2,1)}, u32[]{:S(2)}, u32[]{:S(2)}) collective-permute-start(bf16[2048,512]{1,0:T(8,128)(2,1)} %refs_0_.1), channel_id=1, source_target_pairs={{0,2},{1,7},{2,4},{3,1},{4,6},{5,3},{6,0},{7,5},{8,10},{9,15},{10,... | collective-permute-start | bytes 6291464 | tf_op jit(solution)/shard_map/ppermute | solution.py:373
  6.2 8.9 %copy-start = (bf16[2048,512]{1,0:T(8,128)(2,1)S(1)}, bf16[2048,512]{1,0:T(8,128)(2,1)}, u32[]{:S(2)}) copy-start(bf16[2048,512]{1,0:T(8,128)(2,1)} %refs_0_.1) | copy-start | bytes 6291460
  7.5 34.6 %all-to-all-start = ((bf16[16,384,128]{2,1,0:T(8,128)(2,1)}), bf16[16,384,128]{2,1,0:T(8,128)(2,1)}, u32[]{:S(2)}, u32[]{:S(2)}) async-start(bf16[16,384,128]{2,1,0:T(8,128)(2,1)} %pad_maximum_fusion), calls=%async_computation | async-start | bytes 3145728 | tf_op jit(solution)/shard_map/all_to_all | solution.py:385
  16.7 54.5 %collective-permute-start.3 = (bf16[1024,512]{1,0:T(8,128)(2,1)}, bf16[1024,512]{1,0:T(8,128)(2,1)S(1)}, u32[]{:S(2)}, u32[]{:S(2)}) collective-permute-start(bf16[1024,512]{1,0:T(8,128)(2,1)} %get-tuple-element.22), channel_id=1, source_target_pairs={{0,6},{1,3},{2,0},{3,5},{4,2},{5,7},{6,4},{7,1},{8,14},{9,11},{10,... | collective-permute-start | bytes 3145736 | tf_op jit(solution)/shard_map/ppermute | solution.py:376
  34.5 37.2 %collective-permute-start.2 = (bf16[2048,512]{1,0:T(8,128)(2,1)}, bf16[2048,512]{1,0:T(8,128)(2,1)}, u32[]{:S(2)}, u32[]{:S(2)}) collective-permute-start(bf16[2048,512]{1,0:T(8,128)(2,1)} %collective-permute-done.1.refs_1_), channel_id=1, source_target_pairs={{0,2},{1,7},{2,4},{3,1},{4,6},{5,3},{6,0},{7,5},{8,10},{9,15},{10,... | collective-permute-start | bytes 6291464 | tf_op jit(solution)/shard_map/ppermute | solution.py:374
  42.1 28.1 %copy-start.10 = (bf16[1024,512]{1,0:T(8,128)(2,1)S(1)}, bf16[1024,512]{1,0:T(8,128)(2,1)}, u32[]{:S(2)}) copy-start(bf16[1024,512]{1,0:T(8,128)(2,1)} %get-tuple-element.21) | copy-start | bytes 3145732
  68.2 3.5 %collective-permute-start = (bf16[16,128,128]{2,1,0:T(8,128)(2,1)S(1)}, bf16[16,128,128]{2,1,0:T(8,128)(2,1)S(1)}, u32[]{:S(2)}, u32[]{:S(2)}) collective-permute-start(bf16[16,128,128]{2,1,0:T(8,128)(2,1)S(1)} %all_to_all.20.own_x_ref), channel_id=1, source_target_pairs={{0,1},{1,0},{2,3},{3,2},{4,5},{5,4},{6,7},{7,6},{8,9},{9,8},{10,11... | collective-permute-start | bytes 1572872 | tf_op jit(solution)/shard_map/ppermute | solution.py:388
  70.2 14.9 %collective-permute-start.4 = (bf16[1024,512]{1,0:T(8,128)(2,1)S(1)}, bf16[1024,512]{1,0:T(8,128)(2,1)S(1)}, u32[]{:S(2)}, u32[]{:S(2)}) collective-permute-start(bf16[1024,512]{1,0:T(8,128)(2,1)S(1)} %copy-done.10), channel_id=1, source_target_pairs={{0,6},{1,3},{2,0},{3,5},{4,2},{5,7},{6,4},{7,1},{8,14},{9,11},{10,... | collective-permute-start | bytes 3145736 | tf_op jit(solution)/shard_map/ppermute | solution.py:377
  75.3 10.3 %copy-start.5 = (s32[1,128,2]{1,2,0:T(2,128)S(1)}, s32[1,128,2]{1,2,0:T(2,128)}, u32[]{:S(2)}) copy-start(s32[1,128,2]{1,2,0:T(2,128)} %param.23) | copy-start | bytes 3076
  75.3 11.9 %copy-start.1 = (bf16[1,128,4096]{2,1,0:T(8,128)(2,1)S(1)}, bf16[1,128,4096]{2,1,0:T(8,128)(2,1)}, u32[]{:S(2)}) copy-start(bf16[1,128,4096]{2,1,0:T(8,128)(2,1)} %param.16) | copy-start | bytes 3145732
  75.4 11.9 %copy-start.2 = (f32[4096]{0:T(1024)S(1)}, f32[4096]{0:T(1024)}, u32[]{:S(2)}) copy-start(f32[4096]{0:T(1024)} %param.18) | copy-start | bytes 49156
  75.4 11.8 %copy-start.3 = (f32[4096]{0:T(1024)S(1)}, f32[4096]{0:T(1024)}, u32[]{:S(2)}) copy-start(f32[4096]{0:T(1024)} %param.19) | copy-start | bytes 49156
  75.4 11.8 %collective-permute-start.5 = (f32[4,128,512]{2,1,0:T(8,128)S(1)}, f32[4,128,512]{2,1,0:T(8,128)S(1)}, u32[]{:S(2)}, u32[]{:S(2)}) collective-permute-start(f32[4,128,512]{2,1,0:T(8,128)S(1)} %get-tuple-element.17), channel_id=1, source_target_pairs={{0,1},{1,0},{2,3},{3,2},{4,5},{5,4},{6,7},{7,6},{8,9},{9,8},{10,11... | collective-permute-start | bytes 3145736 | tf_op jit(solution)/shard_map/ppermute | solution.py:390
  85.0 51.2 %copy-start.9 = (bf16[1,512,4096]{2,1,0:T(8,128)(2,1)S(1)}, bf16[1,512,4096]{2,1,0:T(8,128)(2,1)}, u32[]{:S(2)}) copy-start(bf16[1,512,4096]{2,1,0:T(8,128)(2,1)} %param.22) | copy-start | bytes 12582916
  85.6 1.6 collective-permute-start.6
  87.2 49.0 %copy-start.8 = (bf16[1,4096,512]{2,1,0:T(8,128)(2,1)S(1)}, bf16[1,4096,512]{2,1,0:T(8,128)(2,1)}, u32[]{:S(2)}) copy-start(bf16[1,4096,512]{2,1,0:T(8,128)(2,1)} %param.21) | copy-start | bytes 12582916
  90.1 46.1 %copy-start.7 = (bf16[1,4096,512]{2,1,0:T(8,128)(2,1)S(1)}, bf16[1,4096,512]{2,1,0:T(8,128)(2,1)}, u32[]{:S(2)}) copy-start(bf16[1,4096,512]{2,1,0:T(8,128)(2,1)} %param.20) | copy-start | bytes 12582916
  143.0 45.7 %copy-start.4 = (f32[4096]{0:T(1024)S(1)}, f32[4096]{0:T(1024)}, u32[]{:S(2)}) copy-start(f32[4096]{0:T(1024)} %param.25) | copy-start | bytes 49156
  143.0 45.6 %copy-start.6 = (f32[1,128,2]{1,2,0:T(2,128)S(1)}, f32[1,128,2]{1,2,0:T(2,128)}, u32[]{:S(2)}) copy-start(f32[1,128,2]{1,2,0:T(2,128)} %param.24) | copy-start | bytes 3076

commit v9 on v8

--- a/solution.py
+++ b/solution.py
@@ -195,7 +195,7 @@
 ):
     chip, core = lax.axis_index("yh") * 2 + lax.axis_index("yl"), lax.axis_index("c")
     for member, near, far in ((core, own_ref, own_far_ref), (1 - core, got_ref, got_far_ref)):
-        for k, step in enumerate((0, 3 - 2 * member, 2, 1 + 2 * member)):
+        for k, step in enumerate((0, 3 - 2 * member, 1 + 2 * member, 2)):
             at = lax.rem(chip + step, 4) * 1024 + member * 512
             block = near[k] if k < 3 else near[k] + far[0]
             proj_ref[:, pl.ds(pl.multiple_of(at, 512), 512)] = block
@@ -371,10 +371,10 @@
     back = [(d, (d + (6, 2)[d % 2]) % 8) for d in range(8)]
     swap = [(0, 1), (1, 0)]
     w_first = lax.ppermute(out_weight, DP, onward)
-    w_far = lax.ppermute(w_first, DP, onward)
+    w_second = lax.ppermute(out_weight, DP, back)
     half = out_weight.shape[0] // 2
-    w_second = lax.ppermute(out_weight[:half], DP, back)
-    w_last = lax.ppermute(out_weight[half:], DP, back)
+    w_far = lax.ppermute(w_first[:half], DP, onward)
+    w_last = lax.ppermute(w_first[half:], DP, onward)
 
     picks = jnp.transpose(routes[0])
     rank, slots = route(picks)
@@ -386,7 +386,7 @@
     attended = attend(by_head)
     own_x = lax.all_to_all(attended, "sp", split_axis=0, concat_axis=0, tiled=True)
     other_x = lax.ppermute(own_x, "c", swap)
-    own, other = project(own_x, other_x, (out_weight, w_first, w_far, w_second))
+    own, other = project(own_x, other_x, (out_weight, w_first, w_second, w_far))
     got = lax.ppermute(other, "c", swap)
     own_far, other_far = project(own_x, other_x, (w_last,), half)
     got_far = lax.ppermute(other_far, "c", swap)

time: 192 us -> 195 us (1.016)
  starting transfers between devices: 18.1 us -> 20.3 us
  blocking collectives: 106 us -> 108 us
    all_to_all x1, waiting for transfers between devices: 4.25 us -> 1.19 us  [layer(): lax.all_to_all(packed, 'sp', split_axis=0, concat_axis=0, tiled=True)]
    ppermute x1, waiting for transfers between devices: 17.8 us -> 20.8 us  [layer(): w_first = lax.ppermute(out_weight, DP, onward)]
    all_to_all x1, blocking collectives: 14.6 us -> 17.5 us  [layer(): lax.all_to_all(attended, 'sp', split_axis=0, concat_axis=0, tiled=True)]
    ppermute x1, starting transfers between devices: 0.09 us -> 2.15 us  [layer(): got_far = lax.ppermute(other_far, 'c', swap)]
where the time goes in v9:
time: 195 us; the launch traced here: 194 us
  blocking collectives  108 us (55%)
  waiting for transfers between devices  32.5 us (17%)
  Pallas kernels  27.6 us (14%)
  starting transfers between devices  20.3 us (10%)
  local copies, waits for them, and re-layouts  4.18 us (2%)
    all_to_all x1, blocking collectives, layer(): lax.all_to_all(result, ALL, split_axis=0, concat_axis=0, tiled=True)  45.6 us
    all_to_all x1, blocking collectives, layer(): lax.all_to_all(outgoing, ALL, split_axis=0, concat_axis=0, tiled=True)  45.2 us
    ppermute x1, waiting for transfers between devices, layer(): w_first = lax.ppermute(out_weight, DP, onward)  20.8 us
    all_to_all x1, blocking collectives, layer(): lax.all_to_all(attended, 'sp', split_axis=0, concat_axis=0, tiled=True)  17.5 us
    pallas_call x1, Pallas kernels, attend(): pl.pallas_call(attend_kernel, out_shape=jax.ShapeDtypeStruct((blocks, 128...  11.5 us
    ppermute x1, waiting for transfers between devices, layer(): w_last = lax.ppermute(w_first[half:], DP, onward)  8.85 us
    all_to_all x1, starting transfers between devices, layer(): lax.all_to_all(packed, 'sp', split_axis=0, concat_axis=0, tiled=True)  7.64 us
    pallas_call x1, Pallas kernels, run_experts(): pl.pallas_call(expert_kernel, out_shape=jax.ShapeDtypeStruct(x.shape, BF1...  6.74 us
  transfers between devices with their start and end apart: 8, of which 5 were waited for; matrix products, arithmetic and copies ran while one was open for 3% of the time, Pallas kernels for 8%

profile of v9, /device:TPU:1, one launch (start us, length us, event | category | flops | bytes accessed | tf_op | source)
XLA Modules:
  0.0 194.5 jit_solution(11411724798629193578)
XLA Ops:
  0.0 3.6 %collective-permute-start.1 = (bf16[2048,512]{1,0:T(8,128)(2,1)}, bf16[2048,512]{1,0:T(8,128)(2,1)S(1)}, u32[]{:S(2)}, u32[]{:S(2)}) collective-permute-start(bf16[2048,512]{1,0:T(8,128)(2,1)} %refs_0_.1), channel_id=1, source_target_pairs={{0,2},{1,7},{2,4},{3,1},{4,6},{5,3},{6,0},{7,5},{8,10},{9,15},{10,... | collective-permute-start | bytes 6291464 | tf_op jit(solution)/shard_map/ppermute | solution.py:373
  3.6 1.2 copy.20
  4.7 1.5 copy_bitcast_fusion
  6.2 1.3 pad_maximum_fusion
  7.5 7.6 %all-to-all-start = ((bf16[16,384,128]{2,1,0:T(8,128)(2,1)}), bf16[16,384,128]{2,1,0:T(8,128)(2,1)}, u32[]{:S(2)}, u32[]{:S(2)}) async-start(bf16[16,384,128]{2,1,0:T(8,128)(2,1)} %pad_maximum_fusion), calls=%async_computation | async-start | bytes 3145728 | tf_op jit(solution)/shard_map/all_to_all | solution.py:385
  15.1 0.1 collective-permute-start.2
  15.2 20.8 %collective-permute-done.1.refs_1_ = bf16[2048,512]{1,0:T(8,128)(2,1)S(1)} collective-permute-done((bf16[2048,512]{1,0:T(8,128)(2,1)}, bf16[2048,512]{1,0:T(8,128)(2,1)S(1)}, u32[]{:S(2)}, u32[]{:S(2)}) %collective-permute-start.1) | collective-permute-done | bytes 2097184 | tf_op jit(solution)/shard_map/ppermute | solution.py:373
  36.0 1.5 fusion
  37.5 3.4 %collective-permute-start.3 = (bf16[1024,512]{1,0:T(8,128)(2,1)}, bf16[1024,512]{1,0:T(8,128)(2,1)S(1)}, u32[]{:S(2)}, u32[]{:S(2)}) collective-permute-start(bf16[1024,512]{1,0:T(8,128)(2,1)} %get-tuple-element.22), channel_id=1, source_target_pairs={{0,2},{1,7},{2,4},{3,1},{4,6},{5,3},{6,0},{7,5},{8,10},{9,15},{10,... | collective-permute-start | bytes 3145736 | tf_op jit(solution)/shard_map/ppermute | solution.py:376
  40.9 1.2 all-to-all-done.x_ref
  42.1 11.5 %attend.1 = bf16[16,128,128]{2,1,0:T(8,128)(2,1)S(1)} custom-call(bf16[16,384,128]{2,1,0:T(8,128)(2,1)} %all-to-all-done.x_ref), custom_call_target="tpu_custom_call" | custom-call | flops 12000000000 | bytes 3000000 | tf_op jit(solution)/shard_map/attend/pallas_call | solution.py:77
  53.6 17.5 %all_to_all.20.own_x_ref = bf16[16,128,128]{2,1,0:T(8,128)(2,1)S(1)} all-to-all(bf16[16,128,128]{2,1,0:T(8,128)(2,1)S(1)} %attend.1), channel_id=1, replica_groups=mesh['sp'=16,'yh'=2,'yl'=2,'c'=2] {'sp'}, dimensions={0} | all-to-all | bytes 1048576 | tf_op jit(solution)/shard_map/all_to_all | solution.py:387
  71.1 2.2 %collective-permute-start = (bf16[16,128,128]{2,1,0:T(8,128)(2,1)S(1)}, bf16[16,128,128]{2,1,0:T(8,128)(2,1)S(1)}, u32[]{:S(2)}, u32[]{:S(2)}) collective-permute-start(bf16[16,128,128]{2,1,0:T(8,128)(2,1)S(1)} %all_to_all.20.own_x_ref), channel_id=1, source_target_pairs={{0,1},{1,0},{2,3},{3,2},{4,5},{5,4},{6,7},{7,6},{8,9},{9,8},{10,11... | collective-permute-start | bytes 1572872 | tf_op jit(solution)/shard_map/ppermute | solution.py:388
  73.4 0.0 copy-done.10
  73.4 0.8 collective-permute-start.4
  74.1 0.0 collective-permute-done.2.refs_2_
  74.1 0.8 collective-permute-done.other_x_ref
  74.9 0.0 collective-permute-done.3.refs_3_
  74.9 0.0 copy-done.9
  74.9 3.0 %shard_map.127 = (f32[4,128,512]{2,1,0:T(8,128)S(1)}, f32[4,128,512]{2,1,0:T(8,128)S(1)}) custom-call(bf16[16,128,128]{2,1,0:T(8,128)(2,1)S(1)} %all_to_all.20.own_x_ref, bf16[16,128,128]{2,1,0:T(8,128)(2,1)S(1)} %collective-permute-done.other_x_ref, bf16[2048,512]{1,0:T(8,128)(2,1)S(1)} %copy-done.9, bf16[2048,512]{1,0:T(8,128)(2,1)S(1)} %collective-permute-done.1.refs_1_, ...), custom_call_target="tpu_custom_call" | custom-call | flops 4000000000 | bytes 12000000 | tf_op jit(solution)/shard_map/pallas_call | solution.py:164
  78.0 0.0 copy-start.4
  78.0 0.0 copy-start
  78.0 0.0 copy-start.1
  78.0 0.0 copy-start.2
  78.0 0.5 collective-permute-start.5
  78.5 8.8 %collective-permute-done.4.refs_0_ = bf16[1024,512]{1,0:T(8,128)(2,1)S(1)} collective-permute-done((bf16[1024,512]{1,0:T(8,128)(2,1)S(1)}, bf16[1024,512]{1,0:T(8,128)(2,1)S(1)}, u32[]{:S(2)}, u32[]{:S(2)}) %collective-permute-start.4) | collective-permute-done | bytes 1048608 | tf_op jit(solution)/shard_map/ppermute | solution.py:377
  87.3 0.5 shard_map.128
  87.9 2.1 %collective-permute-start.6 = (f32[1,128,512]{2,1,0:T(8,128)S(1)}, f32[1,128,512]{2,1,0:T(8,128)S(1)}, u32[]{:S(2)}, u32[]{:S(2)}) collective-permute-start(f32[1,128,512]{2,1,0:T(8,128)S(1)} %get-tuple-element.18), channel_id=1, source_target_pairs={{0,1},{1,0},{2,3},{3,2},{4,5},{5,4},{6,7},{7,6},{8,9},{9,8},{10,11... | collective-permute-start | bytes 786440 | tf_op jit(solution)/shard_map/ppermute | solution.py:392
  90.0 0.0 copy-done.4
  90.0 0.3 route.1
  90.3 0.9 collective-permute-done.6.got_far_ref
  91.2 0.0 collective-permute-done.5.got_ref
  91.2 0.0 copy-done
  91.2 0.0 copy-done.1
  91.2 0.0 copy-done.2
  91.2 0.0 copy-start.7
  91.2 2.8 %mix.1 = (bf16[128,32,128]{2,1,0:T(8,128)(2,1)S(1)}, bf16[128,96,128]{2,1,0:T(8,128)(2,1)S(1)}) custom-call(s32[8,128]{1,0:T(8,128)S(1)} %get-tuple-element.14.slot_ref, f32[4,128,512]{2,1,0:T(8,128)S(1)} %get-tuple-element.15.own_ref, f32[1,128,512]{2,1,0:T(8,128)S(1)} %get-tuple-element.16.own_far_ref, f32[4,128,512]{2,1,0:T(8,128)S(1)} %collective-permute-done.5.got_ref, ...), custom_call_target="tpu_custom_call" | custom-call | flops 1000000000 | bytes 8000000 | tf_op jit(solution)/shard_map/mix/pallas_call | solution.py:231
  94.0 0.0 copy-start.6
  94.0 45.2 %all_to_all.21.x_ref = bf16[128,96,128]{2,1,0:T(8,128)(2,1)S(1)} all-to-all(bf16[128,96,128]{2,1,0:T(8,128)(2,1)S(1)} %get-tuple-element.19), channel_id=1, replica_groups=mesh['sp'=16,'yh'=2,'yl'=2,'c'=2] {'sp','yh','yl','c'}, dimensions={0} | all-to-all | bytes 6291456 | tf_op jit(solution)/shard_map/all_to_all | solution.py:397
  139.3 0.0 copy-done.8
  139.3 0.0 copy-done.7
  139.3 0.0 copy-done.6
  139.3 6.7 %experts.1 = bf16[128,96,128]{2,1,0:T(8,128)(2,1)S(1)} custom-call(bf16[128,96,128]{2,1,0:T(8,128)(2,1)S(1)} %all_to_all.21.x_ref, bf16[4096,512]{1,0:T(8,128)(2,1)S(1)} %bitcast.34, bf16[4096,512]{1,0:T(8,128)(2,1)S(1)} %bitcast.35, bf16[512,4096]{1,0:T(8,128)(2,1)S(1)} %bitcast.36), custom_call_target="tpu_custom_call" | custom-call | flops 6000000000 | bytes 19000000 | tf_op jit(solution)/shard_map/experts/pallas_call | solution.py:295
  146.0 0.0 copy-start.3
  146.1 0.0 copy-start.5
  146.1 45.6 %all_to_all.22.x_ref = bf16[128,96,128]{2,1,0:T(8,128)(2,1)S(1)} all-to-all(bf16[128,96,128]{2,1,0:T(8,128)(2,1)S(1)} %experts.1), channel_id=1, replica_groups=mesh['sp'=16,'yh'=2,'yl'=2,'c'=2] {'sp','yh','yl','c'}, dimensions={0} | all-to-all | bytes 6291456 | tf_op jit(solution)/shard_map/all_to_all | solution.py:399
  191.7 0.0 copy-done.5
  191.7 2.6 %combine.1 = bf16[128,4096]{1,0:T(8,128)(2,1)} custom-call(s32[2,128]{1,0:T(2,128)S(1)} %bitcast.32, s32[2,128]{1,0:T(2,128)S(1)} %get-tuple-element.13.rank_ref, f32[2,128]{1,0:T(2,128)S(1)} %bitcast.33, bf16[128,96,128]{2,1,0:T(8,128)(2,1)S(1)} %all_to_all.22.x_ref, bf16[128,32,128]{2,1,0:T(8,128)(2,1)S(1)} %get-tuple-element.20.stream_ref, ...), custom_call_target="tpu_custom_call" | custom-call | flops 1000000000 | bytes 6000000 | tf_op jit(solution)/shard_map/combine/pallas_call | solution.py:354
  (4 shorter events, 0.0 us)
Async XLA Ops:
  0.0 36.0 %collective-permute-start.1 = (bf16[2048,512]{1,0:T(8,128)(2,1)}, bf16[2048,512]{1,0:T(8,128)(2,1)S(1)}, u32[]{:S(2)}, u32[]{:S(2)}) collective-permute-start(bf16[2048,512]{1,0:T(8,128)(2,1)} %refs_0_.1), channel_id=1, source_target_pairs={{0,2},{1,7},{2,4},{3,1},{4,6},{5,3},{6,0},{7,5},{8,10},{9,15},{10,... | collective-permute-start | bytes 6291464 | tf_op jit(solution)/shard_map/ppermute | solution.py:373
  7.5 34.6 %all-to-all-start = ((bf16[16,384,128]{2,1,0:T(8,128)(2,1)}), bf16[16,384,128]{2,1,0:T(8,128)(2,1)}, u32[]{:S(2)}, u32[]{:S(2)}) async-start(bf16[16,384,128]{2,1,0:T(8,128)(2,1)} %pad_maximum_fusion), calls=%async_computation | async-start | bytes 3145728 | tf_op jit(solution)/shard_map/all_to_all | solution.py:385
  15.1 59.0 %collective-permute-start.2 = (bf16[2048,512]{1,0:T(8,128)(2,1)}, bf16[2048,512]{1,0:T(8,128)(2,1)}, u32[]{:S(2)}, u32[]{:S(2)}) collective-permute-start(bf16[2048,512]{1,0:T(8,128)(2,1)} %refs_0_.1), channel_id=1, source_target_pairs={{0,6},{1,3},{2,0},{3,5},{4,2},{5,7},{6,4},{7,1},{8,14},{9,11},{10,... | collective-permute-start | bytes 6291464 | tf_op jit(solution)/shard_map/ppermute | solution.py:374
  37.5 37.4 %collective-permute-start.3 = (bf16[1024,512]{1,0:T(8,128)(2,1)}, bf16[1024,512]{1,0:T(8,128)(2,1)S(1)}, u32[]{:S(2)}, u32[]{:S(2)}) collective-permute-start(bf16[1024,512]{1,0:T(8,128)(2,1)} %get-tuple-element.22), channel_id=1, source_target_pairs={{0,2},{1,7},{2,4},{3,1},{4,6},{5,3},{6,0},{7,5},{8,10},{9,15},{10,... | collective-permute-start | bytes 3145736 | tf_op jit(solution)/shard_map/ppermute | solution.py:376
  42.1 31.3 %copy-start.10 = (bf16[1024,512]{1,0:T(8,128)(2,1)S(1)}, bf16[1024,512]{1,0:T(8,128)(2,1)}, u32[]{:S(2)}) copy-start(bf16[1024,512]{1,0:T(8,128)(2,1)} %get-tuple-element.21) | copy-start | bytes 3145732
  42.1 32.8 %copy-start.9 = (bf16[2048,512]{1,0:T(8,128)(2,1)S(1)}, bf16[2048,512]{1,0:T(8,128)(2,1)}, u32[]{:S(2)}) copy-start(bf16[2048,512]{1,0:T(8,128)(2,1)} %refs_0_.1) | copy-start | bytes 6291460
  71.1 3.8 %collective-permute-start = (bf16[16,128,128]{2,1,0:T(8,128)(2,1)S(1)}, bf16[16,128,128]{2,1,0:T(8,128)(2,1)S(1)}, u32[]{:S(2)}, u32[]{:S(2)}) collective-permute-start(bf16[16,128,128]{2,1,0:T(8,128)(2,1)S(1)} %all_to_all.20.own_x_ref), channel_id=1, source_target_pairs={{0,1},{1,0},{2,3},{3,2},{4,5},{5,4},{6,7},{7,6},{8,9},{9,8},{10,11... | collective-permute-start | bytes 1572872 | tf_op jit(solution)/shard_map/ppermute | solution.py:388
  73.4 13.9 %collective-permute-start.4 = (bf16[1024,512]{1,0:T(8,128)(2,1)S(1)}, bf16[1024,512]{1,0:T(8,128)(2,1)S(1)}, u32[]{:S(2)}, u32[]{:S(2)}) collective-permute-start(bf16[1024,512]{1,0:T(8,128)(2,1)S(1)} %copy-done.10), channel_id=1, source_target_pairs={{0,2},{1,7},{2,4},{3,1},{4,6},{5,3},{6,0},{7,5},{8,10},{9,15},{10,... | collective-permute-start | bytes 3145736 | tf_op jit(solution)/shard_map/ppermute | solution.py:377
  78.0 12.1 %copy-start.4 = (s32[1,128,2]{1,2,0:T(2,128)S(1)}, s32[1,128,2]{1,2,0:T(2,128)}, u32[]{:S(2)}) copy-start(s32[1,128,2]{1,2,0:T(2,128)} %param.23) | copy-start | bytes 3076
  78.0 13.2 %copy-start = (bf16[1,128,4096]{2,1,0:T(8,128)(2,1)S(1)}, bf16[1,128,4096]{2,1,0:T(8,128)(2,1)}, u32[]{:S(2)}) copy-start(bf16[1,128,4096]{2,1,0:T(8,128)(2,1)} %param.16) | copy-start | bytes 3145732
  78.0 13.2 %copy-start.1 = (f32[4096]{0:T(1024)S(1)}, f32[4096]{0:T(1024)}, u32[]{:S(2)}) copy-start(f32[4096]{0:T(1024)} %param.18) | copy-start | bytes 49156
  78.0 13.2 %copy-start.2 = (f32[4096]{0:T(1024)S(1)}, f32[4096]{0:T(1024)}, u32[]{:S(2)}) copy-start(f32[4096]{0:T(1024)} %param.19) | copy-start | bytes 49156
  78.0 13.2 %collective-permute-start.5 = (f32[4,128,512]{2,1,0:T(8,128)S(1)}, f32[4,128,512]{2,1,0:T(8,128)S(1)}, u32[]{:S(2)}, u32[]{:S(2)}) collective-permute-start(f32[4,128,512]{2,1,0:T(8,128)S(1)} %get-tuple-element.17), channel_id=1, source_target_pairs={{0,1},{1,0},{2,3},{3,2},{4,5},{5,4},{6,7},{7,6},{8,9},{9,8},{10,11... | collective-permute-start | bytes 3145736 | tf_op jit(solution)/shard_map/ppermute | solution.py:390
  87.3 52.0 %copy-start.8 = (bf16[1,512,4096]{2,1,0:T(8,128)(2,1)S(1)}, bf16[1,512,4096]{2,1,0:T(8,128)(2,1)}, u32[]{:S(2)}) copy-start(bf16[1,512,4096]{2,1,0:T(8,128)(2,1)} %param.22) | copy-start | bytes 12582916
  87.9 3.3 %collective-permute-start.6 = (f32[1,128,512]{2,1,0:T(8,128)S(1)}, f32[1,128,512]{2,1,0:T(8,128)S(1)}, u32[]{:S(2)}, u32[]{:S(2)}) collective-permute-start(f32[1,128,512]{2,1,0:T(8,128)S(1)} %get-tuple-element.18), channel_id=1, source_target_pairs={{0,1},{1,0},{2,3},{3,2},{4,5},{5,4},{6,7},{7,6},{8,9},{9,8},{10,11... | collective-permute-start | bytes 786440 | tf_op jit(solution)/shard_map/ppermute | solution.py:392
  91.2 48.1 %copy-start.7 = (bf16[1,4096,512]{2,1,0:T(8,128)(2,1)S(1)}, bf16[1,4096,512]{2,1,0:T(8,128)(2,1)}, u32[]{:S(2)}) copy-start(bf16[1,4096,512]{2,1,0:T(8,128)(2,1)} %param.21) | copy-start | bytes 12582916
  94.0 45.3 %copy-start.6 = (bf16[1,4096,512]{2,1,0:T(8,128)(2,1)S(1)}, bf16[1,4096,512]{2,1,0:T(8,128)(2,1)}, u32[]{:S(2)}) copy-start(bf16[1,4096,512]{2,1,0:T(8,128)(2,1)} %param.20) | copy-start | bytes 12582916
  146.0 45.7 %copy-start.3 = (f32[4096]{0:T(1024)S(1)}, f32[4096]{0:T(1024)}, u32[]{:S(2)}) copy-start(f32[4096]{0:T(1024)} %param.25) | copy-start | bytes 49156
  146.1 45.6 %copy-start.5 = (f32[1,128,2]{1,2,0:T(2,128)S(1)}, f32[1,128,2]{1,2,0:T(2,128)}, u32[]{:S(2)}) copy-start(f32[1,128,2]{1,2,0:T(2,128)} %param.24) | copy-start | bytes 3076
